TPU v7x, 512 devices: a whole 4x8x8 slice. The times are simulated.
512 devices in a mesh: sp: 32 (over z, x), tp: 16 (over y, core).
Axes of the slice: x: 4, y: 8, z: 8, core: 2. Of those that a mesh axis runs over, the one named last changes fastest.
Arguments:
- glu_value: bfloat16 [6144, 1024], P('sp', 'tp'), may hold values from -6 to 6
- glu_gate: bfloat16 [6144, 1024], P('sp', 'tp'), may hold values from -6 to 6
- doc_ids: int32 [6144], P('sp'), may hold values from 0 to 15, never falling along the last dimension, each value on 1 to 768 neighbouring positions
- conv_kernel: bfloat16 [31, 1024], P(None, 'tp')
- conv_gain: float32 [1024], P('tp'), may hold values from 0.1 to 1.9
- out_weight: bfloat16 [1024, 2048], P('tp'), may hold values from -0.1875 to 0.1875
- residual: bfloat16 [6144, 2048], P('sp'), may hold values from -6 to 6
- mix_gain: float32 [2048], replicated, may hold values from 0.1 to 1.9
- routes: int32 [6144, 2], P('sp'), may hold values from 0 to 31, all different within a row; in each aligned block of 192 rows (0 to 191, 192 to 383, ...) at most 24 rows name the same one
- route_weights: float32 [6144, 2], P('sp'), may hold values from 0.2 to 1
- expert_gate: bfloat16 [32, 2048, 5120], P('sp', None, 'tp'), may hold values from -0.125 to 0.125
- expert_up: bfloat16 [32, 2048, 5120], P('sp', None, 'tp'), may hold values from -0.125 to 0.125
- expert_down: bfloat16 [32, 5120, 2048], P('sp', 'tp')
- final_gain: float32 [2048], P('tp'), may hold values from 0.1 to 1.9
Outputs:
- block_out: bfloat16 [6144, 2048], P('sp', 'tp')
Inputs may be any that keep to these rules, and one draw needn't show every extreme that they name: `routes`: each row names two different experts. In each aligned block of 192 rows no expert is named by more than 24 rows, and in every draw some block has an expert named by exactly 24 rows. `doc_ids`: document numbers never fall along the sequence.
All inputs are finite; a program needn't handle non-finite values.
Results may differ from a plain program's by a relative error of at most 0.022.
Values may be sent and summed in bfloat16 or wider, within the bound.
No kernel may reach another device: no remote copies, remote signals or barrier semaphores. Data moves between devices by JAX's collectives and lax.ppermute only.
A program may use at most 64 MiB of HBM per device.

v0:
```python
import jax
import jax.numpy as jnp
from jax import lax
from jax.sharding import Mesh
from jax.sharding import PartitionSpec as P

TP = ("tp_0", "tp_1")


residual_alpha = 1.41421356
norm_eps = 1e-05


def from_behind(value, axis, by):
    peers = lax.axis_size(axis)
    pairs = [(i, i + by) for i in range(peers) if 0 <= i + by < peers]
    return lax.ppermute(value, axis, pairs)


def copy_for_each(value, axis):
    peers = lax.axis_size(axis)
    return lax.all_to_all(
        jnp.broadcast_to(value[None], (peers, *value.shape)), axis, 0, 0, tiled=True
    )


def over_copies(value, axis):
    everything = copy_for_each(value, axis)
    return jnp.sum(everything, axis=0)


def in_one(arrays, axis):
    line, at, finished = (jnp.concatenate([a.reshape(-1) for a in arrays]), 0, [])
    subtotal = over_copies(line, axis)
    for a in arrays:
        finished.append(subtotal[at : at + a.size].reshape(a.shape))
        at += a.size
    return tuple(finished)


def over_pieces(value, axis):
    return lax.all_gather(value, axis).astype(jnp.float32).sum(0)


def summed_rows(value, axes, dim):
    for axis in axes:
        value = lax.psum_scatter(value, axis, scatter_dimension=dim, tiled=True)
    return value


def scaled_norm(pre_norm, gain):
    row_mean = jnp.mean(pre_norm, -1, keepdims=True)
    row_var = jnp.mean(pre_norm * pre_norm, -1, keepdims=True) - row_mean * row_mean
    return (pre_norm - row_mean) * lax.rsqrt(row_var + norm_eps) * gain


def local(
    glu_value,
    glu_gate,
    doc_ids,
    conv_kernel,
    conv_gain,
    out_weight,
    residual,
    mix_gain,
    routes,
    route_weights,
    expert_gate,
    expert_up,
    expert_down,
    final_gain,
):
    tok_rows = glu_value.shape[0]
    rim_len = conv_kernel.shape[0] - 1
    channels = glu_value.shape[1] * lax.axis_size(TP)
    gated_rows = (
        glu_value.astype(jnp.float32) * jax.nn.sigmoid(glu_gate.astype(jnp.float32))
    ).astype(jnp.bfloat16)
    rim_rows, rim_ids = from_behind(
        (gated_rows[tok_rows - rim_len :], doc_ids[tok_rows - rim_len :]), "sp", 1
    )
    extended = jnp.concatenate([rim_rows, gated_rows], 0).astype(jnp.float32)
    ext_ids = jnp.concatenate([rim_ids, doc_ids], 0)
    kernel = conv_kernel.astype(jnp.float32)
    filtered = jnp.zeros(gated_rows.shape, jnp.float32)
    for shift_by in range(rim_len + 1):
        begin_at = rim_len - shift_by
        same_doc = (ext_ids[begin_at : begin_at + tok_rows] == doc_ids)[:, None]
        filtered = (
            filtered
            + jnp.where(same_doc, extended[begin_at : begin_at + tok_rows], 0.0) * kernel[shift_by]
        )
    row_sum, row_square = in_one((jnp.sum(filtered, 1), jnp.sum(filtered * filtered, 1)), TP)
    row_mean = row_sum[:, None] / channels
    row_var = row_square[:, None] / channels - row_mean * row_mean
    conv_out = jax.nn.silu(
        (filtered - row_mean) * lax.rsqrt(row_var + norm_eps) * conv_gain
    ).astype(jnp.bfloat16)
    mix_total = over_pieces(
        jnp.dot(conv_out, out_weight, preferred_element_type=jnp.float32).astype(jnp.bfloat16), TP
    ).astype(jnp.float32)
    mixed_rows = scaled_norm(
        residual_alpha * residual.astype(jnp.float32) + mix_total, mix_gain
    ).astype(jnp.bfloat16)
    experts = expert_gate.shape[0] * lax.axis_size("sp")
    capacity = 4 * tok_rows // experts
    chosen = routes.reshape(-1)
    member = (chosen[:, None] == jnp.arange(experts, dtype=jnp.int32)[None, :]).astype(jnp.int32)
    earlier = jnp.cumsum(member, 0) - member
    slot_index = chosen * capacity + jnp.sum(earlier * member, 1)
    dispatch_table = jnp.any(
        jnp.arange(experts * capacity, dtype=jnp.int32)[:, None, None]
        == slot_index.reshape(tok_rows, 2)[None],
        -1,
    ).astype(jnp.bfloat16)
    feat_block = mixed_rows.shape[1] // lax.axis_size(TP)
    offset = lax.axis_index(TP) * feat_block
    w_gate = expert_gate[0]
    w_up = expert_up[0]
    w_down = expert_down[0]
    row_slice = lax.dynamic_slice_in_dim(mixed_rows, offset, feat_block, 1)
    outgoing = (
        jnp.dot(dispatch_table, row_slice, preferred_element_type=jnp.float32)
        .astype(jnp.bfloat16)
        .reshape(experts, capacity, feat_block)
    )
    arrived = lax.all_to_all(outgoing, "sp", split_axis=0, concat_axis=0, tiled=True)
    sources, slot_count, part_width = arrived.shape
    flat_rows = arrived.reshape(sources * slot_count, part_width)
    col_piece = lax.all_gather(flat_rows, TP, axis=1, tiled=True)
    gate_proj = jnp.dot(col_piece, w_gate, preferred_element_type=jnp.float32)
    up_proj = jnp.dot(col_piece, w_up, preferred_element_type=jnp.float32)
    hidden = (jax.nn.silu(gate_proj) * up_proj).astype(jnp.bfloat16)
    partial_value = jnp.dot(hidden, w_down, preferred_element_type=jnp.float32).reshape(
        sources, slot_count, -1
    )
    summed = (
        summed_rows(partial_value.astype(jnp.bfloat16), TP, 2)
        .astype(jnp.float32)
        .astype(jnp.bfloat16)
    )
    returned = lax.all_to_all(summed, "sp", split_axis=0, concat_axis=0, tiled=True)
    flat_back = returned.reshape(experts * capacity, feat_block)
    picked = flat_back[slot_index].astype(jnp.float32).reshape(tok_rows, 2, feat_block)
    moe_sum = jnp.sum(route_weights[:, :, None] * picked, 1)
    own_cols = lax.dynamic_slice_in_dim(mixed_rows, offset, feat_block, 1).astype(jnp.float32)
    pre_norm = residual_alpha * own_cols + moe_sum
    fin_sum, fin_square = in_one((jnp.sum(pre_norm, 1), jnp.sum(pre_norm * pre_norm, 1)), TP)
    features = feat_block * lax.axis_size(TP)
    fin_mean = fin_sum[:, None] / features
    fin_var = fin_square[:, None] / features - fin_mean * fin_mean
    return ((pre_norm - fin_mean) * lax.rsqrt(fin_var + norm_eps) * final_gain).astype(jnp.bfloat16)


def solution(mesh):
    finer = Mesh(mesh.devices.reshape(mesh.shape["sp"], 8, 2), ("sp", "tp_0", "tp_1"))
    placed = (
        P("sp", TP),
        P("sp", TP),
        P("sp"),
        P(None, TP),
        P(TP),
        P(TP, None),
        P("sp", None),
        P(),
        P("sp", None),
        P("sp", None),
        P("sp", None, TP),
        P("sp", None, TP),
        P("sp", TP, None),
        P(TP),
    )
    return jax.shard_map(local, mesh=finer, in_specs=placed, out_specs=P("sp", TP), check_vma=False)
```

profile of v0, /device:TPU:1, one launch (start us, length us, event | category | flops | bytes accessed | tf_op | source)
XLA Modules:
  0.0 322.3 jit_solution(10232544135182544080)
XLA Ops:
  6.5 0.9 slice.303
  7.4 3.9 %collective-permute-start.1 = (s32[30]{0:T(128)S(1)}, s32[30]{0:T(128)S(1)}, u32[]{:S(2)}, u32[]{:S(2)}) collective-permute-start(s32[30]{0:T(128)S(1)} %slice.303), channel_id=1, source_target_pairs={{0,16},{16,32},{32,48},{48,64},{64,80},{80,96},{96,112},{112,128},... | collective-permute-start | bytes 368 | tf_op jit(solution)/shard_map/ppermute | solution.py:17
  11.3 0.8 multiply_convert_fusion.2
  12.2 3.1 collective-permute-start
  16.8 0.8 slice_compare_fusion.29
  17.6 0.8 slice_compare_fusion.28
  18.5 0.9 fusion.85
  19.5 15.5 %all_to_all.22 = f32[16,1,384]{2,1,0:T(1,128)S(1)} all-to-all(f32[16,1,384]{2,1,0:T(1,128)S(1)} %broadcast_in_dim.277), channel_id=1, replica_groups=mesh['sp'=32,'tp_0'=8,'tp_1'=2] {'tp_0','tp_1'}, dimensions={0} | all-to-all | bytes 49152 | tf_op jit(solution)/shard_map/all_to_all | solution.py:22
  35.1 1.4 convolution_convert_fusion.1
  37.1 0.9 reduce-window.6
  38.6 0.8 dynamic-slice
  39.5 74.9 %all-gather.6.cloned.1.call-done = bf16[3072,2048]{1,0:T(8,128)(2,1)} async-done(((bf16[192,2048]{1,0:T(8,128)(2,1)}), bf16[3072,2048]{1,0:T(8,128)(2,1)}) %all-gather.6.cloned.1.call-update) | async-done | bytes 12582928 | tf_op jit(solution)/shard_map/all_gather | solution.py:42
  114.4 7.7 %convert_reduce_fusion = f32[192,2048]{1,0:T(8,128)S(1)} fusion(bf16[16,192,2048]{2,1,0:T(8,128)(2,1)} %bitcast.110), kind=kLoop, calls=%fused_computation.1 | loop fusion | flops 12189696 | bytes 14155776 | tf_op jit(solution)/shard_map/reduce_sum | solution.py:42
  122.1 1.5 fusion.84
  123.6 1.1 copy-done.1
  125.2 20.4 %all_to_all.23 = bf16[32,24,128]{2,1,0:T(8,128)(2,1)} all-to-all(bf16[32,24,128]{2,1,0:T(8,128)(2,1)S(1)} %bitcast.117), channel_id=1, replica_groups=mesh['sp'=32,'tp_0'=8,'tp_1'=2] {'sp'}, dimensions={0} | all-to-all | bytes 393216 | tf_op jit(solution)/shard_map/all_to_all | solution.py:127
  145.7 42.2 %all-gather.4.cloned.1.call-done = bf16[768,2048]{1,0:T(8,128)(2,1)} async-done(((bf16[768,128]{1,0:T(8,128)(2,1)}), bf16[768,2048]{1,0:T(8,128)(2,1)}) %all-gather.4.cloned.1.call-update) | async-done | bytes 3145744 | tf_op jit(solution)/shard_map/all_gather | solution.py:130
  187.9 3.6 %fusion.2 = f32[768,320]{0,1:T(8,128)S(1)} fusion(bf16[768,2048]{1,0:T(8,128)(2,1)} %all-gather.4.cloned.1.call-done, bf16[1,2048,320]{1,2,0:T(8,128)(2,1)} %param.24), kind=kOutput, calls=%fused_computation.9 | convolution fusion | flops 1006632960 | bytes 5439488 | tf_op jit(solution)/shard_map/dot_general | solution.py:131
  191.6 2.7 fusion.4
  194.6 3.5 %convolution_convert_fusion = bf16[32,24,2048]{2,1,0:T(8,128)(2,1)} fusion(bf16[32,24,320]{2,1,0:T(8,128)(2,1)S(1)} %bitcast.115, bf16[1,320,2048]{2,1,0:T(8,128)(2,1)S(1)} %copy-done), kind=kOutput, calls=%fused_computation.2 | convolution fusion | flops 1008205824 | bytes 4947968 | tf_op jit(solution)/shard_map/dot_general | solution.py:134
  198.3 44.2 %reduce-scatter.5.cloned.1.call-done = bf16[32,24,256]{2,1,0:T(8,128)(2,1)} async-done(((bf16[32,24,2048]{2,1,0:T(8,128)(2,1)}), bf16[32,24,256]{2,1,0:T(8,128)(2,1)}) %reduce-scatter.5.cloned.1.call-update) | async-done | bytes 393232 | tf_op jit(solution)/shard_map/reduce_scatter | solution.py:47
  242.5 3.8 %copy.46 = bf16[32,24,256]{1,0,2:T(8,128)(2,1)S(1)} copy(bf16[32,24,256]{2,1,0:T(8,128)(2,1)} %reduce-scatter.5.cloned.1.call-done) | data formatting | bytes 786432
  246.3 4.2 %reshape.163 = bf16[256,768]{1,0:T(8,128)(2,1)} reshape(bf16[256,32,24]{2,1,0:T(8,128)(2,1)S(1)} %bitcast.111) | data formatting | bytes 786432
  250.6 20.5 %reduce-scatter.7.cloned.1.call-done = bf16[128,768]{1,0:T(8,128)(2,1)} async-done(((bf16[256,768]{1,0:T(8,128)(2,1)}), bf16[128,768]{1,0:T(8,128)(2,1)}) %reduce-scatter.7.cloned.1.call-update) | async-done | bytes 196624
  271.1 2.6 reshape.164
  273.7 1.7 copy.47
  275.5 8.9 %all-to-all-start.2 = ((bf16[32,24,128]{2,1,0:T(8,128)(2,1)}), bf16[32,24,128]{2,1,0:T(8,128)(2,1)S(1)}, u32[]{:S(2)}, u32[]{:S(2)}) async-start(bf16[32,24,128]{2,1,0:T(8,128)(2,1)} %copy.47), calls=%async_computation.3 | async-start | bytes 393216 | tf_op jit(solution)/shard_map/all_to_all | solution.py:142
  284.7 10.3 %all-to-all-done.2 = bf16[32,24,128]{2,1,0:T(8,128)(2,1)S(1)} async-done(((bf16[32,24,128]{2,1,0:T(8,128)(2,1)}), bf16[32,24,128]{2,1,0:T(8,128)(2,1)S(1)}, u32[]{:S(2)}, u32[]{:S(2)}) %all-to-all-start.2) | async-done | bytes 196640 | tf_op jit(solution)/shard_map/all_to_all | solution.py:142
  295.0 1.4 gather_fusion
  296.8 1.1 fusion.80
  298.0 15.9 %all_to_all.24 = f32[16,1,384]{2,1,0:T(1,128)S(1)} all-to-all(f32[16,1,384]{2,1,0:T(1,128)S(1)} %broadcast_in_dim.278), channel_id=1, replica_groups=mesh['sp'=32,'tp_0'=8,'tp_1'=2] {'tp_0','tp_1'}, dimensions={0} | all-to-all | bytes 49152 | tf_op jit(solution)/shard_map/all_to_all | solution.py:22
  314.1 1.7 multiply_convert_fusion
  (58 shorter events, 5.0 us)
Async XLA Ops:
  6.5 188.0 %copy-start = (bf16[1,320,2048]{2,1,0:T(8,128)(2,1)S(1)}, bf16[1,320,2048]{2,1,0:T(8,128)(2,1)}, u32[]{:S(2)}) copy-start(bf16[1,320,2048]{2,1,0:T(8,128)(2,1)} %param.26) | copy-start | bytes 3932164
  6.5 28.6 %copy-start.5 = (f32[64]{0:T(128)S(1)}, f32[64]{0:T(128)}, u32[]{:S(2)}) copy-start(f32[64]{0:T(128)} %param.18) | copy-start | bytes 772
  6.5 28.6 %copy-start.2 = (bf16[64,2048]{1,0:T(8,128)(2,1)S(1)}, bf16[64,2048]{1,0:T(8,128)(2,1)}, u32[]{:S(2)}) copy-start(bf16[64,2048]{1,0:T(8,128)(2,1)} %param.19) | copy-start | bytes 786436
  6.5 107.8 %all-gather.6.cloned.1.call-start = ((), (), s32[]{:S(2)}) async-start(), calls=%async_computation.8 | async-start | bytes 13369344 | tf_op jit(solution)/shard_map/all_gather | solution.py:42
  7.4 8.7 %collective-permute-start.1 = (s32[30]{0:T(128)S(1)}, s32[30]{0:T(128)S(1)}, u32[]{:S(2)}, u32[]{:S(2)}) collective-permute-start(s32[30]{0:T(128)S(1)} %slice.303), channel_id=1, source_target_pairs={{0,16},{16,32},{32,48},{48,64},{64,80},{80,96},{96,112},{112,128},... | collective-permute-start | bytes 368 | tf_op jit(solution)/shard_map/ppermute | solution.py:17
  12.2 6.2 %collective-permute-start = (bf16[30,64]{0,1:T(8,128)(2,1)S(1)}, bf16[30,64]{0,1:T(8,128)(2,1)S(1)}, u32[]{:S(2)}, u32[]{:S(2)}) collective-permute-start(bf16[30,64]{0,1:T(8,128)(2,1)S(1)} %slice.402), channel_id=1, source_target_pairs={{0,16},{16,32},{32,48},{48,64},{64,80},{80,96},{96,112},{112,128},... | collective-permute-start | bytes 11528 | tf_op jit(solution)/shard_map/ppermute | solution.py:17
  18.5 18.1 %copy-start.3 = (s32[192,2]{0,1:T(2,128)S(1)}, s32[192,2]{0,1:T(2,128)}, u32[]{:S(2)}) copy-start(s32[192,2]{0,1:T(2,128)} %param.22) | copy-start | bytes 4612
  36.6 151.4 %all-gather.4.cloned.1.call-start = ((), (), s32[]{:S(2)}) async-start(), calls=%async_computation.6 | async-start | bytes 3342336 | tf_op jit(solution)/shard_map/all_gather | solution.py:130
  123.6 1.1 copy-start.1
  145.7 96.8 %reduce-scatter.5.cloned.1.call-start = ((), (), s32[]{:S(2)}) async-start(), calls=%async_computation.7 | async-start | bytes 3538944 | tf_op jit(solution)/shard_map/reduce_scatter | solution.py:47
  187.9 3.6 %copy-start.7 = (bf16[768,2048]{1,0:T(8,128)(2,1)S(1)}, bf16[768,2048]{1,0:T(8,128)(2,1)}, u32[]{:S(2)}) copy-start(bf16[768,2048]{1,0:T(8,128)(2,1)} %all-gather.4.cloned.1.call-done) | copy-start | bytes 9437188
  198.1 73.1 %reduce-scatter.7.cloned.1.call-start = ((), (), s32[]{:S(2)}) async-start(), calls=%async_computation.9 | async-start | bytes 589824
  250.6 34.0 %copy-start.4 = (f32[192,2]{0,1:T(2,128)S(1)}, f32[192,2]{0,1:T(2,128)}, u32[]{:S(2)}) copy-start(f32[192,2]{0,1:T(2,128)} %param.23) | copy-start | bytes 4612
  273.7 40.3 %copy-start.6 = (f32[128]{0:T(128)S(1)}, f32[128]{0:T(128)}, u32[]{:S(2)}) copy-start(f32[128]{0:T(128)} %param.27) | copy-start | bytes 1540
  275.5 19.5 %all-to-all-start.2 = ((bf16[32,24,128]{2,1,0:T(8,128)(2,1)}), bf16[32,24,128]{2,1,0:T(8,128)(2,1)S(1)}, u32[]{:S(2)}, u32[]{:S(2)}) async-start(bf16[32,24,128]{2,1,0:T(8,128)(2,1)} %copy.47), calls=%async_computation.3 | async-start | bytes 393216 | tf_op jit(solution)/shard_map/all_to_all | solution.py:142
Sparse Core Ops, SparseCore 0:
  36.7 77.6 all-gather.5
  145.8 42.1 all-gather.3
  198.2 44.2 reduce-scatter.4
  250.7 20.3 reduce-scatter.6
where the time goes:
time: 323 us; the launch traced here: 322 us
  waiting for transfers between devices  192 us (59%)
  blocking collectives  51.8 us (16%)
  other arithmetic  18.8 us (6%)
  local copies, waits for them, and re-layouts  18.2 us (6%)
  starting transfers between devices  16.2 us (5%)
  between operations  13.4 us (4%)
  matrix products  11.6 us (4%)
    all_gather x1, waiting for transfers between devices, over_pieces(): return lax.all_gather(value, axis).astype(jnp.float32).sum(0)  74.9 us
    reduce_scatter x1, waiting for transfers between devices, summed_rows(): value = lax.psum_scatter(value, axis, scatter_dimension=dim, tiled=True)  44.2 us
    all_gather x1, waiting for transfers between devices, local(): col_piece = lax.all_gather(flat_rows, TP, axis=1, tiled=True)  42.2 us
    all_to_all x2, blocking collectives, copy_for_each(): lax.all_to_all(jnp.broadcast_to(value[None], (peers, *value.shape)), axis...  31.4 us
    unnamed x5, waiting for transfers between devices  20.6 us
    all_to_all x1, blocking collectives, local(): lax.all_to_all(outgoing, 'sp', split_axis=0, concat_axis=0, tiled=True)  20.4 us
    unnamed x22, local copies, waits for them, and re-layouts  13.8 us
    all_to_all x1, waiting for transfers between devices, local(): lax.all_to_all(summed, 'sp', split_axis=0, concat_axis=0, tiled=True)  10.3 us
  transfers between devices with their start and end apart: 7, of which 5 were waited for; matrix products, arithmetic and copies ran while one was open for 2% of the time, Pallas kernels for 0%

commit v1 on v0

v1 whole, which is shorter than its diff:
```python
import jax
import jax.numpy as jnp
from jax import lax
from jax.sharding import Mesh
from jax.sharding import PartitionSpec as P

TP = ("y", "c")

residual_alpha = 1.41421356
norm_eps = 1e-05
row_scale = 64.0


def from_behind(value, axis, by):
    peers = lax.axis_size(axis)
    pairs = [(i, i + by) for i in range(peers) if 0 <= i + by < peers]
    return lax.ppermute(value, axis, pairs)


def swap(value, axis):
    return lax.ppermute(value, axis, [(0, 1), (1, 0)])


def summed_over(value, axis, peers):
    copies = jnp.broadcast_to(value[None], (peers, *value.shape))
    return jnp.sum(lax.all_to_all(copies, axis, 0, 0, tiled=True), axis=0)


def local(
    glu_value,
    glu_gate,
    doc_ids,
    conv_kernel,
    conv_gain,
    out_weight,
    residual,
    mix_gain,
    routes,
    route_weights,
    expert_gate,
    expert_up,
    expert_down,
    final_gain,
):
    f32, bf16 = jnp.float32, jnp.bfloat16
    n_sp, n_y, n_c = lax.axis_size("sp"), lax.axis_size("y"), lax.axis_size("c")
    n_tp = n_y * n_c
    at_c = lax.axis_index("c")
    at_tp = lax.axis_index(TP)
    tok_rows, own_ch = glu_value.shape
    rim_len = conv_kernel.shape[0] - 1
    channels = own_ch * n_tp
    features = residual.shape[1]
    feat_block = features // n_tp

    gated_rows = (glu_value.astype(f32) * jax.nn.sigmoid(glu_gate.astype(f32))).astype(bf16)
    rim_rows, rim_ids = from_behind(
        (gated_rows[tok_rows - rim_len :], doc_ids[tok_rows - rim_len :]), "sp", 1
    )
    packed = jnp.concatenate(
        [rim_rows.astype(f32), gated_rows.astype(f32), conv_kernel.astype(f32), conv_gain[None]], 0
    )
    packed = lax.all_gather(packed, "c", axis=1, tiled=True)
    extended = packed[: rim_len + tok_rows]
    kernel = packed[rim_len + tok_rows : 2 * rim_len + tok_rows + 1]
    gain = packed[2 * rim_len + tok_rows + 1]
    ext_ids = jnp.concatenate([rim_ids, doc_ids], 0)
    filtered = jnp.zeros((tok_rows, n_c * own_ch), f32)
    for shift_by in range(rim_len + 1):
        begin_at = rim_len - shift_by
        same_doc = (ext_ids[begin_at : begin_at + tok_rows] == doc_ids)[:, None]
        filtered = (
            filtered
            + jnp.where(same_doc, extended[begin_at : begin_at + tok_rows], 0.0) * kernel[shift_by]
        )
    stats = summed_over(
        jnp.concatenate([jnp.sum(filtered, 1), jnp.sum(filtered * filtered, 1)]).reshape(-1, 128),
        "y",
        n_y,
    ).reshape(2, tok_rows)
    row_mean = stats[0][:, None] / channels
    row_var = stats[1][:, None] / channels - row_mean * row_mean
    conv_out = jax.nn.silu((filtered - row_mean) * lax.rsqrt(row_var + norm_eps) * gain).astype(bf16)

    weight_parts = out_weight.reshape(own_ch, n_y, n_c, feat_block).transpose(2, 0, 1, 3)
    weight_half = lax.all_to_all(weight_parts, "c", 0, 0, tiled=True)
    weight_half = weight_half.reshape(n_c * own_ch, n_y, feat_block)
    mix_parts = jnp.einsum("tk,kyf->ytf", conv_out, weight_half, preferred_element_type=f32)
    mix_parts = lax.all_to_all(mix_parts.astype(bf16), "y", 0, 0, tiled=True)
    own_residual = lax.dynamic_slice_in_dim(residual, at_tp * feat_block, feat_block, 1)
    own_z = residual_alpha * own_residual.astype(f32) + jnp.sum(mix_parts.astype(f32), 0)

    experts = expert_gate.shape[0] * n_sp
    capacity = 4 * tok_rows // experts
    chosen = routes.reshape(-1)
    member = (chosen[:, None] == jnp.arange(experts, dtype=jnp.int32)[None, :]).astype(jnp.int32)
    earlier = jnp.cumsum(member, 0) - member
    slot_index = (chosen * capacity + jnp.sum(earlier * member, 1)).reshape(tok_rows, 2)
    slots = jnp.arange(experts * capacity, dtype=jnp.int32)
    dispatch_table = jnp.any(slots[:, None, None] == slot_index[None], -1).astype(bf16)

    outgoing = jnp.dot(dispatch_table, own_z.astype(bf16), preferred_element_type=f32)
    outgoing = (outgoing * row_scale).astype(jnp.float16).reshape(experts, capacity, feat_block)
    arrived = lax.all_to_all(outgoing, "sp", 0, 0, tiled=True)
    rows = n_sp * capacity
    gathered = lax.all_gather(arrived.reshape(rows, feat_block), TP, axis=0, tiled=False)

    wide = gathered.astype(f32)
    in_mean = jnp.sum(wide, (0, 2)) * (1.0 / (row_scale * features))
    in_square = jnp.sum(wide * wide, (0, 2)) * (1.0 / (row_scale * row_scale * features))
    in_rstd = lax.rsqrt(in_square - in_mean * in_mean + norm_eps)
    in_rows = (
        (wide * (1.0 / row_scale) - in_mean[None, :, None])
        * in_rstd[None, :, None]
        * mix_gain.reshape(n_tp, 1, feat_block)
    ).astype(bf16)
    in_rows = in_rows.transpose(1, 0, 2).reshape(rows, features)
    gate_proj = jnp.dot(in_rows, expert_gate[0], preferred_element_type=f32)
    up_proj = jnp.dot(in_rows, expert_up[0], preferred_element_type=f32)
    hidden = (jax.nn.silu(gate_proj) * up_proj).astype(bf16)

    down_parts = expert_down[0].reshape(-1, n_y, n_c, feat_block)
    down_mine = lax.dynamic_index_in_dim(down_parts, at_c, 2, keepdims=False)
    down_else = swap(lax.dynamic_index_in_dim(down_parts, 1 - at_c, 2, keepdims=False), "c")
    hidden_else = swap(hidden, "c")
    hidden_both = jnp.concatenate([hidden, hidden_else], 1)
    down_both = jnp.concatenate([down_mine, down_else], 0)
    parts = jnp.einsum(
        "sik,kyf->syif",
        hidden_both.reshape(n_sp, capacity, -1),
        down_both,
        preferred_element_type=f32,
    ).astype(bf16)
    parts = parts.reshape(n_sp * n_y, capacity, feat_block)
    returned = lax.all_to_all(parts, ("sp", "y"), 0, 0, tiled=True)
    returned = returned.reshape(experts, n_y, capacity, feat_block)
    expert_out = jnp.sum(returned.astype(f32), 1).astype(bf16).reshape(experts * capacity, feat_block)
    first = (slot_index[:, :1] == slots[None, :]).astype(bf16)
    second = (slot_index[:, 1:] == slots[None, :]).astype(bf16)
    moe_sum = route_weights[:, :1] * jnp.dot(
        first, expert_out, preferred_element_type=f32
    ) + route_weights[:, 1:] * jnp.dot(second, expert_out, preferred_element_type=f32)

    own_gain = lax.dynamic_slice_in_dim(mix_gain, at_tp * feat_block, feat_block, 0)[None]
    z_gain = own_z * own_gain
    sums = jnp.stack(
        [
            jnp.sum(own_z, 1),
            jnp.sum(own_z * own_z, 1),
            jnp.sum(z_gain, 1),
            jnp.sum(z_gain * z_gain, 1),
            jnp.sum(z_gain * own_gain, 1),
            jnp.sum(z_gain * moe_sum, 1),
            jnp.sum(own_gain * moe_sum, 1),
            jnp.sum(moe_sum, 1),
            jnp.sum(moe_sum * moe_sum, 1),
            jnp.zeros_like(moe_sum[:, 0]),
        ]
    )
    sums = summed_over(sums.reshape(-1, 128), TP, n_tp).reshape(10, tok_rows)
    z_mean = sums[0] / features
    z_rstd = lax.rsqrt(sums[1] / features - z_mean * z_mean + norm_eps)
    ar = residual_alpha * z_rstd
    fin_sum = ar * (sums[2] - z_mean * jnp.sum(mix_gain)) + sums[7]
    fin_square = (
        ar * ar * (sums[3] - 2.0 * z_mean * sums[4] + z_mean * z_mean * jnp.sum(mix_gain * mix_gain))
        + 2.0 * ar * (sums[5] - z_mean * sums[6])
        + sums[8]
    )
    fin_mean = fin_sum / features
    fin_rstd = lax.rsqrt(fin_square / features - fin_mean * fin_mean + norm_eps)
    pre_norm = ar[:, None] * (own_z - z_mean[:, None]) * own_gain + moe_sum
    return ((pre_norm - fin_mean[:, None]) * fin_rstd[:, None] * final_gain).astype(bf16)


def solution(mesh):
    finer = Mesh(mesh.devices.reshape(mesh.shape["sp"], 8, 2), ("sp", "y", "c"))
    placed = (
        P("sp", TP),
        P("sp", TP),
        P("sp"),
        P(None, TP),
        P(TP),
        P(TP, None),
        P("sp", None),
        P(),
        P("sp", None),
        P("sp", None),
        P("sp", None, TP),
        P("sp", None, TP),
        P("sp", TP, None),
        P(TP),
    )
    return jax.shard_map(local, mesh=finer, in_specs=placed, out_specs=P("sp", TP), check_vma=False)
```

time: 323 us -> 210 us (0.65)
  waiting for transfers between devices: 192 us -> 67.4 us
  starting transfers between devices: 16.2 us -> 63.3 us
  blocking collectives: 51.8 us -> 29.7 us
  between operations: 13.4 us -> 0.92 us
  local copies, waits for them, and re-layouts: 18.2 us -> 25.2 us
  other arithmetic: 18.8 us -> 13.9 us
  matrix products: 11.6 us -> 8.23 us
    all_gather x2 -> x0, waiting for transfers between devices: 117 us -> none  [the longest x1 74.9 us: over_pieces(): return lax.all_gather(value, axis).astype(jnp.float32).sum(0)]
    all_to_all x1 -> x6, waiting for transfers between devices: 10.3 us -> 66.8 us  [the longest x1 41.5 us: local(): returned = lax.all_to_all(parts, ('sp', 'y'), 0, 0, tiled=True)]
    all_to_all x3 -> x0, blocking collectives: 51.8 us -> none  [the longest x2 31.4 us: copy_for_each(): lax.all_to_all(jnp.broadcast_to(value[None], (peers, *value.shape)), axis...]
    reduce_scatter x1 -> x0, waiting for transfers between devices: 44.2 us -> none  [summed_rows(): value = lax.psum_scatter(value, axis, scatter_dimension=dim, tiled=True)]
    all_to_all x1 -> x6, starting transfers between devices: 8.9 us -> 49.2 us  [the longest x1 15.9 us: local(): returned = lax.all_to_all(parts, ('sp', 'y'), 0, 0, tiled=True)]
    all_gather x0 -> x2, blocking collectives: none -> 29.7 us  [the longest x1 27.8 us: local(): lax.all_gather(arrived.reshape(rows, feat_block), TP, axis=0, tiled=False)]
    unnamed x5 -> x0, waiting for transfers between devices: 20.6 us -> none
    unnamed x22 -> x19, local copies, waits for them, and re-layouts: 13.8 us -> 2.4 us
  transfers between devices with their start and end apart: 7 -> 10, of which waited for: 5 -> 5; matrix products, arithmetic and copies ran while one was open for 2% -> 17% of each run, Pallas kernels for 0% -> 0%
where the time goes in v1:
time: 210 us; the launch traced here: 209 us
  waiting for transfers between devices  67.4 us (32%)
  starting transfers between devices  63.3 us (30%)
  blocking collectives  29.7 us (14%)
  local copies, waits for them, and re-layouts  25.2 us (12%)
  other arithmetic  13.9 us (7%)
  matrix products  8.23 us (4%)
    all_to_all x1, waiting for transfers between devices, local(): returned = lax.all_to_all(parts, ('sp', 'y'), 0, 0, tiled=True)  41.5 us
    all_gather x1, blocking collectives, local(): lax.all_gather(arrived.reshape(rows, feat_block), TP, axis=0, tiled=False)  27.8 us
    all_to_all x1, starting transfers between devices, local(): returned = lax.all_to_all(parts, ('sp', 'y'), 0, 0, tiled=True)  15.9 us
    all_to_all x2, waiting for transfers between devices, summed_over(): return jnp.sum(lax.all_to_all(copies, axis, 0, 0, tiled=True), axis=0)  14.4 us
    all_to_all x1, starting transfers between devices, local(): arrived = lax.all_to_all(outgoing, 'sp', 0, 0, tiled=True)  12.5 us
    all_to_all x2, starting transfers between devices, summed_over(): return jnp.sum(lax.all_to_all(copies, axis, 0, 0, tiled=True), axis=0)  11.6 us
    all_to_all x1, waiting for transfers between devices, local(): mix_parts = lax.all_to_all(mix_parts.astype(bf16), 'y', 0, 0, tiled=True)  10.9 us
    ppermute x2, starting transfers between devices, swap(): return lax.ppermute(value, axis, [(0, 1), (1, 0)])  7.06 us
  transfers between devices with their start and end apart: 10, of which 5 were waited for; matrix products, arithmetic and copies ran while one was open for 17% of the time, Pallas kernels for 0%

profile of v1, /device:TPU:1, one launch (start us, length us, event | category | flops | bytes accessed | tf_op | source)
XLA Modules:
  0.0 208.6 jit_solution(11123523421009321162)
XLA Ops:
  0.0 0.9 fusion.96
  1.0 3.9 %collective-permute-start = (bf16[30,64]{0,1:T(8,128)(2,1)S(1)}, bf16[30,64]{0,1:T(8,128)(2,1)S(1)}, u32[]{:S(2)}, u32[]{:S(2)}) collective-permute-start(bf16[30,64]{0,1:T(8,128)(2,1)S(1)} %slice.512), channel_id=1, source_target_pairs={{0,16},{16,32},{32,48},{48,64},{64,80},{80,96},{96,112},{112,128},... | collective-permute-start | bytes 11528 | tf_op jit(solution)/shard_map/ppermute | solution.py:17
  5.7 3.1 %collective-permute-start.1 = (s32[30]{0:T(128)S(1)}, s32[30]{0:T(128)S(1)}, u32[]{:S(2)}, u32[]{:S(2)}) collective-permute-start(s32[30]{0:T(128)S(1)} %slice.403), channel_id=1, source_target_pairs={{0,16},{16,32},{32,48},{48,64},{64,80},{80,96},{96,112},{112,128},... | collective-permute-start | bytes 368 | tf_op jit(solution)/shard_map/ppermute | solution.py:17
  8.8 1.1 reshape.240
  10.7 5.8 %all-to-all-start.1 = ((bf16[2,64,8,128]{3,1,2,0:T(8,128)(2,1)}), bf16[2,64,8,128]{3,1,2,0:T(8,128)(2,1)S(1)}, u32[]{:S(2)}, u32[]{:S(2)}) async-start(bf16[2,64,8,128]{3,1,2,0:T(8,128)(2,1)} %copy.123), calls=%async_computation.1 | async-start | bytes 524288 | tf_op jit(solution)/shard_map/all_to_all | solution.py:86
  20.4 1.9 all_gather.6
  23.7 1.9 fusion.94
  26.3 5.7 %all-to-all-start = ((f32[8,3,128]{2,1,0:T(4,128)}), f32[8,3,128]{2,1,0:T(4,128)S(1)}, u32[]{:S(2)}, u32[]{:S(2)}) async-start(f32[8,3,128]{2,1,0:T(4,128)} %broadcast_in_dim.283), calls=%async_computation | async-start | bytes 32768 | tf_op jit(solution)/shard_map/all_to_all | solution.py:26
  32.3 6.4 %all-to-all-done = f32[8,3,128]{2,1,0:T(4,128)S(1)} async-done(((f32[8,3,128]{2,1,0:T(4,128)}), f32[8,3,128]{2,1,0:T(4,128)S(1)}, u32[]{:S(2)}, u32[]{:S(2)}) %all-to-all-start) | async-done | bytes 12320 | tf_op jit(solution)/shard_map/all_to_all | solution.py:26
  38.8 1.1 fusion.14
  39.9 3.5 %all-to-all-start.2 = ((bf16[8,192,128]{2,1,0:T(8,128)(2,1)}), bf16[8,192,128]{2,1,0:T(8,128)(2,1)S(1)}, u32[]{:S(2)}, u32[]{:S(2)}) async-start(bf16[8,192,128]{2,1,0:T(8,128)(2,1)} %fusion.14), calls=%async_computation.2 | async-start | bytes 786432 | tf_op jit(solution)/shard_map/all_to_all | solution.py:89
  45.2 10.9 %all-to-all-done.2 = bf16[8,192,128]{2,1,0:T(8,128)(2,1)S(1)} async-done(((bf16[8,192,128]{2,1,0:T(8,128)(2,1)}), bf16[8,192,128]{2,1,0:T(8,128)(2,1)S(1)}, u32[]{:S(2)}, u32[]{:S(2)}) %all-to-all-start.2) | async-done | bytes 393248 | tf_op jit(solution)/shard_map/all_to_all | solution.py:89
  57.0 1.1 fusion.16
  58.1 12.5 %all-to-all-start.3 = ((f16[32,24,128]{2,1,0:T(8,128)(2,1)}), f16[32,24,128]{2,1,0:T(8,128)(2,1)S(1)}, u32[]{:S(2)}, u32[]{:S(2)}) async-start(f16[32,24,128]{2,1,0:T(8,128)(2,1)} %bitcast.20), calls=%async_computation.3 | async-start | bytes 393216 | tf_op jit(solution)/shard_map/all_to_all | solution.py:104
  70.6 3.6 %reshape_squeeze.3 = bf16[320,8,2,128]{3,2,1,0:T(2,128)(2,1)S(1)} reshape(bf16[1,320,2048]{2,1,0:T(8,128)(2,1)} %param.26) | data formatting | bytes 2621440 | tf_op jit(solution)/shard_map/reshape;squeeze | solution.py:122
  74.2 3.8 %constant_dynamic-slice_fusion.1 = (bf16[320,8,1,128]{3,2,1,0:T(2,128)(2,1)}, bf16[320,8,1,128]{3,2,1,0:T(2,128)(2,1)S(1)}) fusion(bf16[320,8,2,128]{3,2,1,0:T(2,128)(2,1)S(1)} %reshape_squeeze.3, s32[]{:T(128)S(6)} %select_n.134, s32[]{:T(128)S(6)} %select_n.135), kind=kLoop, calls=%fused_computation.235 | loop fusion | bytes 2621448 | tf_op jit(solution)/shard_map/jit(dynamic_index_in_dim)/dynamic_slice | solution.py:123
  78.0 1.1 copy.152
  79.1 5.0 %collective-permute-start.2 = (bf16[320,8,128]{2,0,1:T(8,128)(2,1)}, bf16[320,8,128]{2,0,1:T(8,128)(2,1)}, u32[]{:S(2)}, u32[]{:S(2)}) collective-permute-start(bf16[320,8,128]{2,0,1:T(8,128)(2,1)} %bitcast.91), channel_id=1, source_target_pairs={{0,1},{1,0},{2,3},{3,2},{4,5},{5,4},{6,7},{7,6},{8,9},{9,8},{10,11... | collective-permute-start | bytes 1966088 | tf_op jit(solution)/shard_map/ppermute | solution.py:21
  84.1 27.8 %all-gather.1 = f16[16,768,128]{2,1,0:T(8,128)(2,1)} all-gather(f16[1,768,128]{2,1,0:T(8,128)(2,1)S(1)} %bitcast.99), channel_id=1, replica_groups=mesh['sp'=32,'y'=8,'c'=2] {'y','c'}, dimensions={0}, use_global_device_ids=true | all-gather | bytes 3342336 | tf_op jit(solution)/shard_map/all_gather | solution.py:106
  111.9 5.1 %copy.132 = f16[16,768,128]{1,2,0:T(8,128)(2,1)} copy(f16[16,768,128]{2,1,0:T(8,128)(2,1)} %all-gather.1) | data formatting | bytes 6291456 | tf_op jit(solution)/shard_map/all_gather | solution.py:106
  117.0 2.9 %convert_reduce_fusion = (f32[768]{0:T(1024)S(1)}, f32[768]{0:T(1024)S(1)}) fusion(f16[16,768,128]{1,2,0:T(8,128)(2,1)} %copy.132), kind=kLoop, calls=%fused_computation.1 | loop fusion | flops 6289920 | bytes 3151872 | tf_op jit(solution)/shard_map/reduce_sum | solution.py:109
  119.9 1.2 fusion.3
  121.1 1.2 fusion.9
  122.4 1.3 fusion.11
  123.7 2.1 collective-permute-start.3
  125.8 1.1 copy.153
  128.2 2.7 %fusion.5 = bf16[32,8,24,128]{3,0,2,1:T(8,128)(2,1)S(1)} fusion(bf16[320,8,128]{2,0,1:T(8,128)(2,1)} %collective-permute-done.2, bf16[320,8,128]{2,0,1:T(8,128)(2,1)} %bitcast.100, bf16[32,24,640]{2,1,0:T(8,128)(2,1)S(1)} %bitcast.98), kind=kOutput, calls=%fused_computation.10 | convolution fusion | flops 1010040832 | bytes 3866624 | tf_op jit(solution)/shard_map/sik,kyf->syif/dot_general | solution.py:128
  130.9 1.8 copy.135
  132.6 15.9 %all-to-all-start.4 = ((bf16[256,24,128]{2,1,0:T(8,128)(2,1)}), bf16[256,24,128]{2,1,0:T(8,128)(2,1)S(1)}, u32[]{:S(2)}, u32[]{:S(2)}) async-start(bf16[256,24,128]{2,1,0:T(8,128)(2,1)} %bitcast.94), calls=%async_computation.4 | async-start | bytes 3145728 | tf_op jit(solution)/shard_map/all_to_all | solution.py:135
  148.6 41.5 %all-to-all-done.4 = bf16[256,24,128]{2,1,0:T(8,128)(2,1)S(1)} async-done(((bf16[256,24,128]{2,1,0:T(8,128)(2,1)}), bf16[256,24,128]{2,1,0:T(8,128)(2,1)S(1)}, u32[]{:S(2)}, u32[]{:S(2)}) %all-to-all-start.4) | async-done | bytes 1572896 | tf_op jit(solution)/shard_map/all_to_all | solution.py:135
  192.0 5.9 %all-to-all-start.5 = ((f32[16,15,128]{2,1,0:T(8,128)}), f32[16,15,128]{2,1,0:T(8,128)S(1)}, u32[]{:S(2)}, u32[]{:S(2)}) async-start(f32[16,15,128]{2,1,0:T(8,128)} %broadcast_in_dim.285), calls=%async_computation.5 | async-start | bytes 262144 | tf_op jit(solution)/shard_map/all_to_all | solution.py:26
  199.0 8.0 %all-to-all-done.5 = f32[16,15,128]{2,1,0:T(8,128)S(1)} async-done(((f32[16,15,128]{2,1,0:T(8,128)}), f32[16,15,128]{2,1,0:T(8,128)S(1)}, u32[]{:S(2)}, u32[]{:S(2)}) %all-to-all-start.5) | async-done | bytes 122912 | tf_op jit(solution)/shard_map/all_to_all | solution.py:26
  (74 shorter events, 16.1 us)
Async XLA Ops:
  0.0 121.1 %copy-start = (bf16[1,2048,320]{1,2,0:T(8,128)(2,1)S(1)}, bf16[1,2048,320]{1,2,0:T(8,128)(2,1)}, u32[]{:S(2)}) copy-start(bf16[1,2048,320]{1,2,0:T(8,128)(2,1)} %param.24) | copy-start | bytes 3932164
  1.0 19.3 %collective-permute-start = (bf16[30,64]{0,1:T(8,128)(2,1)S(1)}, bf16[30,64]{0,1:T(8,128)(2,1)S(1)}, u32[]{:S(2)}, u32[]{:S(2)}) collective-permute-start(bf16[30,64]{0,1:T(8,128)(2,1)S(1)} %slice.512), channel_id=1, source_target_pairs={{0,16},{16,32},{32,48},{48,64},{64,80},{80,96},{96,112},{112,128},... | collective-permute-start | bytes 11528 | tf_op jit(solution)/shard_map/ppermute | solution.py:17
  5.7 12.3 %collective-permute-start.1 = (s32[30]{0:T(128)S(1)}, s32[30]{0:T(128)S(1)}, u32[]{:S(2)}, u32[]{:S(2)}) collective-permute-start(s32[30]{0:T(128)S(1)} %slice.403), channel_id=1, source_target_pairs={{0,16},{16,32},{32,48},{48,64},{64,80},{80,96},{96,112},{112,128},... | collective-permute-start | bytes 368 | tf_op jit(solution)/shard_map/ppermute | solution.py:17
  10.7 15.0 %all-to-all-start.1 = ((bf16[2,64,8,128]{3,1,2,0:T(8,128)(2,1)}), bf16[2,64,8,128]{3,1,2,0:T(8,128)(2,1)S(1)}, u32[]{:S(2)}, u32[]{:S(2)}) async-start(bf16[2,64,8,128]{3,1,2,0:T(8,128)(2,1)} %copy.123), calls=%async_computation.1 | async-start | bytes 524288 | tf_op jit(solution)/shard_map/all_to_all | solution.py:86
  23.7 8.3 %copy-start.4 = (s32[192,2]{0,1:T(2,128)S(1)}, s32[192,2]{0,1:T(2,128)}, u32[]{:S(2)}) copy-start(s32[192,2]{0,1:T(2,128)} %param.22) | copy-start | bytes 4612
  26.3 12.4 %all-to-all-start = ((f32[8,3,128]{2,1,0:T(4,128)}), f32[8,3,128]{2,1,0:T(4,128)S(1)}, u32[]{:S(2)}, u32[]{:S(2)}) async-start(f32[8,3,128]{2,1,0:T(4,128)} %broadcast_in_dim.283), calls=%async_computation | async-start | bytes 32768 | tf_op jit(solution)/shard_map/all_to_all | solution.py:26
  39.9 16.2 %all-to-all-start.2 = ((bf16[8,192,128]{2,1,0:T(8,128)(2,1)}), bf16[8,192,128]{2,1,0:T(8,128)(2,1)S(1)}, u32[]{:S(2)}, u32[]{:S(2)}) async-start(bf16[8,192,128]{2,1,0:T(8,128)(2,1)} %fusion.14), calls=%async_computation.2 | async-start | bytes 786432 | tf_op jit(solution)/shard_map/all_to_all | solution.py:89
  58.1 26.0 %all-to-all-start.3 = ((f16[32,24,128]{2,1,0:T(8,128)(2,1)}), f16[32,24,128]{2,1,0:T(8,128)(2,1)S(1)}, u32[]{:S(2)}, u32[]{:S(2)}) async-start(f16[32,24,128]{2,1,0:T(8,128)(2,1)} %bitcast.20), calls=%async_computation.3 | async-start | bytes 393216 | tf_op jit(solution)/shard_map/all_to_all | solution.py:104
  79.1 49.1 %collective-permute-start.2 = (bf16[320,8,128]{2,0,1:T(8,128)(2,1)}, bf16[320,8,128]{2,0,1:T(8,128)(2,1)}, u32[]{:S(2)}, u32[]{:S(2)}) collective-permute-start(bf16[320,8,128]{2,0,1:T(8,128)(2,1)} %bitcast.91), channel_id=1, source_target_pairs={{0,1},{1,0},{2,3},{3,2},{4,5},{5,4},{6,7},{7,6},{8,9},{9,8},{10,11... | collective-permute-start | bytes 1966088 | tf_op jit(solution)/shard_map/ppermute | solution.py:21
  117.0 2.9 %copy-start.1 = (f16[16,768,128]{1,2,0:T(8,128)(2,1)S(1)}, f16[16,768,128]{1,2,0:T(8,128)(2,1)}, u32[]{:S(2)}) copy-start(f16[16,768,128]{1,2,0:T(8,128)(2,1)} %copy.132) | copy-start | bytes 9437188
  117.0 2.9 %copy-start.3 = (f32[2048]{0:T(1024)S(1)}, f32[2048]{0:T(1024)}, u32[]{:S(2)}) copy-start(f32[2048]{0:T(1024)} %param.21) | copy-start | bytes 24580
  121.1 1.3 copy-start.7
  122.4 3.3 %copy-start.2 = (bf16[320,8,1,128]{3,2,1,0:T(2,128)(2,1)S(1)}, bf16[320,8,1,128]{3,2,1,0:T(2,128)(2,1)}, u32[]{:S(2)}) copy-start(bf16[320,8,1,128]{3,2,1,0:T(2,128)(2,1)} %get-tuple-element.64) | copy-start | bytes 1966084
  123.7 3.8 %collective-permute-start.3 = (bf16[768,320]{0,1:T(8,128)(2,1)S(1)}, bf16[768,320]{0,1:T(8,128)(2,1)S(1)}, u32[]{:S(2)}, u32[]{:S(2)}) collective-permute-start(bf16[768,320]{0,1:T(8,128)(2,1)S(1)} %fusion.11), channel_id=1, source_target_pairs={{0,1},{1,0},{2,3},{3,2},{4,5},{5,4},{6,7},{7,6},{8,9},{9,8},{10,11... | collective-permute-start | bytes 1474568 | tf_op jit(solution)/shard_map/ppermute | solution.py:21
  132.6 16.0 %copy-start.5 = (f32[192,2]{0,1:T(2,128)S(1)}, f32[192,2]{0,1:T(2,128)}, u32[]{:S(2)}) copy-start(f32[192,2]{0,1:T(2,128)} %param.23) | copy-start | bytes 4612
  132.6 57.5 %all-to-all-start.4 = ((bf16[256,24,128]{2,1,0:T(8,128)(2,1)}), bf16[256,24,128]{2,1,0:T(8,128)(2,1)S(1)}, u32[]{:S(2)}, u32[]{:S(2)}) async-start(bf16[256,24,128]{2,1,0:T(8,128)(2,1)} %bitcast.94), calls=%async_computation.4 | async-start | bytes 3145728 | tf_op jit(solution)/shard_map/all_to_all | solution.py:135
  148.5 59.3 %copy-start.6 = (f32[128]{0:T(128)S(1)}, f32[128]{0:T(128)}, u32[]{:S(2)}) copy-start(f32[128]{0:T(128)} %param.27) | copy-start | bytes 1540
  192.0 15.1 %all-to-all-start.5 = ((f32[16,15,128]{2,1,0:T(8,128)}), f32[16,15,128]{2,1,0:T(8,128)S(1)}, u32[]{:S(2)}, u32[]{:S(2)}) async-start(f32[16,15,128]{2,1,0:T(8,128)} %broadcast_in_dim.285), calls=%async_computation.5 | async-start | bytes 262144 | tf_op jit(solution)/shard_map/all_to_all | solution.py:26

commit v2 on v1

--- a/solution.py
+++ b/solution.py
@@ -1,6 +1,10 @@
+import functools
+
 import jax
 import jax.numpy as jnp
 from jax import lax
+from jax.experimental import pallas as pl
+from jax.experimental.pallas import tpu as pltpu
 from jax.sharding import Mesh
 from jax.sharding import PartitionSpec as P
 
@@ -24,6 +28,71 @@
 def summed_over(value, axis, peers):
     copies = jnp.broadcast_to(value[None], (peers, *value.shape))
     return jnp.sum(lax.all_to_all(copies, axis, 0, 0, tiled=True), axis=0)
+
+
+def conv_body(packed_ref, ids_ref, filtered_ref, sums_ref, *, lags, tok_rows):
+    packed = packed_ref[...]
+    ids = ids_ref[...]
+    total = jnp.zeros((packed.shape[0], tok_rows), jnp.float32)
+    for lag in range(lags):
+        rows = packed if lag == 0 else pltpu.roll(packed, lag, 1)
+        other = ids if lag == 0 else pltpu.roll(ids, lag, 1)
+        same_doc = other[:1, :tok_rows] == ids[:1, :tok_rows]
+        tap = packed[:, tok_rows + lag : tok_rows + lag + 1]
+        total = total + jnp.where(same_doc, rows[:, :tok_rows], 0.0) * tap
+    filtered_ref[...] = total
+    sums = jnp.concatenate(
+        [jnp.sum(total, 0, keepdims=True), jnp.sum(total * total, 0, keepdims=True)], 0
+    )
+    sums_ref[...] = jnp.broadcast_to(sums[None], sums_ref.shape)
+
+
+def mix_body(at_ref, filtered_ref, sums_ref, packed_ref, mine_ref, else_ref, out_ref, *, gain_at, channels):
+    first = at_ref[0] == 0
+    peers, tok_rows, block = out_ref.shape
+    sums = jnp.sum(sums_ref[...], 0)
+    row_mean = sums[:1] / channels
+    row_var = sums[1:] / channels - row_mean * row_mean
+    gain = packed_ref[:, gain_at : gain_at + 1]
+    normed = (filtered_ref[...] - row_mean) * lax.rsqrt(row_var + norm_eps) * gain
+    conv_out = (normed / (1.0 + jnp.exp(-normed))).T.astype(jnp.bfloat16)
+    for peer in range(0, peers, 2):
+        columns = []
+        for step in range(2):
+            at = pl.multiple_of((2 * (peer + step) + at_ref[0]) * block, block)
+            mine, other = mine_ref[:, pl.ds(at, block)], else_ref[:, pl.ds(at, block)]
+            columns.append(
+                jnp.concatenate([jnp.where(first, mine, other), jnp.where(first, other, mine)], 0)
+            )
+        part = jnp.dot(
+            conv_out, jnp.concatenate(columns, 1), preferred_element_type=jnp.float32
+        ).astype(jnp.bfloat16)
+        out_ref[peer] = part[:, :block]
+        out_ref[peer + 1] = part[:, block:]
+
+
+def down_body(at_ref, mine_ref, else_ref, down_mine_ref, down_else_ref, out_ref):
+    n_sp, peers, capacity, block = out_ref.shape
+    hidden = jnp.concatenate([mine_ref[...], else_ref[...]], 0)
+    for peer in range(0, peers, 2):
+        columns = []
+        for step in range(2):
+            at = pl.multiple_of((2 * (peer + step) + at_ref[0]) * block, block)
+            columns.append(
+                jnp.concatenate([down_mine_ref[:, pl.ds(at, block)], down_else_ref[:, pl.ds(at, block)]], 0)
+            )
+        part = lax.dot_general(
+            hidden,
+            jnp.concatenate(columns, 1),
+            (((0,), (0,)), ((), ())),
+            preferred_element_type=jnp.float32,
+        ).astype(jnp.bfloat16)
+        out_ref[:, peer] = part[:, :block].reshape(n_sp, capacity, block)
+        out_ref[:, peer + 1] = part[:, block:].reshape(n_sp, capacity, block)
+
+
+def whole(memory=None):
+    return pl.BlockSpec(memory_space=memory or pltpu.VMEM)
 
 
 def local(
@@ -45,48 +114,57 @@
     f32, bf16 = jnp.float32, jnp.bfloat16
     n_sp, n_y, n_c = lax.axis_size("sp"), lax.axis_size("y"), lax.axis_size("c")
     n_tp = n_y * n_c
-    at_c = lax.axis_index("c")
+    at_core = lax.axis_index("c").astype(jnp.int32).reshape(1)
     at_tp = lax.axis_index(TP)
     tok_rows, own_ch = glu_value.shape
-    rim_len = conv_kernel.shape[0] - 1
+    lags = conv_kernel.shape[0]
+    rim_len = lags - 1
     channels = own_ch * n_tp
     features = residual.shape[1]
     feat_block = features // n_tp
 
-    gated_rows = (glu_value.astype(f32) * jax.nn.sigmoid(glu_gate.astype(f32))).astype(bf16)
-    rim_rows, rim_ids = from_behind(
-        (gated_rows[tok_rows - rim_len :], doc_ids[tok_rows - rim_len :]), "sp", 1
-    )
+    value, gate = glu_value.T.astype(f32), glu_gate.T.astype(f32)
+    gated = (value * jax.nn.sigmoid(gate)).astype(bf16)
+    ids = doc_ids.astype(f32)[None]
+    rim = jnp.concatenate([gated[:, tok_rows - rim_len :], ids[:, tok_rows - rim_len :].astype(bf16)], 0)
+    rim = from_behind(rim, "sp", 1).astype(f32)
+    lanes = 256
+    blank = lanes - tok_rows - lags - 1 - rim_len
     packed = jnp.concatenate(
-        [rim_rows.astype(f32), gated_rows.astype(f32), conv_kernel.astype(f32), conv_gain[None]], 0
-    )
-    packed = lax.all_gather(packed, "c", axis=1, tiled=True)
-    extended = packed[: rim_len + tok_rows]
-    kernel = packed[rim_len + tok_rows : 2 * rim_len + tok_rows + 1]
-    gain = packed[2 * rim_len + tok_rows + 1]
-    ext_ids = jnp.concatenate([rim_ids, doc_ids], 0)
-    filtered = jnp.zeros((tok_rows, n_c * own_ch), f32)
-    for shift_by in range(rim_len + 1):
-        begin_at = rim_len - shift_by
-        same_doc = (ext_ids[begin_at : begin_at + tok_rows] == doc_ids)[:, None]
-        filtered = (
-            filtered
-            + jnp.where(same_doc, extended[begin_at : begin_at + tok_rows], 0.0) * kernel[shift_by]
-        )
-    stats = summed_over(
-        jnp.concatenate([jnp.sum(filtered, 1), jnp.sum(filtered * filtered, 1)]).reshape(-1, 128),
-        "y",
-        n_y,
-    ).reshape(2, tok_rows)
-    row_mean = stats[0][:, None] / channels
-    row_var = stats[1][:, None] / channels - row_mean * row_mean
-    conv_out = jax.nn.silu((filtered - row_mean) * lax.rsqrt(row_var + norm_eps) * gain).astype(bf16)
-
-    weight_parts = out_weight.reshape(own_ch, n_y, n_c, feat_block).transpose(2, 0, 1, 3)
-    weight_half = lax.all_to_all(weight_parts, "c", 0, 0, tiled=True)
-    weight_half = weight_half.reshape(n_c * own_ch, n_y, feat_block)
-    mix_parts = jnp.einsum("tk,kyf->ytf", conv_out, weight_half, preferred_element_type=f32)
-    mix_parts = lax.all_to_all(mix_parts.astype(bf16), "y", 0, 0, tiled=True)
+        [
+            gated.astype(f32),
+            conv_kernel.T.astype(f32),
+            conv_gain[:, None],
+            jnp.zeros((own_ch, blank), f32),
+            rim[:own_ch],
+        ],
+        1,
+    )
+    packed = lax.all_gather(packed, "c", axis=0, tiled=True)
+    packed_ids = jnp.concatenate(
+        [ids, jnp.zeros((1, lanes - tok_rows - rim_len), f32), rim[own_ch:]], 1
+    )
+    packed_ids = jnp.broadcast_to(packed_ids, (8, lanes))
+    filtered, sums = pl.pallas_call(
+        functools.partial(conv_body, lags=lags, tok_rows=tok_rows),
+        out_shape=(
+            jax.ShapeDtypeStruct((n_c * own_ch, tok_rows), f32),
+            jax.ShapeDtypeStruct((n_y, 2, tok_rows), f32),
+        ),
+        in_specs=[whole()] * 2,
+        out_specs=(whole(), whole()),
+        name="conv",
+    )(packed, packed_ids)
+    sums = lax.all_to_all(sums, "y", 0, 0, tiled=True)
+    weight_else = swap(out_weight, "c")
+    mix_parts = pl.pallas_call(
+        functools.partial(mix_body, gain_at=tok_rows + lags, channels=channels),
+        out_shape=jax.ShapeDtypeStruct((n_y, tok_rows, feat_block), bf16),
+        in_specs=[whole(pltpu.SMEM)] + [whole()] * 5,
+        out_specs=whole(),
+        name="mix",
+    )(at_core, filtered, sums, packed, out_weight, weight_else)
+    mix_parts = lax.all_to_all(mix_parts, "y", 0, 0, tiled=True)
     own_residual = lax.dynamic_slice_in_dim(residual, at_tp * feat_block, feat_block, 1)
     own_z = residual_alpha * own_residual.astype(f32) + jnp.sum(mix_parts.astype(f32), 0)
 
@@ -103,34 +181,27 @@
     outgoing = (outgoing * row_scale).astype(jnp.float16).reshape(experts, capacity, feat_block)
     arrived = lax.all_to_all(outgoing, "sp", 0, 0, tiled=True)
     rows = n_sp * capacity
-    gathered = lax.all_gather(arrived.reshape(rows, feat_block), TP, axis=0, tiled=False)
+    gathered = lax.all_gather(arrived.reshape(rows, feat_block).T, TP, axis=0, tiled=True)
 
     wide = gathered.astype(f32)
-    in_mean = jnp.sum(wide, (0, 2)) * (1.0 / (row_scale * features))
-    in_square = jnp.sum(wide * wide, (0, 2)) * (1.0 / (row_scale * row_scale * features))
+    in_mean = jnp.sum(wide, 0) * (1.0 / (row_scale * features))
+    in_square = jnp.sum(wide * wide, 0) * (1.0 / (row_scale * row_scale * features))
     in_rstd = lax.rsqrt(in_square - in_mean * in_mean + norm_eps)
     in_rows = (
-        (wide * (1.0 / row_scale) - in_mean[None, :, None])
-        * in_rstd[None, :, None]
-        * mix_gain.reshape(n_tp, 1, feat_block)
+        (wide * (1.0 / row_scale) - in_mean[None]) * in_rstd[None] * mix_gain[:, None]
     ).astype(bf16)
-    in_rows = in_rows.transpose(1, 0, 2).reshape(rows, features)
-    gate_proj = jnp.dot(in_rows, expert_gate[0], preferred_element_type=f32)
-    up_proj = jnp.dot(in_rows, expert_up[0], preferred_element_type=f32)
+    gate_proj = jnp.einsum("kf,kr->fr", expert_gate[0], in_rows, preferred_element_type=f32)
+    up_proj = jnp.einsum("kf,kr->fr", expert_up[0], in_rows, preferred_element_type=f32)
     hidden = (jax.nn.silu(gate_proj) * up_proj).astype(bf16)
 
-    down_parts = expert_down[0].reshape(-1, n_y, n_c, feat_block)
-    down_mine = lax.dynamic_index_in_dim(down_parts, at_c, 2, keepdims=False)
-    down_else = swap(lax.dynamic_index_in_dim(down_parts, 1 - at_c, 2, keepdims=False), "c")
-    hidden_else = swap(hidden, "c")
-    hidden_both = jnp.concatenate([hidden, hidden_else], 1)
-    down_both = jnp.concatenate([down_mine, down_else], 0)
-    parts = jnp.einsum(
-        "sik,kyf->syif",
-        hidden_both.reshape(n_sp, capacity, -1),
-        down_both,
-        preferred_element_type=f32,
-    ).astype(bf16)
+    w_down = expert_down[0]
+    parts = pl.pallas_call(
+        down_body,
+        out_shape=jax.ShapeDtypeStruct((n_sp, n_y, capacity, feat_block), bf16),
+        in_specs=[whole(pltpu.SMEM)] + [whole()] * 4,
+        out_specs=whole(),
+        name="down",
+    )(at_core, hidden, swap(hidden, "c"), w_down, swap(w_down, "c"))
     parts = parts.reshape(n_sp * n_y, capacity, feat_block)
     returned = lax.all_to_all(parts, ("sp", "y"), 0, 0, tiled=True)
     returned = returned.reshape(experts, n_y, capacity, feat_block)

time: 210 us -> 189 us (0.900)
  local copies, waits for them, and re-layouts: 25.2 us -> 6.29 us
  starting transfers between devices: 63.3 us -> 52.2 us
  Pallas kernels: 0 us -> 10.3 us
  other arithmetic: 13.9 us -> 7.11 us
  waiting for transfers between devices: 67.4 us -> 72.8 us
  blocking collectives: 29.7 us -> 33.2 us
  matrix products: 8.23 us -> 5.26 us
    pallas_call x0 -> x3, Pallas kernels: none -> 10.3 us  [the longest x1 4.63 us: local(): pl.pallas_call(down_body, out_shape=jax.ShapeDtypeStruct((n_sp, n_y, capa...]
    all_to_all x1, starting transfers between devices: 15.9 us -> 9.49 us  [local(): returned = lax.all_to_all(parts, ('sp', 'y'), 0, 0, tiled=True)]
    all_to_all x2 -> x1, waiting for transfers between devices: 14.4 us -> 8.02 us  [summed_over(): return jnp.sum(lax.all_to_all(copies, axis, 0, 0, tiled=True), axis=0)]
    ppermute x2 -> x3, starting transfers between devices: 7.06 us -> 13.3 us  [swap(): return lax.ppermute(value, axis, [(0, 1), (1, 0)])]
    all_to_all x2, waiting for transfers between devices: 10.9 us -> 16.6 us  [the longest x1 10.9 us: local(): mix_parts = lax.all_to_all(mix_parts, 'y', 0, 0, tiled=True)]
    all_to_all x2 -> x1, starting transfers between devices: 11.6 us -> 5.85 us  [summed_over(): return jnp.sum(lax.all_to_all(copies, axis, 0, 0, tiled=True), axis=0)]
    all_gather x1 -> x0, local copies, waits for them, and re-layouts: 5.09 us -> none  [local(): lax.all_gather(arrived.reshape(rows, feat_block), TP, axis=0, tiled=False)]
    all_to_all x1, waiting for transfers between devices: 0.01 us -> 4.85 us  [local(): arrived = lax.all_to_all(outgoing, 'sp', 0, 0, tiled=True)]
  transfers between devices with their start and end apart: 10 -> 9, of which waited for: 5 -> 6; matrix products, arithmetic and copies ran while one was open for 17% -> 5% of each run, Pallas kernels for 0% -> 2%
where the time goes in v2:
time: 189 us; the launch traced here: 188 us
  waiting for transfers between devices  72.8 us (39%)
  starting transfers between devices  52.2 us (28%)
  blocking collectives  33.2 us (18%)
  Pallas kernels  10.3 us (5%)
  other arithmetic  7.11 us (4%)
  local copies, waits for them, and re-layouts  6.29 us (3%)
  matrix products  5.26 us (3%)
    all_to_all x1, waiting for transfers between devices, local(): returned = lax.all_to_all(parts, ('sp', 'y'), 0, 0, tiled=True)  41.5 us
    all_gather x1, blocking collectives, local(): lax.all_gather(arrived.reshape(rows, feat_block).T, TP, axis=0, tiled=True)  31.1 us
    ppermute x3, starting transfers between devices, swap(): return lax.ppermute(value, axis, [(0, 1), (1, 0)])  13.3 us
    all_to_all x1, starting transfers between devices, local(): arrived = lax.all_to_all(outgoing, 'sp', 0, 0, tiled=True)  12.6 us
    all_to_all x1, waiting for transfers between devices, local(): mix_parts = lax.all_to_all(mix_parts, 'y', 0, 0, tiled=True)  10.9 us
    all_to_all x1, starting transfers between devices, local(): returned = lax.all_to_all(parts, ('sp', 'y'), 0, 0, tiled=True)  9.49 us
    all_to_all x1, waiting for transfers between devices, summed_over(): return jnp.sum(lax.all_to_all(copies, axis, 0, 0, tiled=True), axis=0)  8.02 us
    all_to_all x1, starting transfers between devices, summed_over(): return jnp.sum(lax.all_to_all(copies, axis, 0, 0, tiled=True), axis=0)  5.85 us
  transfers between devices with their start and end apart: 9, of which 6 were waited for; matrix products, arithmetic and copies ran while one was open for 5% of the time, Pallas kernels for 2%

profile of v2, /device:TPU:1, one launch (start us, length us, event | category | flops | bytes accessed | tf_op | source)
XLA Modules:
  0.0 188.1 jit_solution(13451800168066024382)
XLA Ops:
  0.0 1.0 fusion.21
  1.0 0.7 convert_element_type.73
  1.8 3.9 %collective-permute-start = (bf16[65,30]{1,0:T(8,128)(2,1)S(1)}, bf16[65,30]{1,0:T(8,128)(2,1)S(1)}, u32[]{:S(2)}, u32[]{:S(2)}) collective-permute-start(bf16[65,30]{1,0:T(8,128)(2,1)S(1)} %pad_maximum_fusion), channel_id=1, source_target_pairs={{0,16},{16,32},{32,48},{48,64},{64,80},{80,96},{96,112},{112,128},... | collective-permute-start | bytes 11708 | tf_op jit(solution)/shard_map/ppermute | solution.py:21
  5.8 6.1 %collective-permute-start.1 = (bf16[64,2048]{1,0:T(8,128)(2,1)}, bf16[64,2048]{1,0:T(8,128)(2,1)S(1)}, u32[]{:S(2)}, u32[]{:S(2)}) collective-permute-start(bf16[64,2048]{1,0:T(8,128)(2,1)} %mine_ref.1), channel_id=1, source_target_pairs={{0,1},{1,0},{2,3},{3,2},{4,5},{5,4},{6,7},{7,6},{8,9},{9,8},{10,11... | collective-permute-start | bytes 786440 | tf_op jit(solution)/shard_map/ppermute | solution.py:25
  11.9 0.8 copy.69
  12.7 0.7 copy.70
  13.6 2.0 %all_gather.6.packed_ref = f32[128,256]{1,0:T(8,128)} all-gather(f32[64,256]{1,0:T(8,128)S(1)} %concatenate.10), channel_id=1, replica_groups=mesh['sp'=32,'y'=8,'c'=2] {'c'}, dimensions={0}, use_global_device_ids=true | all-gather | bytes 196608 | tf_op jit(solution)/shard_map/all_gather | solution.py:143
  16.3 3.4 %conv.1 = (f32[128,192]{1,0:T(8,128)}, f32[8,2,192]{2,1,0:T(2,128)}) custom-call(f32[128,256]{1,0:T(8,128)} %all_gather.6.packed_ref, f32[8,256]{1,0:T(8,128)} %broadcast_in_dim.21.ids_ref), custom_call_target="tpu_custom_call" | custom-call | tf_op jit(solution)/shard_map/conv/pallas_call | solution.py:148
  19.7 3.6 %all-to-all-start = ((f32[8,2,192]{2,1,0:T(2,128)}), f32[8,2,192]{2,1,0:T(2,128)S(1)}, u32[]{:S(2)}, u32[]{:S(2)}) async-start(f32[8,2,192]{2,1,0:T(2,128)} %get-tuple-element.8), calls=%async_computation | async-start | bytes 32768 | tf_op jit(solution)/shard_map/all_to_all | solution.py:158
  23.3 0.8 copy.71
  24.3 5.7 %all-to-all-done.sums_ref = f32[8,2,192]{2,1,0:T(2,128)S(1)} async-done(((f32[8,2,192]{2,1,0:T(2,128)}), f32[8,2,192]{2,1,0:T(2,128)S(1)}, u32[]{:S(2)}, u32[]{:S(2)}) %all-to-all-start) | async-done | bytes 12320 | tf_op jit(solution)/shard_map/all_to_all | solution.py:158
  30.7 2.3 %mix.1 = bf16[8,192,128]{2,1,0:T(8,128)(2,1)} custom-call(s32[1]{0:T(128)} %bitcast.at_ref, f32[128,192]{1,0:T(8,128)} %get-tuple-element.7.filtered_ref, f32[8,2,192]{2,1,0:T(2,128)} %copy-done.6, f32[128,256]{1,0:T(8,128)} %all_gather.6.packed_ref, bf16[64,2048]{1,0:T(8,128)(2,1)} %mine_ref.1, bf16[64,2048]{1,0:T(8,128)(2,1)} %copy-done.5), custom_call_target="tpu_custom_call" | custom-call | tf_op jit(solution)/shard_map/mix/pallas_call | solution.py:160
  33.0 3.5 %all-to-all-start.1 = ((bf16[8,192,128]{2,1,0:T(8,128)(2,1)}), bf16[8,192,128]{2,1,0:T(8,128)(2,1)S(1)}, u32[]{:S(2)}, u32[]{:S(2)}) async-start(bf16[8,192,128]{2,1,0:T(8,128)(2,1)} %mix.1), calls=%async_computation.1 | async-start | bytes 786432 | tf_op jit(solution)/shard_map/all_to_all | solution.py:167
  36.6 0.9 reduce-window.6
  38.3 10.9 %all-to-all-done.1 = bf16[8,192,128]{2,1,0:T(8,128)(2,1)S(1)} async-done(((bf16[8,192,128]{2,1,0:T(8,128)(2,1)}), bf16[8,192,128]{2,1,0:T(8,128)(2,1)S(1)}, u32[]{:S(2)}, u32[]{:S(2)}) %all-to-all-start.1) | async-done | bytes 393248 | tf_op jit(solution)/shard_map/all_to_all | solution.py:167
  49.2 0.8 multiply_add_fusion
  50.7 1.1 fusion.12
  51.8 12.6 %all-to-all-start.2 = ((f16[32,24,128]{2,1,0:T(8,128)(2,1)}), f16[32,24,128]{2,1,0:T(8,128)(2,1)S(1)}, u32[]{:S(2)}, u32[]{:S(2)}) async-start(f16[32,24,128]{2,1,0:T(8,128)(2,1)} %bitcast.14), calls=%async_computation.2 | async-start | bytes 393216 | tf_op jit(solution)/shard_map/all_to_all | solution.py:182
  64.4 5.0 %collective-permute-start.3 = (bf16[320,2048]{1,0:T(8,128)(2,1)S(1)}, bf16[320,2048]{1,0:T(8,128)(2,1)}, u32[]{:S(2)}, u32[]{:S(2)}) collective-permute-start(bf16[320,2048]{1,0:T(8,128)(2,1)S(1)} %bitcast.79), channel_id=1, source_target_pairs={{0,1},{1,0},{2,3},{3,2},{4,5},{5,4},{6,7},{7,6},{8,9},{9,8},{10,11... | collective-permute-start | bytes 3932168 | tf_op jit(solution)/shard_map/ppermute | solution.py:25
  69.4 4.8 %all-to-all-done.2 = f16[32,24,128]{2,1,0:T(8,128)(2,1)S(1)} async-done(((f16[32,24,128]{2,1,0:T(8,128)(2,1)}), f16[32,24,128]{2,1,0:T(8,128)(2,1)S(1)}, u32[]{:S(2)}, u32[]{:S(2)}) %all-to-all-start.2) | async-done | bytes 196640 | tf_op jit(solution)/shard_map/all_to_all | solution.py:182
  74.3 31.1 %all-gather.1 = f16[2048,768]{0,1:T(8,128)(2,1)S(1)} all-gather(f16[128,768]{0,1:T(8,128)(2,1)S(1)} %bitcast.80), channel_id=1, replica_groups=mesh['sp'=32,'y'=8,'c'=2] {'y','c'}, dimensions={0}, use_global_device_ids=true | all-gather | bytes 3342336 | tf_op jit(solution)/shard_map/all_gather | solution.py:184
  105.4 1.0 convert_reduce_fusion
  106.4 1.6 convolution_bitcast_fusion.1
  108.0 1.7 fusion.8.mine_ref
  109.8 2.2 %collective-permute-start.2 = (bf16[320,768]{1,0:T(8,128)(2,1)S(1)}, bf16[320,768]{1,0:T(8,128)(2,1)}, u32[]{:S(2)}, u32[]{:S(2)}) collective-permute-start(bf16[320,768]{1,0:T(8,128)(2,1)S(1)} %fusion.8.mine_ref), channel_id=1, source_target_pairs={{0,1},{1,0},{2,3},{3,2},{4,5},{5,4},{6,7},{7,6},{8,9},{9,8},{10,11... | collective-permute-start | bytes 1474568 | tf_op jit(solution)/shard_map/ppermute | solution.py:25
  112.0 1.8 collective-permute-done.2.else_ref
  113.8 4.6 %down.1 = bf16[32,8,24,128]{3,2,1,0:T(8,128)(2,1)} custom-call(s32[1]{0:T(128)} %bitcast.at_ref, bf16[320,768]{1,0:T(8,128)(2,1)} %copy-done.2, bf16[320,768]{1,0:T(8,128)(2,1)} %collective-permute-done.2.else_ref, bf16[320,2048]{1,0:T(8,128)(2,1)} %bitcast.78, bf16[320,2048]{1,0:T(8,128)(2,1)} %collective-permute-done.3.down_else_ref), custom_call_target="tpu_custom_call" | custom-call | tf_op jit(solution)/shard_map/down/pallas_call | solution.py:198
  118.4 9.5 %all-to-all-start.3 = ((bf16[256,24,128]{2,1,0:T(8,128)(2,1)}), bf16[256,24,128]{2,1,0:T(8,128)(2,1)S(1)}, u32[]{:S(2)}, u32[]{:S(2)}) async-start(bf16[256,24,128]{2,1,0:T(8,128)(2,1)} %bitcast.77), calls=%async_computation.3 | async-start | bytes 3145728 | tf_op jit(solution)/shard_map/all_to_all | solution.py:206
  128.0 41.5 %all-to-all-done.3 = bf16[256,24,128]{2,1,0:T(8,128)(2,1)S(1)} async-done(((bf16[256,24,128]{2,1,0:T(8,128)(2,1)}), bf16[256,24,128]{2,1,0:T(8,128)(2,1)S(1)}, u32[]{:S(2)}, u32[]{:S(2)}) %all-to-all-start.3) | async-done | bytes 1572896 | tf_op jit(solution)/shard_map/all_to_all | solution.py:206
  171.4 5.8 %all-to-all-start.4 = ((f32[16,15,128]{2,1,0:T(8,128)}), f32[16,15,128]{2,1,0:T(8,128)S(1)}, u32[]{:S(2)}, u32[]{:S(2)}) async-start(f32[16,15,128]{2,1,0:T(8,128)} %broadcast_in_dim.46), calls=%async_computation.4 | async-start | bytes 262144 | tf_op jit(solution)/shard_map/all_to_all | solution.py:30
  178.4 8.0 %all-to-all-done.4 = f32[16,15,128]{2,1,0:T(8,128)S(1)} async-done(((f32[16,15,128]{2,1,0:T(8,128)}), f32[16,15,128]{2,1,0:T(8,128)S(1)}, u32[]{:S(2)}, u32[]{:S(2)}) %all-to-all-start.4) | async-done | bytes 122912 | tf_op jit(solution)/shard_map/all_to_all | solution.py:30
  187.3 0.8 multiply_convert_fusion
  (65 shorter events, 6.8 us)
Async XLA Ops:
  0.0 106.4 %copy-start = (bf16[1,2048,320]{1,2,0:T(8,128)(2,1)S(1)}, bf16[1,2048,320]{1,2,0:T(8,128)(2,1)}, u32[]{:S(2)}) copy-start(bf16[1,2048,320]{1,2,0:T(8,128)(2,1)} %param.24) | copy-start | bytes 3932164
  0.0 38.1 %copy-start.7 = (s32[192,2]{0,1:T(2,128)S(1)}, s32[192,2]{0,1:T(2,128)}, u32[]{:S(2)}) copy-start(s32[192,2]{0,1:T(2,128)} %param.22) | copy-start | bytes 4612
  0.0 64.4 %copy-start.1 = (bf16[1,320,2048]{2,1,0:T(8,128)(2,1)S(1)}, bf16[1,320,2048]{2,1,0:T(8,128)(2,1)}, u32[]{:S(2)}) copy-start(bf16[1,320,2048]{2,1,0:T(8,128)(2,1)} %param.26) | copy-start | bytes 3932164
  1.8 11.7 %collective-permute-start = (bf16[65,30]{1,0:T(8,128)(2,1)S(1)}, bf16[65,30]{1,0:T(8,128)(2,1)S(1)}, u32[]{:S(2)}, u32[]{:S(2)}) collective-permute-start(bf16[65,30]{1,0:T(8,128)(2,1)S(1)} %pad_maximum_fusion), channel_id=1, source_target_pairs={{0,16},{16,32},{32,48},{48,64},{64,80},{80,96},{96,112},{112,128},... | collective-permute-start | bytes 11708 | tf_op jit(solution)/shard_map/ppermute | solution.py:21
  5.8 24.2 %collective-permute-start.1 = (bf16[64,2048]{1,0:T(8,128)(2,1)}, bf16[64,2048]{1,0:T(8,128)(2,1)S(1)}, u32[]{:S(2)}, u32[]{:S(2)}) collective-permute-start(bf16[64,2048]{1,0:T(8,128)(2,1)} %mine_ref.1), channel_id=1, source_target_pairs={{0,1},{1,0},{2,3},{3,2},{4,5},{5,4},{6,7},{7,6},{8,9},{9,8},{10,11... | collective-permute-start | bytes 786440 | tf_op jit(solution)/shard_map/ppermute | solution.py:25
  19.7 10.3 %all-to-all-start = ((f32[8,2,192]{2,1,0:T(2,128)}), f32[8,2,192]{2,1,0:T(2,128)S(1)}, u32[]{:S(2)}, u32[]{:S(2)}) async-start(f32[8,2,192]{2,1,0:T(2,128)} %get-tuple-element.8), calls=%async_computation | async-start | bytes 32768 | tf_op jit(solution)/shard_map/all_to_all | solution.py:158
  30.0 0.6 copy-start.6
  30.0 0.7 copy-start.5
  33.0 16.2 %all-to-all-start.1 = ((bf16[8,192,128]{2,1,0:T(8,128)(2,1)}), bf16[8,192,128]{2,1,0:T(8,128)(2,1)S(1)}, u32[]{:S(2)}, u32[]{:S(2)}) async-start(bf16[8,192,128]{2,1,0:T(8,128)(2,1)} %mix.1), calls=%async_computation.1 | async-start | bytes 786432 | tf_op jit(solution)/shard_map/all_to_all | solution.py:167
  50.1 0.6 copy-start.3
  51.8 22.5 %all-to-all-start.2 = ((f16[32,24,128]{2,1,0:T(8,128)(2,1)}), f16[32,24,128]{2,1,0:T(8,128)(2,1)S(1)}, u32[]{:S(2)}, u32[]{:S(2)}) async-start(f16[32,24,128]{2,1,0:T(8,128)(2,1)} %bitcast.14), calls=%async_computation.2 | async-start | bytes 393216 | tf_op jit(solution)/shard_map/all_to_all | solution.py:182
  64.4 47.6 %collective-permute-start.3 = (bf16[320,2048]{1,0:T(8,128)(2,1)S(1)}, bf16[320,2048]{1,0:T(8,128)(2,1)}, u32[]{:S(2)}, u32[]{:S(2)}) collective-permute-start(bf16[320,2048]{1,0:T(8,128)(2,1)S(1)} %bitcast.79), channel_id=1, source_target_pairs={{0,1},{1,0},{2,3},{3,2},{4,5},{5,4},{6,7},{7,6},{8,9},{9,8},{10,11... | collective-permute-start | bytes 3932168 | tf_op jit(solution)/shard_map/ppermute | solution.py:25
  74.3 32.1 %copy-start.8 = (f32[2048]{0:T(1024)S(1)}, f32[2048]{0:T(1024)}, u32[]{:S(2)}) copy-start(f32[2048]{0:T(1024)} %param.21) | copy-start | bytes 24580
  106.4 1.6 copy-start.11
  109.8 4.0 %copy-start.2 = (bf16[320,768]{1,0:T(8,128)(2,1)}, bf16[320,768]{1,0:T(8,128)(2,1)S(1)}, u32[]{:S(2)}) copy-start(bf16[320,768]{1,0:T(8,128)(2,1)S(1)} %fusion.8.mine_ref) | copy-start | bytes 1474564
  109.8 18.3 %copy-start.9 = (f32[192,2]{0,1:T(2,128)S(1)}, f32[192,2]{0,1:T(2,128)}, u32[]{:S(2)}) copy-start(f32[192,2]{0,1:T(2,128)} %param.23) | copy-start | bytes 4612
  109.8 4.0 %collective-permute-start.2 = (bf16[320,768]{1,0:T(8,128)(2,1)S(1)}, bf16[320,768]{1,0:T(8,128)(2,1)}, u32[]{:S(2)}, u32[]{:S(2)}) collective-permute-start(bf16[320,768]{1,0:T(8,128)(2,1)S(1)} %fusion.8.mine_ref), channel_id=1, source_target_pairs={{0,1},{1,0},{2,3},{3,2},{4,5},{5,4},{6,7},{7,6},{8,9},{9,8},{10,11... | collective-permute-start | bytes 1474568 | tf_op jit(solution)/shard_map/ppermute | solution.py:25
  118.4 51.7 %copy-start.4 = (f32[192,128]{1,0:T(8,128)S(1)}, f32[192,128]{1,0:T(8,128)}, u32[]{:S(2)}) copy-start(f32[192,128]{1,0:T(8,128)} %copy-done.3) | copy-start | bytes 294916
  118.4 68.8 %copy-start.10 = (f32[128]{0:T(128)S(1)}, f32[128]{0:T(128)}, u32[]{:S(2)}) copy-start(f32[128]{0:T(128)} %param.27) | copy-start | bytes 1540
  118.4 51.1 %all-to-all-start.3 = ((bf16[256,24,128]{2,1,0:T(8,128)(2,1)}), bf16[256,24,128]{2,1,0:T(8,128)(2,1)S(1)}, u32[]{:S(2)}, u32[]{:S(2)}) async-start(bf16[256,24,128]{2,1,0:T(8,128)(2,1)} %bitcast.77), calls=%async_computation.3 | async-start | bytes 3145728 | tf_op jit(solution)/shard_map/all_to_all | solution.py:206
  171.4 15.0 %all-to-all-start.4 = ((f32[16,15,128]{2,1,0:T(8,128)}), f32[16,15,128]{2,1,0:T(8,128)S(1)}, u32[]{:S(2)}, u32[]{:S(2)}) async-start(f32[16,15,128]{2,1,0:T(8,128)} %broadcast_in_dim.46), calls=%async_computation.4 | async-start | bytes 262144 | tf_op jit(solution)/shard_map/all_to_all | solution.py:30

commit v3 on v2

--- a/solution.py
+++ b/solution.py
@@ -30,45 +30,49 @@
     return jnp.sum(lax.all_to_all(copies, axis, 0, 0, tiled=True), axis=0)
 
 
-def conv_body(packed_ref, ids_ref, filtered_ref, sums_ref, *, lags, tok_rows):
+def conv_body(packed_ref, ids_ref, out_ref, *, lags, tok_rows):
     packed = packed_ref[...]
     ids = ids_ref[...]
-    total = jnp.zeros((packed.shape[0], tok_rows), jnp.float32)
+    lane = lax.broadcasted_iota(jnp.int32, packed.shape, 1)
+    total = jnp.zeros_like(packed)
     for lag in range(lags):
         rows = packed if lag == 0 else pltpu.roll(packed, lag, 1)
         other = ids if lag == 0 else pltpu.roll(ids, lag, 1)
-        same_doc = other[:1, :tok_rows] == ids[:1, :tok_rows]
         tap = packed[:, tok_rows + lag : tok_rows + lag + 1]
-        total = total + jnp.where(same_doc, rows[:, :tok_rows], 0.0) * tap
-    filtered_ref[...] = total
-    sums = jnp.concatenate(
-        [jnp.sum(total, 0, keepdims=True), jnp.sum(total * total, 0, keepdims=True)], 0
-    )
-    sums_ref[...] = jnp.broadcast_to(sums[None], sums_ref.shape)
-
-
-def mix_body(at_ref, filtered_ref, sums_ref, packed_ref, mine_ref, else_ref, out_ref, *, gain_at, channels):
-    first = at_ref[0] == 0
-    peers, tok_rows, block = out_ref.shape
-    sums = jnp.sum(sums_ref[...], 0)
-    row_mean = sums[:1] / channels
-    row_var = sums[1:] / channels - row_mean * row_mean
-    gain = packed_ref[:, gain_at : gain_at + 1]
-    normed = (filtered_ref[...] - row_mean) * lax.rsqrt(row_var + norm_eps) * gain
-    conv_out = (normed / (1.0 + jnp.exp(-normed))).T.astype(jnp.bfloat16)
-    for peer in range(0, peers, 2):
-        columns = []
-        for step in range(2):
-            at = pl.multiple_of((2 * (peer + step) + at_ref[0]) * block, block)
-            mine, other = mine_ref[:, pl.ds(at, block)], else_ref[:, pl.ds(at, block)]
-            columns.append(
-                jnp.concatenate([jnp.where(first, mine, other), jnp.where(first, other, mine)], 0)
-            )
-        part = jnp.dot(
-            conv_out, jnp.concatenate(columns, 1), preferred_element_type=jnp.float32
-        ).astype(jnp.bfloat16)
-        out_ref[peer] = part[:, :block]
-        out_ref[peer + 1] = part[:, block:]
+        total = total + jnp.where(other[:1] == ids[:1], rows, 0.0) * tap
+    left = packed[:, tok_rows + lags : tok_rows + lags + 1]
+    out = jnp.where(lane < tok_rows, total, 0.0).astype(jnp.bfloat16).astype(jnp.float32)
+    for piece in range(3):
+        rounded = left.astype(jnp.bfloat16).astype(jnp.float32)
+        out = jnp.where(lane == tok_rows + piece, rounded, out)
+        left = left - rounded
+    out_ref[...] = out.astype(jnp.bfloat16)
+
+
+def mix_body(slot_ref, filtered_ref, weight_ref, residual_ref, z_ref, out_ref):
+    channels = filtered_ref.shape[0]
+    tok_rows = z_ref.shape[0]
+    filtered = filtered_ref[...].astype(jnp.float32)
+    gain = jnp.sum(filtered[:, tok_rows : tok_rows + 3], 1, keepdims=True)
+    filtered = filtered[:, :tok_rows]
+    row_mean = jnp.sum(filtered, 0, keepdims=True) / channels
+    row_var = jnp.sum(filtered * filtered, 0, keepdims=True) / channels - row_mean * row_mean
+    normed = (filtered - row_mean) * lax.rsqrt(row_var + norm_eps) * gain
+    conv_out = (normed / (1.0 + jnp.exp(-normed))).astype(jnp.bfloat16)
+    mix = lax.dot_general(
+        conv_out, weight_ref[...], (((0,), (0,)), ((), ())), preferred_element_type=jnp.float32
+    )
+    z = residual_alpha * residual_ref[...].astype(jnp.float32) + mix
+    z_ref[...] = z
+    experts, capacity, block = out_ref.shape
+    slot = lax.broadcasted_iota(jnp.int32, (experts * capacity, tok_rows), 0)
+    table = (slot == slot_ref[:1]) | (slot == slot_ref[1:2])
+    outgoing = jnp.dot(
+        jnp.where(table, 1.0, 0.0).astype(jnp.bfloat16),
+        z.astype(jnp.bfloat16),
+        preferred_element_type=jnp.float32,
+    )
+    out_ref[...] = outgoing.astype(jnp.bfloat16).reshape(experts, capacity, block)
 
 
 def down_body(at_ref, mine_ref, else_ref, down_mine_ref, down_else_ref, out_ref):
@@ -119,7 +123,6 @@
     tok_rows, own_ch = glu_value.shape
     lags = conv_kernel.shape[0]
     rim_len = lags - 1
-    channels = own_ch * n_tp
     features = residual.shape[1]
     feat_block = features // n_tp
 
@@ -140,33 +143,21 @@
         ],
         1,
     )
-    packed = lax.all_gather(packed, "c", axis=0, tiled=True)
     packed_ids = jnp.concatenate(
         [ids, jnp.zeros((1, lanes - tok_rows - rim_len), f32), rim[own_ch:]], 1
     )
     packed_ids = jnp.broadcast_to(packed_ids, (8, lanes))
-    filtered, sums = pl.pallas_call(
+    filtered = pl.pallas_call(
         functools.partial(conv_body, lags=lags, tok_rows=tok_rows),
-        out_shape=(
-            jax.ShapeDtypeStruct((n_c * own_ch, tok_rows), f32),
-            jax.ShapeDtypeStruct((n_y, 2, tok_rows), f32),
-        ),
+        out_shape=jax.ShapeDtypeStruct((own_ch, lanes), bf16),
         in_specs=[whole()] * 2,
-        out_specs=(whole(), whole()),
+        out_specs=whole(),
         name="conv",
     )(packed, packed_ids)
-    sums = lax.all_to_all(sums, "y", 0, 0, tiled=True)
-    weight_else = swap(out_weight, "c")
-    mix_parts = pl.pallas_call(
-        functools.partial(mix_body, gain_at=tok_rows + lags, channels=channels),
-        out_shape=jax.ShapeDtypeStruct((n_y, tok_rows, feat_block), bf16),
-        in_specs=[whole(pltpu.SMEM)] + [whole()] * 5,
-        out_specs=whole(),
-        name="mix",
-    )(at_core, filtered, sums, packed, out_weight, weight_else)
-    mix_parts = lax.all_to_all(mix_parts, "y", 0, 0, tiled=True)
+    filtered = lax.all_gather(filtered, TP, axis=0, tiled=True)
+    weight_parts = out_weight.reshape(own_ch, n_tp, feat_block).transpose(1, 0, 2)
+    weight_own = lax.all_to_all(weight_parts, TP, 0, 0, tiled=True).reshape(-1, feat_block)
     own_residual = lax.dynamic_slice_in_dim(residual, at_tp * feat_block, feat_block, 1)
-    own_z = residual_alpha * own_residual.astype(f32) + jnp.sum(mix_parts.astype(f32), 0)
 
     experts = expert_gate.shape[0] * n_sp
     capacity = 4 * tok_rows // experts
@@ -175,13 +166,22 @@
     earlier = jnp.cumsum(member, 0) - member
     slot_index = (chosen * capacity + jnp.sum(earlier * member, 1)).reshape(tok_rows, 2)
     slots = jnp.arange(experts * capacity, dtype=jnp.int32)
-    dispatch_table = jnp.any(slots[:, None, None] == slot_index[None], -1).astype(bf16)
-
-    outgoing = jnp.dot(dispatch_table, own_z.astype(bf16), preferred_element_type=f32)
-    outgoing = (outgoing * row_scale).astype(jnp.float16).reshape(experts, capacity, feat_block)
+    slot_rows = jnp.concatenate([slot_index.T, jnp.zeros((6, tok_rows), jnp.int32)], 0)
+
+    own_z, outgoing = pl.pallas_call(
+        mix_body,
+        out_shape=(
+            jax.ShapeDtypeStruct((tok_rows, feat_block), f32),
+            jax.ShapeDtypeStruct((experts, capacity, feat_block), bf16),
+        ),
+        in_specs=[whole()] * 4,
+        out_specs=(whole(), whole()),
+        name="mix",
+    )(slot_rows, filtered, weight_own, own_residual)
     arrived = lax.all_to_all(outgoing, "sp", 0, 0, tiled=True)
     rows = n_sp * capacity
-    gathered = lax.all_gather(arrived.reshape(rows, feat_block).T, TP, axis=0, tiled=True)
+    arrived = (arrived.reshape(rows, feat_block).T.astype(f32) * row_scale).astype(jnp.float16)
+    gathered = lax.all_gather(arrived, TP, axis=0, tiled=True)
 
     wide = gathered.astype(f32)
     in_mean = jnp.sum(wide, 0) * (1.0 / (row_scale * features))

time: 189 us -> 186 us (0.984)
  blocking collectives: 33.2 us -> 47.1 us
  waiting for transfers between devices: 72.8 us -> 59.5 us
  starting transfers between devices: 52.2 us -> 46.1 us
  local copies, waits for them, and re-layouts: 6.29 us -> 10.8 us
    all_to_all x2 -> x1, waiting for transfers between devices: 16.6 us -> 0.01 us  [local(): lax.all_to_all(weight_parts, TP, 0, 0, tiled=True).reshape(-1, feat_block)]
    all_gather x2, blocking collectives: 33.2 us -> 47.1 us  [the longest x1 26.9 us: local(): gathered = lax.all_gather(arrived, TP, axis=0, tiled=True)]
    ppermute x3 -> x2, starting transfers between devices: 13.3 us -> 4.39 us  [swap(): return lax.ppermute(value, axis, [(0, 1), (1, 0)])]
    all_to_all x1, waiting for transfers between devices: 4.85 us -> 8.26 us  [local(): arrived = lax.all_to_all(outgoing, 'sp', 0, 0, tiled=True)]
    all_to_all x2 -> x1, starting transfers between devices: 7.04 us -> 8.07 us  [local(): lax.all_to_all(weight_parts, TP, 0, 0, tiled=True).reshape(-1, feat_block)]
  transfers between devices with their start and end apart: 9 -> 7, of which waited for: 6 -> 4; matrix products, arithmetic and copies ran while one was open for 5% -> 8% of each run, Pallas kernels for 2% -> 1%
where the time goes in v3:
time: 186 us; the launch traced here: 185 us
  waiting for transfers between devices  59.5 us (32%)
  blocking collectives  47.1 us (25%)
  starting transfers between devices  46.1 us (25%)
  local copies, waits for them, and re-layouts  10.8 us (6%)
  Pallas kernels  10 us (5%)
  other arithmetic  6.8 us (4%)
  matrix products  4.14 us (2%)
    all_to_all x1, waiting for transfers between devices, local(): returned = lax.all_to_all(parts, ('sp', 'y'), 0, 0, tiled=True)  41.5 us
    all_gather x1, blocking collectives, local(): gathered = lax.all_gather(arrived, TP, axis=0, tiled=True)  26.9 us
    all_gather x1, blocking collectives, local(): filtered = lax.all_gather(filtered, TP, axis=0, tiled=True)  20.3 us
    all_to_all x1, starting transfers between devices, local(): arrived = lax.all_to_all(outgoing, 'sp', 0, 0, tiled=True)  12.6 us
    all_to_all x1, starting transfers between devices, local(): returned = lax.all_to_all(parts, ('sp', 'y'), 0, 0, tiled=True)  11.2 us
    all_to_all x1, waiting for transfers between devices, local(): arrived = lax.all_to_all(outgoing, 'sp', 0, 0, tiled=True)  8.26 us
    all_to_all x1, starting transfers between devices, local(): lax.all_to_all(weight_parts, TP, 0, 0, tiled=True).reshape(-1, feat_block)  8.07 us
    all_to_all x1, waiting for transfers between devices, summed_over(): return jnp.sum(lax.all_to_all(copies, axis, 0, 0, tiled=True), axis=0)  8.02 us
  transfers between devices with their start and end apart: 7, of which 4 were waited for; matrix products, arithmetic and copies ran while one was open for 8% of the time, Pallas kernels for 1%

profile of v3, /device:TPU:1, one launch (start us, length us, event | category | flops | bytes accessed | tf_op | source)
XLA Modules:
  0.0 185.3 jit_solution(2389516280867305447)
XLA Ops:
  0.0 0.8 convert_element_type.75
  0.9 0.8 fusion.18
  1.8 3.9 %collective-permute-start = (bf16[65,30]{1,0:T(8,128)(2,1)S(1)}, bf16[65,30]{1,0:T(8,128)(2,1)S(1)}, u32[]{:S(2)}, u32[]{:S(2)}) collective-permute-start(bf16[65,30]{1,0:T(8,128)(2,1)S(1)} %pad_maximum_fusion), channel_id=1, source_target_pairs={{0,16},{16,32},{32,48},{48,64},{64,80},{80,96},{96,112},{112,128},... | collective-permute-start | bytes 11708 | tf_op jit(solution)/shard_map/ppermute | solution.py:21
  5.8 1.7 bitcast_bitcast_fusion
  7.5 8.1 %all-to-all-start = ((bf16[16,64,128]{2,1,0:T(8,128)(2,1)}), bf16[16,64,128]{2,1,0:T(8,128)(2,1)S(1)}, u32[]{:S(2)}, u32[]{:S(2)}) async-start(bf16[16,64,128]{2,1,0:T(8,128)(2,1)} %bitcast_bitcast_fusion), calls=%async_computation | async-start | bytes 524288 | tf_op jit(solution)/shard_map/all_to_all | solution.py:159
  15.5 0.8 copy.60
  16.6 0.9 reduce-window.6
  18.1 0.7 multiply_add_fusion
  18.8 1.4 constant_dynamic-slice_fusion.residual_ref
  20.8 0.8 copy.64
  21.6 0.7 copy.65
  22.5 0.7 concatenate.14.packed_ref
  23.9 2.4 %conv.1 = bf16[64,256]{1,0:T(8,128)(2,1)} custom-call(f32[64,256]{1,0:T(8,128)} %concatenate.14.packed_ref, f32[8,256]{1,0:T(8,128)} %broadcast_in_dim.21.ids_ref), custom_call_target="tpu_custom_call" | custom-call | tf_op jit(solution)/shard_map/conv/pallas_call | solution.py:150
  26.3 20.3 %all_gather.6.filtered_ref = bf16[1024,256]{1,0:T(8,128)(2,1)} all-gather(bf16[64,256]{1,0:T(8,128)(2,1)} %conv.1), channel_id=1, replica_groups=mesh['sp'=32,'y'=8,'c'=2] {'y','c'}, dimensions={0}, use_global_device_ids=true | all-gather | bytes 557056 | tf_op jit(solution)/shard_map/all_gather | solution.py:157
  46.6 0.7 copy-done.2
  47.3 3.0 %mix.1 = (f32[192,128]{1,0:T(8,128)}, bf16[32,24,128]{2,1,0:T(8,128)(2,1)}) custom-call(s32[8,192]{1,0:T(8,128)} %concatenate.12.slot_ref, bf16[1024,256]{1,0:T(8,128)(2,1)} %all_gather.6.filtered_ref, bf16[1024,128]{1,0:T(8,128)(2,1)} %bitcast.87, bf16[192,128]{1,0:T(8,128)(2,1)} %constant_dynamic-slice_fusion.residual_ref), custom_call_target="tpu_custom_call" | custom-call | tf_op jit(solution)/shard_map/mix/pallas_call | solution.py:171
  50.2 12.6 %all-to-all-start.1 = ((bf16[32,24,128]{2,1,0:T(8,128)(2,1)}), bf16[32,24,128]{2,1,0:T(8,128)(2,1)S(1)}, u32[]{:S(2)}, u32[]{:S(2)}) async-start(bf16[32,24,128]{2,1,0:T(8,128)(2,1)} %get-tuple-element.8), calls=%async_computation.1 | async-start | bytes 393216 | tf_op jit(solution)/shard_map/all_to_all | solution.py:181
  62.8 2.4 %collective-permute-start.2 = (bf16[320,2048]{1,0:T(8,128)(2,1)S(1)}, bf16[320,2048]{1,0:T(8,128)(2,1)}, u32[]{:S(2)}, u32[]{:S(2)}) collective-permute-start(bf16[320,2048]{1,0:T(8,128)(2,1)S(1)} %bitcast.86), channel_id=1, source_target_pairs={{0,1},{1,0},{2,3},{3,2},{4,5},{5,4},{6,7},{7,6},{8,9},{9,8},{10,11... | collective-permute-start | bytes 3932168 | tf_op jit(solution)/shard_map/ppermute | solution.py:25
  65.2 8.3 %all-to-all-done.1 = bf16[32,24,128]{2,1,0:T(8,128)(2,1)S(1)} async-done(((bf16[32,24,128]{2,1,0:T(8,128)(2,1)}), bf16[32,24,128]{2,1,0:T(8,128)(2,1)S(1)}, u32[]{:S(2)}, u32[]{:S(2)}) %all-to-all-start.1) | async-done | bytes 196640 | tf_op jit(solution)/shard_map/all_to_all | solution.py:181
  73.5 26.9 %all-gather.1 = f16[2048,768]{0,1:T(8,128)(2,1)S(1)} all-gather(f16[128,768]{0,1:T(8,128)(2,1)S(1)} %bitcast.88), channel_id=1, replica_groups=mesh['sp'=32,'y'=8,'c'=2] {'y','c'}, dimensions={0}, use_global_device_ids=true | all-gather | bytes 3342336 | tf_op jit(solution)/shard_map/all_gather | solution.py:184
  100.4 1.0 convert_reduce_fusion
  101.4 1.6 convolution_bitcast_fusion.1
  103.0 1.7 fusion.8.mine_ref
  104.8 2.0 %collective-permute-start.1 = (bf16[320,768]{1,0:T(8,128)(2,1)S(1)}, bf16[320,768]{1,0:T(8,128)(2,1)S(1)}, u32[]{:S(2)}, u32[]{:S(2)}) collective-permute-start(bf16[320,768]{1,0:T(8,128)(2,1)S(1)} %fusion.8.mine_ref), channel_id=1, source_target_pairs={{0,1},{1,0},{2,3},{3,2},{4,5},{5,4},{6,7},{7,6},{8,9},{9,8},{10,11... | collective-permute-start | bytes 1474568 | tf_op jit(solution)/shard_map/ppermute | solution.py:25
  106.8 1.7 collective-permute-done.1.else_ref
  108.5 0.8 copy-done.4
  109.4 4.6 %down.1 = bf16[32,8,24,128]{3,2,1,0:T(8,128)(2,1)} custom-call(s32[1]{0:T(128)} %bitcast.16.at_ref, bf16[320,768]{1,0:T(8,128)(2,1)} %copy-done.3, bf16[320,768]{1,0:T(8,128)(2,1)} %copy-done.4, bf16[320,2048]{1,0:T(8,128)(2,1)} %bitcast.85, bf16[320,2048]{1,0:T(8,128)(2,1)} %collective-permute-done.2.down_else_ref), custom_call_target="tpu_custom_call" | custom-call | tf_op jit(solution)/shard_map/down/pallas_call | solution.py:198
  114.0 11.2 %all-to-all-start.2 = ((bf16[256,24,128]{2,1,0:T(8,128)(2,1)}), bf16[256,24,128]{2,1,0:T(8,128)(2,1)S(1)}, u32[]{:S(2)}, u32[]{:S(2)}) async-start(bf16[256,24,128]{2,1,0:T(8,128)(2,1)} %bitcast.84), calls=%async_computation.2 | async-start | bytes 3145728 | tf_op jit(solution)/shard_map/all_to_all | solution.py:206
  125.3 41.5 %all-to-all-done.2 = bf16[256,24,128]{2,1,0:T(8,128)(2,1)S(1)} async-done(((bf16[256,24,128]{2,1,0:T(8,128)(2,1)}), bf16[256,24,128]{2,1,0:T(8,128)(2,1)S(1)}, u32[]{:S(2)}, u32[]{:S(2)}) %all-to-all-start.2) | async-done | bytes 1572896 | tf_op jit(solution)/shard_map/all_to_all | solution.py:206
  168.7 5.9 %all-to-all-start.3 = ((f32[16,15,128]{2,1,0:T(8,128)}), f32[16,15,128]{2,1,0:T(8,128)S(1)}, u32[]{:S(2)}, u32[]{:S(2)}) async-start(f32[16,15,128]{2,1,0:T(8,128)} %broadcast_in_dim.46), calls=%async_computation.3 | async-start | bytes 262144 | tf_op jit(solution)/shard_map/all_to_all | solution.py:30
  175.7 8.0 %all-to-all-done.3 = f32[16,15,128]{2,1,0:T(8,128)S(1)} async-done(((f32[16,15,128]{2,1,0:T(8,128)}), f32[16,15,128]{2,1,0:T(8,128)S(1)}, u32[]{:S(2)}, u32[]{:S(2)}) %all-to-all-start.3) | async-done | bytes 122912 | tf_op jit(solution)/shard_map/all_to_all | solution.py:30
  184.5 0.8 multiply_convert_fusion.1
  (57 shorter events, 5.8 us)
Async XLA Ops:
  0.0 101.4 %copy-start = (bf16[1,2048,320]{1,2,0:T(8,128)(2,1)S(1)}, bf16[1,2048,320]{1,2,0:T(8,128)(2,1)}, u32[]{:S(2)}) copy-start(bf16[1,2048,320]{1,2,0:T(8,128)(2,1)} %param.24) | copy-start | bytes 3932164
  0.0 62.8 %copy-start.1 = (bf16[1,320,2048]{2,1,0:T(8,128)(2,1)S(1)}, bf16[1,320,2048]{2,1,0:T(8,128)(2,1)}, u32[]{:S(2)}) copy-start(bf16[1,320,2048]{2,1,0:T(8,128)(2,1)} %param.26) | copy-start | bytes 3932164
  1.8 20.6 %collective-permute-start = (bf16[65,30]{1,0:T(8,128)(2,1)S(1)}, bf16[65,30]{1,0:T(8,128)(2,1)S(1)}, u32[]{:S(2)}, u32[]{:S(2)}) collective-permute-start(bf16[65,30]{1,0:T(8,128)(2,1)S(1)} %pad_maximum_fusion), channel_id=1, source_target_pairs={{0,16},{16,32},{32,48},{48,64},{64,80},{80,96},{96,112},{112,128},... | collective-permute-start | bytes 11708 | tf_op jit(solution)/shard_map/ppermute | solution.py:21
  7.5 39.1 %all-to-all-start = ((bf16[16,64,128]{2,1,0:T(8,128)(2,1)}), bf16[16,64,128]{2,1,0:T(8,128)(2,1)S(1)}, u32[]{:S(2)}, u32[]{:S(2)}) async-start(bf16[16,64,128]{2,1,0:T(8,128)(2,1)} %bitcast_bitcast_fusion), calls=%async_computation | async-start | bytes 524288 | tf_op jit(solution)/shard_map/all_to_all | solution.py:159
  46.6 0.7 copy-start.2
  50.2 23.2 %all-to-all-start.1 = ((bf16[32,24,128]{2,1,0:T(8,128)(2,1)}), bf16[32,24,128]{2,1,0:T(8,128)(2,1)S(1)}, u32[]{:S(2)}, u32[]{:S(2)}) async-start(bf16[32,24,128]{2,1,0:T(8,128)(2,1)} %get-tuple-element.8), calls=%async_computation.1 | async-start | bytes 393216 | tf_op jit(solution)/shard_map/all_to_all | solution.py:181
  62.8 44.0 %collective-permute-start.2 = (bf16[320,2048]{1,0:T(8,128)(2,1)S(1)}, bf16[320,2048]{1,0:T(8,128)(2,1)}, u32[]{:S(2)}, u32[]{:S(2)}) collective-permute-start(bf16[320,2048]{1,0:T(8,128)(2,1)S(1)} %bitcast.86), channel_id=1, source_target_pairs={{0,1},{1,0},{2,3},{3,2},{4,5},{5,4},{6,7},{7,6},{8,9},{9,8},{10,11... | collective-permute-start | bytes 3932168 | tf_op jit(solution)/shard_map/ppermute | solution.py:25
  73.5 27.9 %copy-start.6 = (f32[2048]{0:T(1024)S(1)}, f32[2048]{0:T(1024)}, u32[]{:S(2)}) copy-start(f32[2048]{0:T(1024)} %param.21) | copy-start | bytes 24580
  101.4 1.6 copy-start.9
  104.8 4.6 %copy-start.3 = (bf16[320,768]{1,0:T(8,128)(2,1)}, bf16[320,768]{1,0:T(8,128)(2,1)S(1)}, u32[]{:S(2)}) copy-start(bf16[320,768]{1,0:T(8,128)(2,1)S(1)} %fusion.8.mine_ref) | copy-start | bytes 1474564
  104.8 3.8 %collective-permute-start.1 = (bf16[320,768]{1,0:T(8,128)(2,1)S(1)}, bf16[320,768]{1,0:T(8,128)(2,1)S(1)}, u32[]{:S(2)}, u32[]{:S(2)}) collective-permute-start(bf16[320,768]{1,0:T(8,128)(2,1)S(1)} %fusion.8.mine_ref), channel_id=1, source_target_pairs={{0,1},{1,0},{2,3},{3,2},{4,5},{5,4},{6,7},{7,6},{8,9},{9,8},{10,11... | collective-permute-start | bytes 1474568 | tf_op jit(solution)/shard_map/ppermute | solution.py:25
  108.5 0.8 copy-start.4
  109.4 15.9 %copy-start.7 = (f32[192,2]{0,1:T(2,128)S(1)}, f32[192,2]{0,1:T(2,128)}, u32[]{:S(2)}) copy-start(f32[192,2]{0,1:T(2,128)} %param.23) | copy-start | bytes 4612
  114.0 53.3 %copy-start.5 = (f32[192,128]{1,0:T(8,128)S(1)}, f32[192,128]{1,0:T(8,128)}, u32[]{:S(2)}) copy-start(f32[192,128]{1,0:T(8,128)} %get-tuple-element.7) | copy-start | bytes 294916
  114.0 70.5 %copy-start.8 = (f32[128]{0:T(128)S(1)}, f32[128]{0:T(128)}, u32[]{:S(2)}) copy-start(f32[128]{0:T(128)} %param.27) | copy-start | bytes 1540
  114.0 52.8 %all-to-all-start.2 = ((bf16[256,24,128]{2,1,0:T(8,128)(2,1)}), bf16[256,24,128]{2,1,0:T(8,128)(2,1)S(1)}, u32[]{:S(2)}, u32[]{:S(2)}) async-start(bf16[256,24,128]{2,1,0:T(8,128)(2,1)} %bitcast.84), calls=%async_computation.2 | async-start | bytes 3145728 | tf_op jit(solution)/shard_map/all_to_all | solution.py:206
  168.7 15.1 %all-to-all-start.3 = ((f32[16,15,128]{2,1,0:T(8,128)}), f32[16,15,128]{2,1,0:T(8,128)S(1)}, u32[]{:S(2)}, u32[]{:S(2)}) async-start(f32[16,15,128]{2,1,0:T(8,128)} %broadcast_in_dim.46), calls=%async_computation.3 | async-start | bytes 262144 | tf_op jit(solution)/shard_map/all_to_all | solution.py:30

commit v4 on v3

v4 whole, which is shorter than its diff:
```python
import functools

import jax
import jax.numpy as jnp
from jax import lax
from jax.experimental import pallas as pl
from jax.experimental.pallas import tpu as pltpu
from jax.sharding import Mesh
from jax.sharding import PartitionSpec as P

TP = ("y", "c")

residual_alpha = 1.41421356
norm_eps = 1e-05
row_scale = 64.0


def from_behind(value, axis, by):
    peers = lax.axis_size(axis)
    pairs = [(i, i + by) for i in range(peers) if 0 <= i + by < peers]
    return lax.ppermute(value, axis, pairs)


def swap(value, axis):
    return lax.ppermute(value, axis, [(0, 1), (1, 0)])


def summed_over(value, axis, peers):
    copies = jnp.broadcast_to(value[None], (peers, *value.shape))
    return jnp.sum(lax.all_to_all(copies, axis, 0, 0, tiled=True), axis=0)


def head_body(value_ref, gate_ref, ids_ref, own_ref, rim_ref):
    own_ch, tok_rows = value_ref.shape
    gate = gate_ref[...].astype(jnp.float32)
    gated = value_ref[...].astype(jnp.float32) * (1.0 / (1.0 + jnp.exp(-gate)))
    gated = gated.astype(jnp.bfloat16).astype(jnp.float32)
    ids = jnp.broadcast_to(ids_ref[...].astype(jnp.float32), (own_ref.shape[0] - own_ch, tok_rows))
    rows = jnp.concatenate([gated, ids], 0)
    rows = jnp.concatenate([rows, jnp.zeros((rows.shape[0], own_ref.shape[1] - tok_rows), jnp.float32)], 1)
    own_ref[...] = rows.astype(jnp.bfloat16)
    shifted = pltpu.roll(rows, own_ref.shape[1] - (tok_rows - 128), 1)
    rim_ref[...] = shifted[:, :128].astype(jnp.bfloat16)


def conv_body(own_ref, rim_ref, taps_ref, out_ref, *, lags, tok_rows):
    own_ch = out_ref.shape[0]
    own = own_ref[...].astype(jnp.float32)
    rim = rim_ref[...].astype(jnp.float32)
    lane = lax.broadcasted_iota(jnp.int32, rim.shape, 1)
    behind = jnp.where(lane < tok_rows - 128, own[:, 128:], rim)
    packed = jnp.concatenate([own[:, :128], behind], 1)
    rows, ids = packed[:own_ch], packed[own_ch : own_ch + 8]
    taps = taps_ref[...]
    total = jnp.zeros_like(rows)
    for lag in range(lags):
        moved = rows if lag == 0 else pltpu.roll(rows, lag, 1)
        other = ids if lag == 0 else pltpu.roll(ids, lag, 1)
        total = total + jnp.where(other[:1] == ids[:1], moved, 0.0) * taps[:, lag : lag + 1]
    left = taps[:, lags : lags + 1]
    lane = lax.broadcasted_iota(jnp.int32, rows.shape, 1)
    out = jnp.where(lane < tok_rows, total, 0.0).astype(jnp.bfloat16).astype(jnp.float32)
    for piece in range(3):
        rounded = left.astype(jnp.bfloat16).astype(jnp.float32)
        out = jnp.where(lane == tok_rows + piece, rounded, out)
        left = left - rounded
    out_ref[...] = out.astype(jnp.bfloat16)


def mix_body(at_ref, routes_ref, filtered_ref, weight_ref, residual_ref, z_ref, out_ref, slot_ref):
    channels = filtered_ref.shape[0]
    tok_rows = z_ref.shape[0]
    experts, capacity, block = out_ref.shape
    expert = lax.broadcasted_iota(jnp.int32, (experts, tok_rows), 0)
    named = [expert == routes_ref[pick : pick + 1] for pick in range(2)]
    earlier = lax.broadcasted_iota(jnp.int32, (tok_rows, tok_rows), 0) < lax.broadcasted_iota(
        jnp.int32, (tok_rows, tok_rows), 1
    )
    rank = jnp.dot(
        jnp.where(named[0] | named[1], 1.0, 0.0).astype(jnp.bfloat16),
        jnp.where(earlier, 1.0, 0.0).astype(jnp.bfloat16),
        preferred_element_type=jnp.float32,
    )
    place = expert.astype(jnp.float32) * capacity + rank
    slots = [
        jnp.sum(jnp.where(who, place, 0.0), 0, keepdims=True).astype(jnp.int32) for who in named
    ]
    slot_ref[:1] = slots[0]
    slot_ref[1:2] = slots[1]

    filtered = filtered_ref[...].astype(jnp.float32)
    gain = jnp.sum(filtered[:, tok_rows : tok_rows + 3], 1, keepdims=True)
    filtered = filtered[:, :tok_rows]
    row_mean = jnp.sum(filtered, 0, keepdims=True) / channels
    row_var = jnp.sum(filtered * filtered, 0, keepdims=True) / channels - row_mean * row_mean
    normed = (filtered - row_mean) * lax.rsqrt(row_var + norm_eps) * gain
    conv_out = (normed / (1.0 + jnp.exp(-normed))).astype(jnp.bfloat16)
    mix = lax.dot_general(
        conv_out, weight_ref[...], (((0,), (0,)), ((), ())), preferred_element_type=jnp.float32
    )
    z = residual_alpha * residual_ref[...].astype(jnp.float32) + mix
    z_ref[...] = z
    slot = lax.broadcasted_iota(jnp.int32, (experts * capacity, tok_rows), 0)
    table = (slot == slots[0]) | (slot == slots[1])
    outgoing = jnp.dot(
        jnp.where(table, 1.0, 0.0).astype(jnp.bfloat16),
        z.astype(jnp.bfloat16),
        preferred_element_type=jnp.float32,
    )
    out_ref[...] = outgoing.astype(jnp.bfloat16).reshape(experts, capacity, block)


def down_body(at_ref, mine_ref, else_ref, mine_0, mine_1, else_0, else_1, out_ref, hidden_ref):
    block = out_ref.shape[2]

    @pl.when(pl.program_id(0) == 0)
    def _():
        hidden_ref[...] = jnp.concatenate([mine_ref[...], else_ref[...]], 0).T

    down = jnp.concatenate(
        [
            jnp.concatenate([mine_0[...], else_0[...]], 0),
            jnp.concatenate([mine_1[...], else_1[...]], 0),
        ],
        1,
    )
    part = jnp.dot(hidden_ref[...], down, preferred_element_type=jnp.float32).astype(jnp.bfloat16)
    out_ref[0] = part[:, :block]
    out_ref[1] = part[:, block:]


def whole(memory=None):
    return pl.BlockSpec(memory_space=memory or pltpu.VMEM)


def full(*shape):
    return pl.BlockSpec(shape, lambda *_: (0,) * len(shape))


def local(
    glu_value,
    glu_gate,
    doc_ids,
    conv_kernel,
    conv_gain,
    out_weight,
    residual,
    mix_gain,
    routes,
    route_weights,
    expert_gate,
    expert_up,
    expert_down,
    final_gain,
):
    f32, bf16 = jnp.float32, jnp.bfloat16
    n_sp, n_y, n_c = lax.axis_size("sp"), lax.axis_size("y"), lax.axis_size("c")
    n_tp = n_y * n_c
    at_core = lax.axis_index("c").astype(jnp.int32).reshape(1)
    at_tp = lax.axis_index(TP)
    tok_rows, own_ch = glu_value.shape
    features = residual.shape[1]
    feat_block = features // n_tp

    lanes, more = 256, 16
    own_rows, rim = pl.pallas_call(
        head_body,
        out_shape=(
            jax.ShapeDtypeStruct((own_ch + more, lanes), bf16),
            jax.ShapeDtypeStruct((own_ch + more, 128), bf16),
        ),
        in_specs=[whole()] * 3,
        out_specs=(whole(), whole()),
        name="head",
    )(glu_value.T, glu_gate.T, doc_ids[None])
    rim, own_rows, out_weight = lax.optimization_barrier((rim, own_rows, out_weight))
    rim = from_behind(rim, "sp", 1)
    taps = jnp.concatenate([conv_kernel.astype(f32), conv_gain[None]], 0).T
    filtered = pl.pallas_call(
        functools.partial(conv_body, lags=conv_kernel.shape[0], tok_rows=tok_rows),
        out_shape=jax.ShapeDtypeStruct((own_ch, lanes), bf16),
        in_specs=[whole()] * 3,
        out_specs=whole(),
        name="conv",
    )(own_rows, rim, taps)
    filtered = lax.all_gather(filtered, TP, axis=0, tiled=True)
    weight_parts = out_weight.reshape(own_ch, n_tp, feat_block).transpose(1, 0, 2)
    weight_own = lax.all_to_all(weight_parts, TP, 0, 0, tiled=True).reshape(-1, feat_block)
    experts = expert_gate.shape[0] * n_sp
    capacity = 4 * tok_rows // experts
    own_z, outgoing, slot_rows = pl.pallas_call(
        mix_body,
        out_shape=(
            jax.ShapeDtypeStruct((tok_rows, feat_block), f32),
            jax.ShapeDtypeStruct((experts, capacity, feat_block), bf16),
            jax.ShapeDtypeStruct((2, tok_rows), jnp.int32),
        ),
        grid_spec=pltpu.PrefetchScalarGridSpec(
            num_scalar_prefetch=1,
            grid=(1,),
            in_specs=[
                full(2, tok_rows),
                full(own_ch * n_tp, lanes),
                full(own_ch * n_tp, feat_block),
                pl.BlockSpec((tok_rows, feat_block), lambda i, at: (0, at[0])),
            ],
            out_specs=(
                full(tok_rows, feat_block),
                full(experts, capacity, feat_block),
                full(2, tok_rows),
            ),
        ),
        name="mix",
    )(at_tp.astype(jnp.int32).reshape(1), routes.T, filtered, weight_own, residual)
    arrived = lax.all_to_all(outgoing, "sp", 0, 0, tiled=True)
    rows = n_sp * capacity
    arrived = (arrived.reshape(rows, feat_block).T.astype(f32) * row_scale).astype(jnp.float16)
    gathered = lax.all_gather(arrived, TP, axis=0, tiled=True)

    wide = gathered.astype(f32)
    in_mean = jnp.sum(wide, 0) * (1.0 / (row_scale * features))
    in_square = jnp.sum(wide * wide, 0) * (1.0 / (row_scale * row_scale * features))
    in_rstd = lax.rsqrt(in_square - in_mean * in_mean + norm_eps)
    in_rows = (
        (wide * (1.0 / row_scale) - in_mean[None]) * in_rstd[None] * mix_gain[:, None]
    ).astype(bf16)
    gate_proj = jnp.einsum("kf,kr->fr", expert_gate[0], in_rows, preferred_element_type=f32)
    up_proj = jnp.einsum("kf,kr->fr", expert_up[0], in_rows, preferred_element_type=f32)
    hidden = (jax.nn.silu(gate_proj) * up_proj).astype(bf16)

    w_down = expert_down[0]
    units = w_down.shape[0]
    picks = [
        pl.BlockSpec((units, feat_block), lambda i, at, step=step: (0, 2 * (2 * i + step) + at[0]))
        for step in range(2)
    ]
    parts = pl.pallas_call(
        down_body,
        out_shape=jax.ShapeDtypeStruct((n_y, rows, feat_block), bf16),
        grid_spec=pltpu.PrefetchScalarGridSpec(
            num_scalar_prefetch=1,
            grid=(n_y // 2,),
            in_specs=[full(units, rows), full(units, rows), *picks, *picks],
            out_specs=pl.BlockSpec((2, rows, feat_block), lambda i, at: (i, 0, 0)),
            scratch_shapes=[pltpu.VMEM((rows, n_c * units), bf16)],
        ),
        name="down",
    )(at_core, hidden, swap(hidden, "c"), w_down, w_down, *([swap(w_down, "c")] * 2))
    parts = lax.all_to_all(parts, "y", 0, 0, tiled=True)
    summed = jnp.sum(parts.astype(f32), 0).astype(bf16).reshape(n_sp, capacity, feat_block)
    expert_out = lax.all_to_all(summed, "sp", 0, 0, tiled=True).reshape(rows, feat_block)
    slots = jnp.arange(experts * capacity, dtype=jnp.int32)
    first = (slot_rows[0][:, None] == slots[None, :]).astype(bf16)
    second = (slot_rows[1][:, None] == slots[None, :]).astype(bf16)
    moe_sum = route_weights[:, :1] * jnp.dot(
        first, expert_out, preferred_element_type=f32
    ) + route_weights[:, 1:] * jnp.dot(second, expert_out, preferred_element_type=f32)

    own_gain = lax.dynamic_slice_in_dim(mix_gain, at_tp * feat_block, feat_block, 0)[None]
    z_gain = own_z * own_gain
    sums = jnp.stack(
        [
            jnp.sum(own_z, 1),
            jnp.sum(own_z * own_z, 1),
            jnp.sum(z_gain, 1),
            jnp.sum(z_gain * z_gain, 1),
            jnp.sum(z_gain * own_gain, 1),
            jnp.sum(z_gain * moe_sum, 1),
            jnp.sum(own_gain * moe_sum, 1),
            jnp.sum(moe_sum, 1),
            jnp.sum(moe_sum * moe_sum, 1),
            jnp.zeros_like(moe_sum[:, 0]),
        ]
    )
    sums = summed_over(sums.reshape(-1, 128), TP, n_tp).reshape(10, tok_rows)
    z_mean = sums[0] / features
    z_rstd = lax.rsqrt(sums[1] / features - z_mean * z_mean + norm_eps)
    ar = residual_alpha * z_rstd
    fin_sum = ar * (sums[2] - z_mean * jnp.sum(mix_gain)) + sums[7]
    fin_square = (
        ar * ar * (sums[3] - 2.0 * z_mean * sums[4] + z_mean * z_mean * jnp.sum(mix_gain * mix_gain))
        + 2.0 * ar * (sums[5] - z_mean * sums[6])
        + sums[8]
    )
    fin_mean = fin_sum / features
    fin_rstd = lax.rsqrt(fin_square / features - fin_mean * fin_mean + norm_eps)
    pre_norm = ar[:, None] * (own_z - z_mean[:, None]) * own_gain + moe_sum
    return ((pre_norm - fin_mean[:, None]) * fin_rstd[:, None] * final_gain).astype(bf16)


def solution(mesh):
    finer = Mesh(mesh.devices.reshape(mesh.shape["sp"], 8, 2), ("sp", "y", "c"))
    placed = (
        P("sp", TP),
        P("sp", TP),
        P("sp"),
        P(None, TP),
        P(TP),
        P(TP, None),
        P("sp", None),
        P(),
        P("sp", None),
        P("sp", None),
        P("sp", None, TP),
        P("sp", None, TP),
        P("sp", TP, None),
        P(TP),
    )
    return jax.shard_map(local, mesh=finer, in_specs=placed, out_specs=P("sp", TP), check_vma=False)
```

time: 186 us -> 190 us (1.022)
  waiting for transfers between devices: 59.5 us -> 68.7 us
  local copies, waits for them, and re-layouts: 10.8 us -> 6.35 us
  other arithmetic: 6.8 us -> 4.71 us
  Pallas kernels: 10 us -> 12 us
    all_to_all x1 -> x2, waiting for transfers between devices: 41.5 us -> 50.8 us  [the longest x1 40.4 us: local(): parts = lax.all_to_all(parts, 'y', 0, 0, tiled=True)]
    ppermute x1, starting transfers between devices: 3.93 us -> 1.55 us  [from_behind(): return lax.ppermute(value, axis, pairs)]
    all_to_all x1 -> x2, starting transfers between devices: 11.2 us -> 8.98 us  [the longest x1 5.11 us: local(): parts = lax.all_to_all(parts, 'y', 0, 0, tiled=True)]
    all_to_all x1, starting transfers between devices: 8.07 us -> 10.2 us  [local(): lax.all_to_all(weight_parts, TP, 0, 0, tiled=True).reshape(-1, feat_block)]
    pallas_call x2 -> x3, Pallas kernels: 7.08 us -> 9.02 us  [the longest x1 5.25 us: local(): pl.pallas_call(down_body, out_shape=jax.ShapeDtypeStruct((n_y, rows, feat...]
  transfers between devices with their start and end apart: 7 -> 8, of which waited for: 4 -> 5; matrix products, arithmetic and copies ran while one was open for 8% -> 4% of each run, Pallas kernels for 1% -> 1%
where the time goes in v4:
time: 190 us; the launch traced here: 189 us
  waiting for transfers between devices  68.7 us (36%)
  blocking collectives  47.4 us (25%)
  starting transfers between devices  44.7 us (24%)
  Pallas kernels  12 us (6%)
  local copies, waits for them, and re-layouts  6.35 us (3%)
  other arithmetic  4.71 us (2%)
  matrix products  4.14 us (2%)
    all_to_all x1, waiting for transfers between devices, local(): parts = lax.all_to_all(parts, 'y', 0, 0, tiled=True)  40.4 us
    all_gather x1, blocking collectives, local(): gathered = lax.all_gather(arrived, TP, axis=0, tiled=True)  26.9 us
    all_gather x1, blocking collectives, local(): filtered = lax.all_gather(filtered, TP, axis=0, tiled=True)  20.5 us
    all_to_all x1, starting transfers between devices, local(): arrived = lax.all_to_all(outgoing, 'sp', 0, 0, tiled=True)  14 us
    all_to_all x1, waiting for transfers between devices, local(): lax.all_to_all(summed, 'sp', 0, 0, tiled=True).reshape(rows, feat_block)  10.4 us
    all_to_all x1, starting transfers between devices, local(): lax.all_to_all(weight_parts, TP, 0, 0, tiled=True).reshape(-1, feat_block)  10.2 us
    all_to_all x1, waiting for transfers between devices, local(): arrived = lax.all_to_all(outgoing, 'sp', 0, 0, tiled=True)  8.26 us
    all_to_all x1, waiting for transfers between devices, summed_over(): return jnp.sum(lax.all_to_all(copies, axis, 0, 0, tiled=True), axis=0)  8.02 us
  transfers between devices with their start and end apart: 8, of which 5 were waited for; matrix products, arithmetic and copies ran while one was open for 4% of the time, Pallas kernels for 1%

profile of v4, /device:TPU:1, one launch (start us, length us, event | category | flops | bytes accessed | tf_op | source)
XLA Modules:
  0.0 188.8 jit_solution(15519695619779748845)
XLA Ops:
  0.0 1.6 head.1
  1.6 1.7 bitcast_bitcast_fusion
  3.4 10.2 %all-to-all-start = ((bf16[16,64,128]{2,1,0:T(8,128)(2,1)}), bf16[16,64,128]{2,1,0:T(8,128)(2,1)S(1)}, u32[]{:S(2)}, u32[]{:S(2)}) async-start(bf16[16,64,128]{2,1,0:T(8,128)(2,1)} %bitcast_bitcast_fusion), calls=%async_computation | async-start | bytes 524288 | tf_op jit(solution)/shard_map/all_to_all | solution.py:188
  13.5 1.6 collective-permute-start
  15.1 0.8 copy.25
  15.9 0.7 copy.26
  16.6 0.7 maximum_bitcast_fusion.taps_ref
  17.9 2.1 %conv.1 = bf16[64,256]{1,0:T(8,128)(2,1)} custom-call(bf16[80,256]{1,0:T(8,128)(2,1)} %get-tuple-element.15.own_ref, bf16[80,128]{1,0:T(8,128)(2,1)} %copy-done.6, f32[64,32]{1,0:T(8,128)} %maximum_bitcast_fusion.taps_ref), custom_call_target="tpu_custom_call" | custom-call | tf_op jit(solution)/shard_map/conv/pallas_call | solution.py:179
  20.0 20.5 %all_gather.6.filtered_ref = bf16[1024,256]{1,0:T(8,128)(2,1)} all-gather(bf16[64,256]{1,0:T(8,128)(2,1)} %conv.1), channel_id=1, replica_groups=mesh['sp'=32,'y'=8,'c'=2] {'y','c'}, dimensions={0}, use_global_device_ids=true | all-gather | bytes 557056 | tf_op jit(solution)/shard_map/all_gather | solution.py:186
  40.6 0.7 copy-done.2
  41.3 3.0 %mix.1 = (f32[192,128]{1,0:T(8,128)}, bf16[32,24,128]{2,1,0:T(8,128)(2,1)}, s32[2,192]{1,0:T(2,128)}) custom-call(s32[1]{0:T(128)} %bitcast.at_ref, s32[2,192]{1,0:T(2,128)} %bitcast.80, bf16[1024,256]{1,0:T(8,128)(2,1)} %all_gather.6.filtered_ref, bf16[1024,128]{1,0:T(8,128)(2,1)} %bitcast.65, bf16[192,2048]{1,0:T(8,128)(2,1)} %residual_ref.1), custom_call_target="tpu_custom_call" | custom-call | tf_op jit(solution)/shard_map/mix/pallas_call | solution.py:191
  44.2 14.0 %all-to-all-start.1 = ((bf16[32,24,128]{2,1,0:T(8,128)(2,1)}), bf16[32,24,128]{2,1,0:T(8,128)(2,1)S(1)}, u32[]{:S(2)}, u32[]{:S(2)}) async-start(bf16[32,24,128]{2,1,0:T(8,128)(2,1)} %get-tuple-element.20), calls=%async_computation.1 | async-start | bytes 393216 | tf_op jit(solution)/shard_map/all_to_all | solution.py:215
  58.2 2.4 %collective-permute-start.2 = (bf16[320,2048]{1,0:T(8,128)(2,1)S(1)}, bf16[320,2048]{1,0:T(8,128)(2,1)}, u32[]{:S(2)}, u32[]{:S(2)}) collective-permute-start(bf16[320,2048]{1,0:T(8,128)(2,1)S(1)} %bitcast.64), channel_id=1, source_target_pairs={{0,1},{1,0},{2,3},{3,2},{4,5},{5,4},{6,7},{7,6},{8,9},{9,8},{10,11... | collective-permute-start | bytes 3932168 | tf_op jit(solution)/shard_map/ppermute | solution.py:25
  60.6 8.3 %all-to-all-done.1 = bf16[32,24,128]{2,1,0:T(8,128)(2,1)S(1)} async-done(((bf16[32,24,128]{2,1,0:T(8,128)(2,1)}), bf16[32,24,128]{2,1,0:T(8,128)(2,1)S(1)}, u32[]{:S(2)}, u32[]{:S(2)}) %all-to-all-start.1) | async-done | bytes 196640 | tf_op jit(solution)/shard_map/all_to_all | solution.py:215
  68.9 26.9 %all-gather.1 = f16[2048,768]{0,1:T(8,128)(2,1)S(1)} all-gather(f16[128,768]{0,1:T(8,128)(2,1)S(1)} %bitcast.66), channel_id=1, replica_groups=mesh['sp'=32,'y'=8,'c'=2] {'y','c'}, dimensions={0}, use_global_device_ids=true | all-gather | bytes 3342336 | tf_op jit(solution)/shard_map/all_gather | solution.py:218
  95.8 1.0 convert_reduce_fusion
  96.8 1.6 convolution_bitcast_fusion.1
  98.4 1.7 fusion.8.mine_ref
  100.2 2.0 %collective-permute-start.1 = (bf16[320,768]{1,0:T(8,128)(2,1)S(1)}, bf16[320,768]{1,0:T(8,128)(2,1)S(1)}, u32[]{:S(2)}, u32[]{:S(2)}) collective-permute-start(bf16[320,768]{1,0:T(8,128)(2,1)S(1)} %fusion.8.mine_ref), channel_id=1, source_target_pairs={{0,1},{1,0},{2,3},{3,2},{4,5},{5,4},{6,7},{7,6},{8,9},{9,8},{10,11... | collective-permute-start | bytes 1474568 | tf_op jit(solution)/shard_map/ppermute | solution.py:25
  102.2 1.7 collective-permute-done.1.else_ref
  103.9 0.8 copy-done.4
  104.7 5.3 %down.1 = bf16[8,768,128]{2,1,0:T(8,128)(2,1)} custom-call(s32[1]{0:T(128)} %bitcast.16.at_ref, bf16[320,768]{1,0:T(8,128)(2,1)} %copy-done.3, bf16[320,768]{1,0:T(8,128)(2,1)} %copy-done.4, bf16[320,2048]{1,0:T(8,128)(2,1)} %bitcast.62, bf16[320,2048]{1,0:T(8,128)(2,1)} %bitcast.63, bf16[320,2048]{1,0:T(8,128)(2,1)} %collective-permute-done.2.else_0.else_1, ...), custom_call_target="tpu_custom_call" | custom-call | tf_op jit(solution)/shard_map/down/pallas_call | solution.py:237
  110.0 5.1 %all-to-all-start.2 = ((bf16[8,768,128]{2,1,0:T(8,128)(2,1)}), bf16[8,768,128]{2,1,0:T(8,128)(2,1)S(1)}, u32[]{:S(2)}, u32[]{:S(2)}) async-start(bf16[8,768,128]{2,1,0:T(8,128)(2,1)} %down.1), calls=%async_computation.2 | async-start | bytes 3145728 | tf_op jit(solution)/shard_map/all_to_all | solution.py:249
  115.2 40.4 %all-to-all-done.2 = bf16[8,768,128]{2,1,0:T(8,128)(2,1)S(1)} async-done(((bf16[8,768,128]{2,1,0:T(8,128)(2,1)}), bf16[8,768,128]{2,1,0:T(8,128)(2,1)S(1)}, u32[]{:S(2)}, u32[]{:S(2)}) %all-to-all-start.2) | async-done | bytes 1572896 | tf_op jit(solution)/shard_map/all_to_all | solution.py:249
  155.6 0.9 reduce_sum.145
  156.5 3.9 %all-to-all-start.3 = ((bf16[32,24,128]{2,1,0:T(8,128)(2,1)}), bf16[32,24,128]{2,1,0:T(8,128)(2,1)S(1)}, u32[]{:S(2)}, u32[]{:S(2)}) async-start(bf16[32,24,128]{2,1,0:T(8,128)(2,1)} %bitcast.24), calls=%async_computation.3 | async-start | bytes 393216 | tf_op jit(solution)/shard_map/all_to_all | solution.py:251
  160.4 10.4 %all-to-all-done.3 = bf16[32,24,128]{2,1,0:T(8,128)(2,1)S(1)} async-done(((bf16[32,24,128]{2,1,0:T(8,128)(2,1)}), bf16[32,24,128]{2,1,0:T(8,128)(2,1)S(1)}, u32[]{:S(2)}, u32[]{:S(2)}) %all-to-all-start.3) | async-done | bytes 196640 | tf_op jit(solution)/shard_map/all_to_all | solution.py:251
  171.8 0.7 broadcast_in_dim.11
  172.4 5.6 %all-to-all-start.4 = ((f32[16,15,128]{2,1,0:T(8,128)}), f32[16,15,128]{2,1,0:T(8,128)S(1)}, u32[]{:S(2)}, u32[]{:S(2)}) async-start(f32[16,15,128]{2,1,0:T(8,128)} %broadcast_in_dim.11), calls=%async_computation.4 | async-start | bytes 262144 | tf_op jit(solution)/shard_map/all_to_all | solution.py:30
  179.2 8.0 %all-to-all-done.4 = f32[16,15,128]{2,1,0:T(8,128)S(1)} async-done(((f32[16,15,128]{2,1,0:T(8,128)}), f32[16,15,128]{2,1,0:T(8,128)S(1)}, u32[]{:S(2)}, u32[]{:S(2)}) %all-to-all-start.4) | async-done | bytes 122912 | tf_op jit(solution)/shard_map/all_to_all | solution.py:30
  187.4 0.7 add_rsqrt_fusion.1
  188.0 0.8 multiply_convert_fusion.1
  (39 shorter events, 2.5 us)
Async XLA Ops:
  0.0 96.8 %copy-start = (bf16[1,2048,320]{1,2,0:T(8,128)(2,1)S(1)}, bf16[1,2048,320]{1,2,0:T(8,128)(2,1)}, u32[]{:S(2)}) copy-start(bf16[1,2048,320]{1,2,0:T(8,128)(2,1)} %param.24) | copy-start | bytes 3932164
  0.0 58.2 %copy-start.1 = (bf16[1,320,2048]{2,1,0:T(8,128)(2,1)S(1)}, bf16[1,320,2048]{2,1,0:T(8,128)(2,1)}, u32[]{:S(2)}) copy-start(bf16[1,320,2048]{2,1,0:T(8,128)(2,1)} %param.26) | copy-start | bytes 3932164
  3.4 37.2 %all-to-all-start = ((bf16[16,64,128]{2,1,0:T(8,128)(2,1)}), bf16[16,64,128]{2,1,0:T(8,128)(2,1)S(1)}, u32[]{:S(2)}, u32[]{:S(2)}) async-start(bf16[16,64,128]{2,1,0:T(8,128)(2,1)} %bitcast_bitcast_fusion), calls=%async_computation | async-start | bytes 524288 | tf_op jit(solution)/shard_map/all_to_all | solution.py:188
  13.5 3.8 %collective-permute-start = (bf16[80,128]{1,0:T(8,128)(2,1)}, bf16[80,128]{1,0:T(8,128)(2,1)S(1)}, u32[]{:S(2)}, u32[]{:S(2)}) collective-permute-start(bf16[80,128]{1,0:T(8,128)(2,1)} %get-tuple-element.16), channel_id=1, source_target_pairs={{0,16},{16,32},{32,48},{48,64},{64,80},{80,96},{96,112},{112,128},... | collective-permute-start | bytes 61448 | tf_op jit(solution)/shard_map/ppermute | solution.py:21
  17.3 0.6 copy-start.6
  40.6 0.7 copy-start.2
  44.2 24.6 %all-to-all-start.1 = ((bf16[32,24,128]{2,1,0:T(8,128)(2,1)}), bf16[32,24,128]{2,1,0:T(8,128)(2,1)S(1)}, u32[]{:S(2)}, u32[]{:S(2)}) async-start(bf16[32,24,128]{2,1,0:T(8,128)(2,1)} %get-tuple-element.20), calls=%async_computation.1 | async-start | bytes 393216 | tf_op jit(solution)/shard_map/all_to_all | solution.py:215
  58.2 44.0 %collective-permute-start.2 = (bf16[320,2048]{1,0:T(8,128)(2,1)S(1)}, bf16[320,2048]{1,0:T(8,128)(2,1)}, u32[]{:S(2)}, u32[]{:S(2)}) collective-permute-start(bf16[320,2048]{1,0:T(8,128)(2,1)S(1)} %bitcast.64), channel_id=1, source_target_pairs={{0,1},{1,0},{2,3},{3,2},{4,5},{5,4},{6,7},{7,6},{8,9},{9,8},{10,11... | collective-permute-start | bytes 3932168 | tf_op jit(solution)/shard_map/ppermute | solution.py:25
  68.9 27.9 %copy-start.7 = (f32[2048]{0:T(1024)S(1)}, f32[2048]{0:T(1024)}, u32[]{:S(2)}) copy-start(f32[2048]{0:T(1024)} %param.21) | copy-start | bytes 24580
  96.8 1.6 copy-start.11
  100.2 4.6 %copy-start.3 = (bf16[320,768]{1,0:T(8,128)(2,1)}, bf16[320,768]{1,0:T(8,128)(2,1)S(1)}, u32[]{:S(2)}) copy-start(bf16[320,768]{1,0:T(8,128)(2,1)S(1)} %fusion.8.mine_ref) | copy-start | bytes 1474564
  100.2 3.8 %collective-permute-start.1 = (bf16[320,768]{1,0:T(8,128)(2,1)S(1)}, bf16[320,768]{1,0:T(8,128)(2,1)S(1)}, u32[]{:S(2)}, u32[]{:S(2)}) collective-permute-start(bf16[320,768]{1,0:T(8,128)(2,1)S(1)} %fusion.8.mine_ref), channel_id=1, source_target_pairs={{0,1},{1,0},{2,3},{3,2},{4,5},{5,4},{6,7},{7,6},{8,9},{9,8},{10,11... | collective-permute-start | bytes 1474568 | tf_op jit(solution)/shard_map/ppermute | solution.py:25
  103.9 0.8 copy-start.4
  110.0 50.4 %copy-start.8 = (f32[192,2]{0,1:T(2,128)S(1)}, f32[192,2]{0,1:T(2,128)}, u32[]{:S(2)}) copy-start(f32[192,2]{0,1:T(2,128)} %param.23) | copy-start | bytes 4612
  110.0 50.4 %copy-start.9 = (s32[2,192]{1,0:T(2,128)S(1)}, s32[2,192]{1,0:T(2,128)}, u32[]{:S(2)}) copy-start(s32[2,192]{1,0:T(2,128)} %get-tuple-element.19) | copy-start | bytes 4612
  110.0 61.1 %copy-start.5 = (f32[192,128]{1,0:T(8,128)S(1)}, f32[192,128]{1,0:T(8,128)}, u32[]{:S(2)}) copy-start(f32[192,128]{1,0:T(8,128)} %get-tuple-element.18) | copy-start | bytes 294916
  110.0 78.0 %copy-start.10 = (f32[128]{0:T(128)S(1)}, f32[128]{0:T(128)}, u32[]{:S(2)}) copy-start(f32[128]{0:T(128)} %param.27) | copy-start | bytes 1540
  110.0 45.6 %all-to-all-start.2 = ((bf16[8,768,128]{2,1,0:T(8,128)(2,1)}), bf16[8,768,128]{2,1,0:T(8,128)(2,1)S(1)}, u32[]{:S(2)}, u32[]{:S(2)}) async-start(bf16[8,768,128]{2,1,0:T(8,128)(2,1)} %down.1), calls=%async_computation.2 | async-start | bytes 3145728 | tf_op jit(solution)/shard_map/all_to_all | solution.py:249
  156.5 14.3 %all-to-all-start.3 = ((bf16[32,24,128]{2,1,0:T(8,128)(2,1)}), bf16[32,24,128]{2,1,0:T(8,128)(2,1)S(1)}, u32[]{:S(2)}, u32[]{:S(2)}) async-start(bf16[32,24,128]{2,1,0:T(8,128)(2,1)} %bitcast.24), calls=%async_computation.3 | async-start | bytes 393216 | tf_op jit(solution)/shard_map/all_to_all | solution.py:251
  172.4 14.8 %all-to-all-start.4 = ((f32[16,15,128]{2,1,0:T(8,128)}), f32[16,15,128]{2,1,0:T(8,128)S(1)}, u32[]{:S(2)}, u32[]{:S(2)}) async-start(f32[16,15,128]{2,1,0:T(8,128)} %broadcast_in_dim.11), calls=%async_computation.4 | async-start | bytes 262144 | tf_op jit(solution)/shard_map/all_to_all | solution.py:30

commit v5 on v4

--- a/solution.py
+++ b/solution.py
@@ -7,6 +7,7 @@
 from jax.experimental.pallas import tpu as pltpu
 from jax.sharding import Mesh
 from jax.sharding import PartitionSpec as P
+
 
 TP = ("y", "c")
 
@@ -43,7 +44,7 @@
     rim_ref[...] = shifted[:, :128].astype(jnp.bfloat16)
 
 
-def conv_body(own_ref, rim_ref, taps_ref, out_ref, *, lags, tok_rows):
+def conv_body(own_ref, rim_ref, kernel_ref, gain_ref, out_ref, *, lags, tok_rows):
     own_ch = out_ref.shape[0]
     own = own_ref[...].astype(jnp.float32)
     rim = rim_ref[...].astype(jnp.float32)
@@ -51,7 +52,7 @@
     behind = jnp.where(lane < tok_rows - 128, own[:, 128:], rim)
     packed = jnp.concatenate([own[:, :128], behind], 1)
     rows, ids = packed[:own_ch], packed[own_ch : own_ch + 8]
-    taps = taps_ref[...]
+    taps = jnp.concatenate([kernel_ref[...].astype(jnp.float32), gain_ref[...]], 0).T
     total = jnp.zeros_like(rows)
     for lag in range(lags):
         moved = rows if lag == 0 else pltpu.roll(rows, lag, 1)
@@ -110,23 +111,21 @@
     out_ref[...] = outgoing.astype(jnp.bfloat16).reshape(experts, capacity, block)
 
 
-def down_body(at_ref, mine_ref, else_ref, mine_0, mine_1, else_0, else_1, out_ref, hidden_ref):
-    block = out_ref.shape[2]
-
-    @pl.when(pl.program_id(0) == 0)
-    def _():
-        hidden_ref[...] = jnp.concatenate([mine_ref[...], else_ref[...]], 0).T
-
-    down = jnp.concatenate(
-        [
-            jnp.concatenate([mine_0[...], else_0[...]], 0),
-            jnp.concatenate([mine_1[...], else_1[...]], 0),
-        ],
-        1,
-    )
-    part = jnp.dot(hidden_ref[...], down, preferred_element_type=jnp.float32).astype(jnp.bfloat16)
-    out_ref[0] = part[:, :block]
-    out_ref[1] = part[:, block:]
+def down_body(at_ref, mine_ref, else_ref, mine_0, mine_1, else_0, else_1, out_ref):
+    units, block = mine_0.shape
+    n_sp, _, capacity, _ = out_ref.shape
+    part = jnp.dot(
+        mine_ref[:, :units],
+        jnp.concatenate([mine_0[...], mine_1[...]], 1),
+        preferred_element_type=jnp.float32,
+    ) + jnp.dot(
+        else_ref[:, :units],
+        jnp.concatenate([else_0[...], else_1[...]], 1),
+        preferred_element_type=jnp.float32,
+    )
+    part = part.astype(jnp.bfloat16)
+    out_ref[:, 0] = part[:, :block].reshape(n_sp, capacity, block)
+    out_ref[:, 1] = part[:, block:].reshape(n_sp, capacity, block)
 
 
 def whole(memory=None):
@@ -175,17 +174,17 @@
     )(glu_value.T, glu_gate.T, doc_ids[None])
     rim, own_rows, out_weight = lax.optimization_barrier((rim, own_rows, out_weight))
     rim = from_behind(rim, "sp", 1)
-    taps = jnp.concatenate([conv_kernel.astype(f32), conv_gain[None]], 0).T
     filtered = pl.pallas_call(
         functools.partial(conv_body, lags=conv_kernel.shape[0], tok_rows=tok_rows),
         out_shape=jax.ShapeDtypeStruct((own_ch, lanes), bf16),
-        in_specs=[whole()] * 3,
+        in_specs=[whole()] * 4,
         out_specs=whole(),
         name="conv",
-    )(own_rows, rim, taps)
+    )(own_rows, rim, conv_kernel, conv_gain[None])
     filtered = lax.all_gather(filtered, TP, axis=0, tiled=True)
     weight_parts = out_weight.reshape(own_ch, n_tp, feat_block).transpose(1, 0, 2)
-    weight_own = lax.all_to_all(weight_parts, TP, 0, 0, tiled=True).reshape(-1, feat_block)
+    weight_own = lax.all_to_all(weight_parts, TP, 0, 0, tiled=True)
+    weight_own = weight_own.reshape(-1, feat_block)
     experts = expert_gate.shape[0] * n_sp
     capacity = 4 * tok_rows // experts
     own_z, outgoing, slot_rows = pl.pallas_call(
@@ -224,9 +223,11 @@
     in_rows = (
         (wide * (1.0 / row_scale) - in_mean[None]) * in_rstd[None] * mix_gain[:, None]
     ).astype(bf16)
-    gate_proj = jnp.einsum("kf,kr->fr", expert_gate[0], in_rows, preferred_element_type=f32)
-    up_proj = jnp.einsum("kf,kr->fr", expert_up[0], in_rows, preferred_element_type=f32)
+    gate_proj = jnp.einsum("kr,kf->rf", in_rows, expert_gate[0], preferred_element_type=f32)
+    up_proj = jnp.einsum("kr,kf->rf", in_rows, expert_up[0], preferred_element_type=f32)
     hidden = (jax.nn.silu(gate_proj) * up_proj).astype(bf16)
+    wide_units = -(-hidden.shape[1] // 128) * 128
+    hidden = jnp.pad(hidden, ((0, 0), (0, wide_units - hidden.shape[1])))
 
     w_down = expert_down[0]
     units = w_down.shape[0]
@@ -236,19 +237,19 @@
     ]
     parts = pl.pallas_call(
         down_body,
-        out_shape=jax.ShapeDtypeStruct((n_y, rows, feat_block), bf16),
+        out_shape=jax.ShapeDtypeStruct((n_sp, n_y, capacity, feat_block), bf16),
         grid_spec=pltpu.PrefetchScalarGridSpec(
             num_scalar_prefetch=1,
             grid=(n_y // 2,),
-            in_specs=[full(units, rows), full(units, rows), *picks, *picks],
-            out_specs=pl.BlockSpec((2, rows, feat_block), lambda i, at: (i, 0, 0)),
-            scratch_shapes=[pltpu.VMEM((rows, n_c * units), bf16)],
+            in_specs=[full(rows, wide_units), full(rows, wide_units), *picks, *picks],
+            out_specs=pl.BlockSpec((n_sp, 2, capacity, feat_block), lambda i, at: (0, i, 0, 0)),
         ),
         name="down",
     )(at_core, hidden, swap(hidden, "c"), w_down, w_down, *([swap(w_down, "c")] * 2))
-    parts = lax.all_to_all(parts, "y", 0, 0, tiled=True)
-    summed = jnp.sum(parts.astype(f32), 0).astype(bf16).reshape(n_sp, capacity, feat_block)
-    expert_out = lax.all_to_all(summed, "sp", 0, 0, tiled=True).reshape(rows, feat_block)
+    parts = parts.reshape(n_sp * n_y, capacity, feat_block)
+    returned = lax.all_to_all(parts, ("sp", "y"), 0, 0, tiled=True)
+    returned = returned.reshape(experts, n_y, capacity, feat_block)
+    expert_out = jnp.sum(returned.astype(f32), 1).astype(bf16).reshape(rows, feat_block)
     slots = jnp.arange(experts * capacity, dtype=jnp.int32)
     first = (slot_rows[0][:, None] == slots[None, :]).astype(bf16)
     second = (slot_rows[1][:, None] == slots[None, :]).astype(bf16)
@@ -306,4 +307,6 @@
         P("sp", TP, None),
         P(TP),
     )
-    return jax.shard_map(local, mesh=finer, in_specs=placed, out_specs=P("sp", TP), check_vma=False)
+    return jax.shard_map(
+        local, mesh=finer, in_specs=placed, out_specs=P("sp", TP), check_vma=False
+    )

time: 190 us -> 183 us (0.963)
  waiting for transfers between devices: 68.7 us -> 60.7 us
  starting transfers between devices: 44.7 us -> 47.7 us
    all_to_all x3 -> x2, waiting for transfers between devices: 50.8 us -> 41.5 us  [the longest x1 41.5 us: local(): returned = lax.all_to_all(parts, ('sp', 'y'), 0, 0, tiled=True)]
    all_to_all x3 -> x2, starting transfers between devices: 19.1 us -> 21.4 us  [the longest x1 11.2 us: local(): returned = lax.all_to_all(parts, ('sp', 'y'), 0, 0, tiled=True)]
  transfers between devices with their start and end apart: 8 -> 7, of which waited for: 5 -> 5; matrix products, arithmetic and copies ran while one was open for 4% -> 3% of each run, Pallas kernels for 1% -> 1%
where the time goes in v5:
time: 183 us; the launch traced here: 182 us
  waiting for transfers between devices  60.7 us (33%)
  blocking collectives  48 us (26%)
  starting transfers between devices  47.7 us (26%)
  Pallas kernels  12 us (7%)
  local copies, waits for them, and re-layouts  4.88 us (3%)
  matrix products  4.78 us (3%)
  other arithmetic  3.35 us (2%)
    all_to_all x1, waiting for transfers between devices, local(): returned = lax.all_to_all(parts, ('sp', 'y'), 0, 0, tiled=True)  41.5 us
    all_gather x1, blocking collectives, local(): gathered = lax.all_gather(arrived, TP, axis=0, tiled=True)  26.9 us
    all_gather x1, blocking collectives, local(): filtered = lax.all_gather(filtered, TP, axis=0, tiled=True)  21.1 us
    all_to_all x1, starting transfers between devices, local(): arrived = lax.all_to_all(outgoing, 'sp', 0, 0, tiled=True)  14.5 us
    all_to_all x1, starting transfers between devices, local(): returned = lax.all_to_all(parts, ('sp', 'y'), 0, 0, tiled=True)  11.2 us
    all_to_all x1, starting transfers between devices, local(): weight_own = lax.all_to_all(weight_parts, TP, 0, 0, tiled=True)  10.2 us
    all_to_all x1, waiting for transfers between devices, local(): arrived = lax.all_to_all(outgoing, 'sp', 0, 0, tiled=True)  8.26 us
    all_to_all x1, waiting for transfers between devices, summed_over(): return jnp.sum(lax.all_to_all(copies, axis, 0, 0, tiled=True), axis=0)  8.02 us
  transfers between devices with their start and end apart: 7, of which 5 were waited for; matrix products, arithmetic and copies ran while one was open for 3% of the time, Pallas kernels for 1%

profile of v5, /device:TPU:1, one launch (start us, length us, event | category | flops | bytes accessed | tf_op | source)
XLA Modules:
  0.0 182.2 jit_solution(5948393494733942807)
XLA Ops:
  0.0 1.6 head.1
  1.6 1.7 bitcast_bitcast_fusion
  3.4 10.2 %all-to-all-start = ((bf16[16,64,128]{2,1,0:T(8,128)(2,1)}), bf16[16,64,128]{2,1,0:T(8,128)(2,1)S(1)}, u32[]{:S(2)}, u32[]{:S(2)}) async-start(bf16[16,64,128]{2,1,0:T(8,128)(2,1)} %bitcast_bitcast_fusion), calls=%async_computation | async-start | bytes 524288 | tf_op jit(solution)/shard_map/all_to_all | solution.py:186
  13.5 1.6 collective-permute-start
  15.1 1.1 collective-permute-done.rim_ref
  16.2 0.6 copy-done.6
  16.8 2.2 %conv.1 = bf16[64,256]{1,0:T(8,128)(2,1)} custom-call(bf16[80,256]{1,0:T(8,128)(2,1)} %get-tuple-element.15.own_ref, bf16[80,128]{1,0:T(8,128)(2,1)} %copy-done.6, bf16[31,64]{1,0:T(8,128)(2,1)} %kernel_ref.1, f32[1,64]{1,0:T(1,128)} %bitcast.86), custom_call_target="tpu_custom_call" | custom-call | tf_op jit(solution)/shard_map/conv/pallas_call | solution.py:177
  19.0 21.1 %all_gather.6.filtered_ref = bf16[1024,256]{1,0:T(8,128)(2,1)} all-gather(bf16[64,256]{1,0:T(8,128)(2,1)} %conv.1), channel_id=1, replica_groups=mesh['sp'=32,'y'=8,'c'=2] {'y','c'}, dimensions={0}, use_global_device_ids=true | all-gather | bytes 557056 | tf_op jit(solution)/shard_map/all_gather | solution.py:184
  40.1 0.7 copy-done.3
  40.8 3.0 %mix.1 = (f32[192,128]{1,0:T(8,128)}, bf16[32,24,128]{2,1,0:T(8,128)(2,1)}, s32[2,192]{1,0:T(2,128)}) custom-call(s32[1]{0:T(128)} %bitcast.at_ref, s32[2,192]{1,0:T(2,128)} %bitcast.71, bf16[1024,256]{1,0:T(8,128)(2,1)} %all_gather.6.filtered_ref, bf16[1024,128]{1,0:T(8,128)(2,1)} %bitcast.56, bf16[192,2048]{1,0:T(8,128)(2,1)} %residual_ref.1), custom_call_target="tpu_custom_call" | custom-call | tf_op jit(solution)/shard_map/mix/pallas_call | solution.py:190
  43.8 14.5 %all-to-all-start.1 = ((bf16[32,24,128]{2,1,0:T(8,128)(2,1)}), bf16[32,24,128]{2,1,0:T(8,128)(2,1)S(1)}, u32[]{:S(2)}, u32[]{:S(2)}) async-start(bf16[32,24,128]{2,1,0:T(8,128)(2,1)} %get-tuple-element.20), calls=%async_computation.1 | async-start | bytes 393216 | tf_op jit(solution)/shard_map/all_to_all | solution.py:214
  58.3 2.4 %collective-permute-start.2 = (bf16[320,2048]{1,0:T(8,128)(2,1)S(1)}, bf16[320,2048]{1,0:T(8,128)(2,1)}, u32[]{:S(2)}, u32[]{:S(2)}) collective-permute-start(bf16[320,2048]{1,0:T(8,128)(2,1)S(1)} %bitcast.55), channel_id=1, source_target_pairs={{0,1},{1,0},{2,3},{3,2},{4,5},{5,4},{6,7},{7,6},{8,9},{9,8},{10,11... | collective-permute-start | bytes 3932168 | tf_op jit(solution)/shard_map/ppermute | solution.py:26
  60.7 8.3 %all-to-all-done.1 = bf16[32,24,128]{2,1,0:T(8,128)(2,1)S(1)} async-done(((bf16[32,24,128]{2,1,0:T(8,128)(2,1)}), bf16[32,24,128]{2,1,0:T(8,128)(2,1)S(1)}, u32[]{:S(2)}, u32[]{:S(2)}) %all-to-all-start.1) | async-done | bytes 196640 | tf_op jit(solution)/shard_map/all_to_all | solution.py:214
  69.0 26.9 %all-gather.1 = f16[2048,768]{0,1:T(8,128)(2,1)S(1)} all-gather(f16[128,768]{0,1:T(8,128)(2,1)S(1)} %bitcast.57), channel_id=1, replica_groups=mesh['sp'=32,'y'=8,'c'=2] {'y','c'}, dimensions={0}, use_global_device_ids=true | all-gather | bytes 3342336 | tf_op jit(solution)/shard_map/all_gather | solution.py:217
  95.9 1.0 convert_reduce_fusion
  96.9 1.9 %fusion.7 = f32[768,320]{1,0:T(8,128)S(1)} fusion(bf16[1,2048,320]{1,2,0:T(8,128)(2,1)S(1)} %copy-done, f16[2048,768]{0,1:T(8,128)(2,1)S(1)} %all-gather.1, f32[2048]{0:T(1024)S(1)} %copy-done.7, f32[768]{0:T(1024)S(1)} %get-tuple-element.52, f32[768]{0:T(1024)S(1)} %get-tuple-element.51), kind=kOutput, calls=%fused_computation.12 | convolution fusion | flops 1016070144 | bytes 5453824 | tf_op jit(solution)/shard_map/kr,kf->rf/dot_general | solution.py:226
  98.9 2.0 %fusion.5 = bf16[768,320]{1,0:T(8,128)(2,1)S(1)} fusion(bf16[1,2048,320]{1,2,0:T(8,128)(2,1)S(1)} %copy-done.11, f32[768,320]{1,0:T(8,128)S(1)} %fusion.7, f16[2048,768]{0,1:T(8,128)(2,1)S(1)} %all-gather.1, f32[2048]{0:T(1024)S(1)} %copy-done.7, f32[768]{0:T(1024)S(1)} %get-tuple-element.52, f32[768]{0:T(1024)S(1)} %get-tuple-element.51), kind=kOutput, calls=%fused_computation.10 | convolution fusion | flops 1017544704 | bytes 5945344 | tf_op jit(solution)/shard_map/kr,kf->rf/dot_general | solution.py:227
  101.0 2.0 %collective-permute-start.1 = (bf16[768,384]{1,0:T(8,128)(2,1)S(1)}, bf16[768,384]{1,0:T(8,128)(2,1)S(1)}, u32[]{:S(2)}, u32[]{:S(2)}) collective-permute-start(bf16[768,384]{1,0:T(8,128)(2,1)S(1)} %pad.4.mine_ref), channel_id=1, source_target_pairs={{0,1},{1,0},{2,3},{3,2},{4,5},{5,4},{6,7},{7,6},{8,9},{9,8},{10,11... | collective-permute-start | bytes 1769480 | tf_op jit(solution)/shard_map/ppermute | solution.py:26
  103.0 1.8 %collective-permute-done.1.else_ref = bf16[768,384]{1,0:T(8,128)(2,1)S(1)} collective-permute-done((bf16[768,384]{1,0:T(8,128)(2,1)S(1)}, bf16[768,384]{1,0:T(8,128)(2,1)S(1)}, u32[]{:S(2)}, u32[]{:S(2)}) %collective-permute-start.1) | collective-permute-done | bytes 589856 | tf_op jit(solution)/shard_map/ppermute | solution.py:26
  104.9 0.8 copy-done.4
  105.7 5.2 %down.1 = bf16[32,8,24,128]{3,2,1,0:T(8,128)(2,1)} custom-call(s32[1]{0:T(128)} %bitcast.15.at_ref, bf16[768,384]{1,0:T(8,128)(2,1)} %copy-done.2, bf16[768,384]{1,0:T(8,128)(2,1)} %copy-done.4, bf16[320,2048]{1,0:T(8,128)(2,1)} %bitcast.53, bf16[320,2048]{1,0:T(8,128)(2,1)} %bitcast.54, bf16[320,2048]{1,0:T(8,128)(2,1)} %collective-permute-done.2.else_0.else_1, ...), custom_call_target="tpu_custom_call" | custom-call | tf_op jit(solution)/shard_map/down/pallas_call | solution.py:238
  110.9 11.2 %all-to-all-start.2 = ((bf16[256,24,128]{2,1,0:T(8,128)(2,1)}), bf16[256,24,128]{2,1,0:T(8,128)(2,1)S(1)}, u32[]{:S(2)}, u32[]{:S(2)}) async-start(bf16[256,24,128]{2,1,0:T(8,128)(2,1)} %bitcast.52), calls=%async_computation.2 | async-start | bytes 3145728 | tf_op jit(solution)/shard_map/all_to_all | solution.py:250
  122.2 41.5 %all-to-all-done.2 = bf16[256,24,128]{2,1,0:T(8,128)(2,1)S(1)} async-done(((bf16[256,24,128]{2,1,0:T(8,128)(2,1)}), bf16[256,24,128]{2,1,0:T(8,128)(2,1)S(1)}, u32[]{:S(2)}, u32[]{:S(2)}) %all-to-all-start.2) | async-done | bytes 1572896 | tf_op jit(solution)/shard_map/all_to_all | solution.py:250
  163.7 0.2 bitcast_reduce_fusion
  164.0 0.3 convolution_multiply_fusion.2
  164.3 0.5 multiply_reduce_fusion
  164.9 0.7 broadcast_in_dim.11
  165.6 5.9 %all-to-all-start.3 = ((f32[16,15,128]{2,1,0:T(8,128)}), f32[16,15,128]{2,1,0:T(8,128)S(1)}, u32[]{:S(2)}, u32[]{:S(2)}) async-start(f32[16,15,128]{2,1,0:T(8,128)} %broadcast_in_dim.11), calls=%async_computation.3 | async-start | bytes 262144 | tf_op jit(solution)/shard_map/all_to_all | solution.py:31
  171.5 0.6 multiply_reduce_fusion.7
  172.6 8.0 %all-to-all-done.3 = f32[16,15,128]{2,1,0:T(8,128)S(1)} async-done(((f32[16,15,128]{2,1,0:T(8,128)}), f32[16,15,128]{2,1,0:T(8,128)S(1)}, u32[]{:S(2)}, u32[]{:S(2)}) %all-to-all-start.3) | async-done | bytes 122912 | tf_op jit(solution)/shard_map/all_to_all | solution.py:31
  180.8 0.7 add_rsqrt_fusion.1
  181.4 0.8 multiply_convert_fusion.1
  (35 shorter events, 0.5 us)
Async XLA Ops:
  0.0 96.9 %copy-start = (bf16[1,2048,320]{1,2,0:T(8,128)(2,1)S(1)}, bf16[1,2048,320]{1,2,0:T(8,128)(2,1)}, u32[]{:S(2)}) copy-start(bf16[1,2048,320]{1,2,0:T(8,128)(2,1)} %param.24) | copy-start | bytes 3932164
  0.0 58.3 %copy-start.1 = (bf16[1,320,2048]{2,1,0:T(8,128)(2,1)S(1)}, bf16[1,320,2048]{2,1,0:T(8,128)(2,1)}, u32[]{:S(2)}) copy-start(bf16[1,320,2048]{2,1,0:T(8,128)(2,1)} %param.26) | copy-start | bytes 3932164
  3.4 36.8 %all-to-all-start = ((bf16[16,64,128]{2,1,0:T(8,128)(2,1)}), bf16[16,64,128]{2,1,0:T(8,128)(2,1)S(1)}, u32[]{:S(2)}, u32[]{:S(2)}) async-start(bf16[16,64,128]{2,1,0:T(8,128)(2,1)} %bitcast_bitcast_fusion), calls=%async_computation | async-start | bytes 524288 | tf_op jit(solution)/shard_map/all_to_all | solution.py:186
  13.5 2.7 %collective-permute-start = (bf16[80,128]{1,0:T(8,128)(2,1)}, bf16[80,128]{1,0:T(8,128)(2,1)S(1)}, u32[]{:S(2)}, u32[]{:S(2)}) collective-permute-start(bf16[80,128]{1,0:T(8,128)(2,1)} %get-tuple-element.16), channel_id=1, source_target_pairs={{0,16},{16,32},{32,48},{48,64},{64,80},{80,96},{96,112},{112,128},... | collective-permute-start | bytes 61448 | tf_op jit(solution)/shard_map/ppermute | solution.py:22
  16.2 0.6 copy-start.6
  40.1 0.7 copy-start.3
  43.8 25.2 %all-to-all-start.1 = ((bf16[32,24,128]{2,1,0:T(8,128)(2,1)}), bf16[32,24,128]{2,1,0:T(8,128)(2,1)S(1)}, u32[]{:S(2)}, u32[]{:S(2)}) async-start(bf16[32,24,128]{2,1,0:T(8,128)(2,1)} %get-tuple-element.20), calls=%async_computation.1 | async-start | bytes 393216 | tf_op jit(solution)/shard_map/all_to_all | solution.py:214
  58.3 44.7 %collective-permute-start.2 = (bf16[320,2048]{1,0:T(8,128)(2,1)S(1)}, bf16[320,2048]{1,0:T(8,128)(2,1)}, u32[]{:S(2)}, u32[]{:S(2)}) collective-permute-start(bf16[320,2048]{1,0:T(8,128)(2,1)S(1)} %bitcast.55), channel_id=1, source_target_pairs={{0,1},{1,0},{2,3},{3,2},{4,5},{5,4},{6,7},{7,6},{8,9},{9,8},{10,11... | collective-permute-start | bytes 3932168 | tf_op jit(solution)/shard_map/ppermute | solution.py:26
  69.0 27.9 %copy-start.7 = (f32[2048]{0:T(1024)S(1)}, f32[2048]{0:T(1024)}, u32[]{:S(2)}) copy-start(f32[2048]{0:T(1024)} %param.21) | copy-start | bytes 24580
  96.9 2.0 %copy-start.11 = (bf16[1,2048,320]{1,2,0:T(8,128)(2,1)S(1)}, bf16[1,2048,320]{1,2,0:T(8,128)(2,1)}, u32[]{:S(2)}) copy-start(bf16[1,2048,320]{1,2,0:T(8,128)(2,1)} %param.25) | copy-start | bytes 3932164
  101.0 4.7 %copy-start.2 = (bf16[768,384]{1,0:T(8,128)(2,1)}, bf16[768,384]{1,0:T(8,128)(2,1)S(1)}, u32[]{:S(2)}) copy-start(bf16[768,384]{1,0:T(8,128)(2,1)S(1)} %pad.4.mine_ref) | copy-start | bytes 1769476
  101.0 3.9 %collective-permute-start.1 = (bf16[768,384]{1,0:T(8,128)(2,1)S(1)}, bf16[768,384]{1,0:T(8,128)(2,1)S(1)}, u32[]{:S(2)}, u32[]{:S(2)}) collective-permute-start(bf16[768,384]{1,0:T(8,128)(2,1)S(1)} %pad.4.mine_ref), channel_id=1, source_target_pairs={{0,1},{1,0},{2,3},{3,2},{4,5},{5,4},{6,7},{7,6},{8,9},{9,8},{10,11... | collective-permute-start | bytes 1769480 | tf_op jit(solution)/shard_map/ppermute | solution.py:26
  104.9 0.8 copy-start.4
  110.9 11.3 %copy-start.8 = (f32[192,2]{0,1:T(2,128)S(1)}, f32[192,2]{0,1:T(2,128)}, u32[]{:S(2)}) copy-start(f32[192,2]{0,1:T(2,128)} %param.23) | copy-start | bytes 4612
  110.9 11.3 %copy-start.9 = (s32[2,192]{1,0:T(2,128)S(1)}, s32[2,192]{1,0:T(2,128)}, u32[]{:S(2)}) copy-start(s32[2,192]{1,0:T(2,128)} %get-tuple-element.19) | copy-start | bytes 4612
  110.9 53.4 %copy-start.5 = (f32[192,128]{1,0:T(8,128)S(1)}, f32[192,128]{1,0:T(8,128)}, u32[]{:S(2)}) copy-start(f32[192,128]{1,0:T(8,128)} %get-tuple-element.18) | copy-start | bytes 294916
  110.9 70.5 %copy-start.10 = (f32[128]{0:T(128)S(1)}, f32[128]{0:T(128)}, u32[]{:S(2)}) copy-start(f32[128]{0:T(128)} %param.27) | copy-start | bytes 1540
  110.9 52.8 %all-to-all-start.2 = ((bf16[256,24,128]{2,1,0:T(8,128)(2,1)}), bf16[256,24,128]{2,1,0:T(8,128)(2,1)S(1)}, u32[]{:S(2)}, u32[]{:S(2)}) async-start(bf16[256,24,128]{2,1,0:T(8,128)(2,1)} %bitcast.52), calls=%async_computation.2 | async-start | bytes 3145728 | tf_op jit(solution)/shard_map/all_to_all | solution.py:250
  165.6 15.1 %all-to-all-start.3 = ((f32[16,15,128]{2,1,0:T(8,128)}), f32[16,15,128]{2,1,0:T(8,128)S(1)}, u32[]{:S(2)}, u32[]{:S(2)}) async-start(f32[16,15,128]{2,1,0:T(8,128)} %broadcast_in_dim.11), calls=%async_computation.3 | async-start | bytes 262144 | tf_op jit(solution)/shard_map/all_to_all | solution.py:31

commit v6 on v5

--- a/solution.py
+++ b/solution.py
@@ -9,7 +9,8 @@
 from jax.sharding import PartitionSpec as P
 
 
-TP = ("y", "c")
+Y = ("yh", "yl")
+TP = ("yh", "yl", "c")
 
 residual_alpha = 1.41421356
 norm_eps = 1e-05
@@ -111,21 +112,24 @@
     out_ref[...] = outgoing.astype(jnp.bfloat16).reshape(experts, capacity, block)
 
 
-def down_body(at_ref, mine_ref, else_ref, mine_0, mine_1, else_0, else_1, out_ref):
-    units, block = mine_0.shape
-    n_sp, _, capacity, _ = out_ref.shape
-    part = jnp.dot(
-        mine_ref[:, :units],
-        jnp.concatenate([mine_0[...], mine_1[...]], 1),
-        preferred_element_type=jnp.float32,
-    ) + jnp.dot(
-        else_ref[:, :units],
-        jnp.concatenate([else_0[...], else_1[...]], 1),
-        preferred_element_type=jnp.float32,
-    )
-    part = part.astype(jnp.bfloat16)
-    out_ref[:, 0] = part[:, :block].reshape(n_sp, capacity, block)
-    out_ref[:, 1] = part[:, block:].reshape(n_sp, capacity, block)
+def down_body(at_ref, mine_ref, else_ref, *refs, picks):
+    weights, outs = refs[: 2 * picks], refs[2 * picks :]
+    hidden = jnp.concatenate([mine_ref[...], else_ref[...]], 0).T
+    down = jnp.concatenate(
+        [
+            jnp.concatenate([weights[pick][...], weights[picks + pick][...]], 0)
+            for pick in range(picks)
+        ],
+        1,
+    )
+    part = jnp.dot(hidden, down, preferred_element_type=jnp.float32).astype(jnp.bfloat16)
+    groups, _, capacity, block = outs[0].shape
+    for number, out_ref in enumerate(outs):
+        rows = slice(number * groups * capacity, (number + 1) * groups * capacity)
+        for pick in range(picks):
+            out_ref[:, pick] = part[rows, pick * block : (pick + 1) * block].reshape(
+                groups, capacity, block
+            )
 
 
 def whole(memory=None):
@@ -153,9 +157,9 @@
     final_gain,
 ):
     f32, bf16 = jnp.float32, jnp.bfloat16
-    n_sp, n_y, n_c = lax.axis_size("sp"), lax.axis_size("y"), lax.axis_size("c")
+    n_sp, n_yh, n_yl, n_c = (lax.axis_size(axis) for axis in ("sp", "yh", "yl", "c"))
+    n_y = n_yh * n_yl
     n_tp = n_y * n_c
-    at_core = lax.axis_index("c").astype(jnp.int32).reshape(1)
     at_tp = lax.axis_index(TP)
     tok_rows, own_ch = glu_value.shape
     features = residual.shape[1]
@@ -223,32 +227,41 @@
     in_rows = (
         (wide * (1.0 / row_scale) - in_mean[None]) * in_rstd[None] * mix_gain[:, None]
     ).astype(bf16)
-    gate_proj = jnp.einsum("kr,kf->rf", in_rows, expert_gate[0], preferred_element_type=f32)
-    up_proj = jnp.einsum("kr,kf->rf", in_rows, expert_up[0], preferred_element_type=f32)
+    gate_proj = jnp.einsum("kf,kr->fr", expert_gate[0], in_rows, preferred_element_type=f32)
+    up_proj = jnp.einsum("kf,kr->fr", expert_up[0], in_rows, preferred_element_type=f32)
     hidden = (jax.nn.silu(gate_proj) * up_proj).astype(bf16)
-    wide_units = -(-hidden.shape[1] // 128) * 128
-    hidden = jnp.pad(hidden, ((0, 0), (0, wide_units - hidden.shape[1])))
 
     w_down = expert_down[0]
     units = w_down.shape[0]
-    picks = [
-        pl.BlockSpec((units, feat_block), lambda i, at, step=step: (0, 2 * (2 * i + step) + at[0]))
-        for step in range(2)
-    ]
-    parts = pl.pallas_call(
-        down_body,
-        out_shape=jax.ShapeDtypeStruct((n_sp, n_y, capacity, feat_block), bf16),
-        grid_spec=pltpu.PrefetchScalarGridSpec(
-            num_scalar_prefetch=1,
-            grid=(n_y // 2,),
-            in_specs=[full(rows, wide_units), full(rows, wide_units), *picks, *picks],
-            out_specs=pl.BlockSpec((n_sp, 2, capacity, feat_block), lambda i, at: (0, i, 0, 0)),
-        ),
-        name="down",
-    )(at_core, hidden, swap(hidden, "c"), w_down, w_down, *([swap(w_down, "c")] * 2))
-    parts = parts.reshape(n_sp * n_y, capacity, feat_block)
-    returned = lax.all_to_all(parts, ("sp", "y"), 0, 0, tiled=True)
-    returned = returned.reshape(experts, n_y, capacity, feat_block)
+    hidden_else, down_else = swap(hidden, "c"), swap(w_down, "c")
+    at_yl, at_c = lax.axis_index("yl"), lax.axis_index("c")
+
+    def down(parity, outs):
+        blocks = (jnp.arange(n_yh) * n_yl + parity) * n_c + at_c
+        picks = [
+            pl.BlockSpec((units, feat_block), lambda i, at, pick=pick: (0, at[pick]))
+            for pick in range(n_yh)
+        ]
+        shape = (n_sp // outs, n_yh, capacity, feat_block)
+        return pl.pallas_call(
+            functools.partial(down_body, picks=n_yh),
+            out_shape=[jax.ShapeDtypeStruct(shape, bf16)] * outs,
+            grid_spec=pltpu.PrefetchScalarGridSpec(
+                num_scalar_prefetch=1,
+                grid=(1,),
+                in_specs=[full(units, rows), full(units, rows), *picks, *picks],
+                out_specs=[full(*shape)] * outs,
+            ),
+        )(blocks.astype(jnp.int32), hidden, hidden_else, *[w_down] * n_yh, *[down_else] * n_yh)
+
+    near, far = down(1 - at_yl, 2)
+    near = lax.ppermute(near, Y, [(i, i ^ 1) for i in range(n_y)])
+    far = lax.ppermute(far, Y, [(i, (i - 1 if i % 2 == 0 else i + 1) % n_y) for i in range(n_y)])
+    (kept,) = down(at_yl, 1)
+    parts = kept.astype(f32) + jnp.concatenate([near, far], 0).astype(f32)
+    parts = parts.astype(bf16).reshape(n_sp * n_yh, capacity, feat_block)
+    returned = lax.all_to_all(parts, ("sp", "yh"), 0, 0, tiled=True)
+    returned = returned.reshape(experts, n_yh, capacity, feat_block)
     expert_out = jnp.sum(returned.astype(f32), 1).astype(bf16).reshape(rows, feat_block)
     slots = jnp.arange(experts * capacity, dtype=jnp.int32)
     first = (slot_rows[0][:, None] == slots[None, :]).astype(bf16)
@@ -290,7 +303,7 @@
 
 
 def solution(mesh):
-    finer = Mesh(mesh.devices.reshape(mesh.shape["sp"], 8, 2), ("sp", "y", "c"))
+    finer = Mesh(mesh.devices.reshape(mesh.shape["sp"], 4, 2, 2), ("sp", "yh", "yl", "c"))
     placed = (
         P("sp", TP),
         P("sp", TP),

time: 183 us -> 181 us (0.989)
  waiting for transfers between devices: 60.7 us -> 53.3 us
  other arithmetic: 3.35 us -> 6.6 us
  Pallas kernels: 12 us -> 14.3 us
    all_to_all x1, waiting for transfers between devices: 41.5 us -> 27.4 us  [local(): returned = lax.all_to_all(parts, ('sp', 'yh'), 0, 0, tiled=True)]
    ppermute x0 -> x2, waiting for transfers between devices: none -> 7.28 us  [the longest x1 4.02 us: local(): lax.ppermute(far, Y, [(i, (i - 1 if i % 2 == 0 else i + 1) % n_y) for i i...]
    ppermute x0 -> x2, starting transfers between devices: none -> 5.7 us  [the longest x1 3.78 us: local(): near = lax.ppermute(near, Y, [(i, i ^ 1) for i in range(n_y)])]
    all_to_all x1, starting transfers between devices: 11.2 us -> 7.97 us  [local(): returned = lax.all_to_all(parts, ('sp', 'yh'), 0, 0, tiled=True)]
    convert_element_type x0 -> x1, other arithmetic: none -> 2.28 us  [local(): parts = parts.astype(bf16).reshape(n_sp * n_yh, capacity, feat_block)]
    pallas_call x1 -> x2, Pallas kernels: 5.21 us -> 7.45 us  [down(): pl.pallas_call(functools.partial(down_body, picks=n_yh), out_shape=[jax.S...]
  transfers between devices with their start and end apart: 7 -> 9, of which waited for: 5 -> 7; matrix products, arithmetic and copies ran while one was open for 3% -> 3% of each run, Pallas kernels for 1% -> 3%
where the time goes in v6:
time: 181 us; the launch traced here: 180 us
  waiting for transfers between devices  53.3 us (29%)
  starting transfers between devices  49.3 us (27%)
  blocking collectives  48 us (27%)
  Pallas kernels  14.3 us (8%)
  other arithmetic  6.6 us (4%)
  matrix products  4.14 us (2%)
  local copies, waits for them, and re-layouts  4 us (2%)
    all_to_all x1, waiting for transfers between devices, local(): returned = lax.all_to_all(parts, ('sp', 'yh'), 0, 0, tiled=True)  27.4 us
    all_gather x1, blocking collectives, local(): gathered = lax.all_gather(arrived, TP, axis=0, tiled=True)  26.9 us
    all_gather x1, blocking collectives, local(): filtered = lax.all_gather(filtered, TP, axis=0, tiled=True)  21.1 us
    all_to_all x1, starting transfers between devices, local(): arrived = lax.all_to_all(outgoing, 'sp', 0, 0, tiled=True)  14.5 us
    all_to_all x1, starting transfers between devices, local(): weight_own = lax.all_to_all(weight_parts, TP, 0, 0, tiled=True)  10.2 us
    all_to_all x1, waiting for transfers between devices, local(): arrived = lax.all_to_all(outgoing, 'sp', 0, 0, tiled=True)  8.26 us
    all_to_all x1, waiting for transfers between devices, summed_over(): return jnp.sum(lax.all_to_all(copies, axis, 0, 0, tiled=True), axis=0)  8.02 us
    all_to_all x1, starting transfers between devices, local(): returned = lax.all_to_all(parts, ('sp', 'yh'), 0, 0, tiled=True)  7.97 us
  transfers between devices with their start and end apart: 9, of which 7 were waited for; matrix products, arithmetic and copies ran while one was open for 3% of the time, Pallas kernels for 3%

profile of v6, /device:TPU:1, one launch (start us, length us, event | category | flops | bytes accessed | tf_op | source)
XLA Modules:
  0.0 180.4 jit_solution(15615774396838458007)
XLA Ops:
  0.0 1.6 head.1
  1.6 1.7 bitcast_bitcast_fusion
  3.4 10.2 %all-to-all-start = ((bf16[16,64,128]{2,1,0:T(8,128)(2,1)}), bf16[16,64,128]{2,1,0:T(8,128)(2,1)S(1)}, u32[]{:S(2)}, u32[]{:S(2)}) async-start(bf16[16,64,128]{2,1,0:T(8,128)(2,1)} %bitcast_bitcast_fusion), calls=%async_computation | async-start | bytes 524288 | tf_op jit(solution)/shard_map/all_to_all | solution.py:190
  13.5 1.6 collective-permute-start
  15.1 1.1 collective-permute-done.rim_ref
  16.8 2.2 %conv.1 = bf16[64,256]{1,0:T(8,128)(2,1)} custom-call(bf16[80,256]{1,0:T(8,128)(2,1)} %get-tuple-element.17.own_ref, bf16[80,128]{1,0:T(8,128)(2,1)} %copy-done.5, bf16[31,64]{1,0:T(8,128)(2,1)} %kernel_ref.1, f32[1,64]{1,0:T(1,128)} %bitcast.100), custom_call_target="tpu_custom_call" | custom-call | tf_op jit(solution)/shard_map/conv/pallas_call | solution.py:181
  19.0 21.1 %all_gather.6.filtered_ref = bf16[1024,256]{1,0:T(8,128)(2,1)} all-gather(bf16[64,256]{1,0:T(8,128)(2,1)} %conv.1), channel_id=1, replica_groups=mesh['sp'=32,'yh'=4,'yl'=2,'c'=2] {'yh','yl','c'}, dimensions={0}, use_global_device_ids=true | all-gather | bytes 557056 | tf_op jit(solution)/shard_map/all_gather | solution.py:188
  40.1 0.7 copy-done.3
  40.8 3.0 %mix.1 = (f32[192,128]{1,0:T(8,128)}, bf16[32,24,128]{2,1,0:T(8,128)(2,1)}, s32[2,192]{1,0:T(2,128)}) custom-call(s32[1]{0:T(128)} %bitcast.at_ref, s32[2,192]{1,0:T(2,128)} %bitcast.85, bf16[1024,256]{1,0:T(8,128)(2,1)} %all_gather.6.filtered_ref, bf16[1024,128]{1,0:T(8,128)(2,1)} %bitcast.70, bf16[192,2048]{1,0:T(8,128)(2,1)} %residual_ref.1), custom_call_target="tpu_custom_call" | custom-call | tf_op jit(solution)/shard_map/mix/pallas_call | solution.py:194
  43.8 14.5 %all-to-all-start.1 = ((bf16[32,24,128]{2,1,0:T(8,128)(2,1)}), bf16[32,24,128]{2,1,0:T(8,128)(2,1)S(1)}, u32[]{:S(2)}, u32[]{:S(2)}) async-start(bf16[32,24,128]{2,1,0:T(8,128)(2,1)} %get-tuple-element.22), calls=%async_computation.1 | async-start | bytes 393216 | tf_op jit(solution)/shard_map/all_to_all | solution.py:218
  58.3 2.4 %collective-permute-start.2 = (bf16[320,2048]{1,0:T(8,128)(2,1)S(1)}, bf16[320,2048]{1,0:T(8,128)(2,1)}, u32[]{:S(2)}, u32[]{:S(2)}) collective-permute-start(bf16[320,2048]{1,0:T(8,128)(2,1)S(1)} %bitcast.69), channel_id=1, source_target_pairs={{0,1},{1,0},{2,3},{3,2},{4,5},{5,4},{6,7},{7,6},{8,9},{9,8},{10,11... | collective-permute-start | bytes 3932168 | tf_op jit(solution)/shard_map/ppermute | solution.py:27
  60.7 8.3 %all-to-all-done.1 = bf16[32,24,128]{2,1,0:T(8,128)(2,1)S(1)} async-done(((bf16[32,24,128]{2,1,0:T(8,128)(2,1)}), bf16[32,24,128]{2,1,0:T(8,128)(2,1)S(1)}, u32[]{:S(2)}, u32[]{:S(2)}) %all-to-all-start.1) | async-done | bytes 196640 | tf_op jit(solution)/shard_map/all_to_all | solution.py:218
  69.0 26.9 %all-gather.1 = f16[2048,768]{0,1:T(8,128)(2,1)S(1)} all-gather(f16[128,768]{0,1:T(8,128)(2,1)S(1)} %bitcast.71), channel_id=1, replica_groups=mesh['sp'=32,'yh'=4,'yl'=2,'c'=2] {'yh','yl','c'}, dimensions={0}, use_global_device_ids=true | all-gather | bytes 3342336 | tf_op jit(solution)/shard_map/all_gather | solution.py:221
  95.9 1.0 convert_reduce_fusion
  96.9 1.6 convolution_bitcast_fusion.1
  98.5 1.8 fusion.8.mine_ref
  100.3 2.1 %collective-permute-start.1 = (bf16[320,768]{1,0:T(8,128)(2,1)S(1)}, bf16[320,768]{1,0:T(8,128)(2,1)}, u32[]{:S(2)}, u32[]{:S(2)}) collective-permute-start(bf16[320,768]{1,0:T(8,128)(2,1)S(1)} %fusion.8.mine_ref), channel_id=1, source_target_pairs={{0,1},{1,0},{2,3},{3,2},{4,5},{5,4},{6,7},{7,6},{8,9},{9,8},{10,11... | collective-permute-start | bytes 1474568 | tf_op jit(solution)/shard_map/ppermute | solution.py:27
  102.9 1.3 collective-permute-done.1.else_ref
  104.2 3.7 %shard_map.137 = (bf16[16,4,24,128]{3,2,1,0:T(8,128)(2,1)}, bf16[16,4,24,128]{3,2,1,0:T(8,128)(2,1)}) custom-call(s32[4]{0:T(128)} %multiply_add_fusion.at_ref, bf16[320,768]{1,0:T(8,128)(2,1)} %copy-done.2, bf16[320,768]{1,0:T(8,128)(2,1)} %collective-permute-done.1.else_ref, bf16[320,2048]{1,0:T(8,128)(2,1)} %bitcast.61, bf16[320,2048]{1,0:T(8,128)(2,1)} %bitcast.62, ...), custom_call_target="tpu_custom_call" | custom-call | tf_op jit(solution)/shard_map/pallas_call | solution.py:246
  107.8 3.8 %collective-permute-start.3 = (bf16[16,4,24,128]{3,2,1,0:T(8,128)(2,1)}, bf16[16,4,24,128]{3,2,1,0:T(8,128)(2,1)S(1)}, u32[]{:S(2)}, u32[]{:S(2)}) collective-permute-start(bf16[16,4,24,128]{3,2,1,0:T(8,128)(2,1)} %get-tuple-element.23), channel_id=1, source_target_pairs={{0,2},{2,0},{4,6},{6,4},{8,10},{10,8},{12,14},{14,12},{1,3},{3,1},... | collective-permute-start | bytes 1179656 | tf_op jit(solution)/shard_map/ppermute | solution.py:258
  111.6 1.9 %collective-permute-start.4 = (bf16[16,4,24,128]{3,2,1,0:T(8,128)(2,1)}, bf16[16,4,24,128]{3,2,1,0:T(8,128)(2,1)S(1)}, u32[]{:S(2)}, u32[]{:S(2)}) collective-permute-start(bf16[16,4,24,128]{3,2,1,0:T(8,128)(2,1)} %get-tuple-element.24), channel_id=1, source_target_pairs={{0,14},{2,4},{4,2},{6,8},{8,6},{10,12},{12,10},{14,0},{1,15},{3,5}... | collective-permute-start | bytes 1179656 | tf_op jit(solution)/shard_map/ppermute | solution.py:259
  114.1 3.8 %shard_map.136 = bf16[32,4,24,128]{3,2,1,0:T(8,128)(2,1)} custom-call(s32[4]{0:T(128)} %multiply_add_fusion.1.at_ref, bf16[320,768]{1,0:T(8,128)(2,1)} %copy-done.2, bf16[320,768]{1,0:T(8,128)(2,1)} %collective-permute-done.1.else_ref, bf16[320,2048]{1,0:T(8,128)(2,1)} %bitcast.65, bf16[320,2048]{1,0:T(8,128)(2,1)} %bitcast.66, bf16[320,2048]{1,0:T(8,128)(2,1)} %bitcast.67, ...), custom_call_target="tpu_custom_call" | custom-call | tf_op jit(solution)/shard_map/pallas_call | solution.py:246
  117.9 3.3 %collective-permute-done.3 = bf16[16,4,24,128]{3,2,1,0:T(8,128)(2,1)S(1)} collective-permute-done((bf16[16,4,24,128]{3,2,1,0:T(8,128)(2,1)}, bf16[16,4,24,128]{3,2,1,0:T(8,128)(2,1)S(1)}, u32[]{:S(2)}, u32[]{:S(2)}) %collective-permute-start.3) | collective-permute-done | bytes 393248 | tf_op jit(solution)/shard_map/ppermute | solution.py:258
  121.2 4.0 %collective-permute-done.4 = bf16[16,4,24,128]{3,2,1,0:T(8,128)(2,1)S(1)} collective-permute-done((bf16[16,4,24,128]{3,2,1,0:T(8,128)(2,1)}, bf16[16,4,24,128]{3,2,1,0:T(8,128)(2,1)S(1)}, u32[]{:S(2)}, u32[]{:S(2)}) %collective-permute-start.4) | collective-permute-done | bytes 393248 | tf_op jit(solution)/shard_map/ppermute | solution.py:259
  125.2 2.3 %add_convert_fusion = bf16[32,4,24,128]{3,2,1,0:T(8,128)(2,1)} fusion(bf16[32,4,24,128]{3,2,1,0:T(8,128)(2,1)} %shard_map.136, bf16[16,4,24,128]{3,2,1,0:T(8,128)(2,1)S(1)} %collective-permute-done.4, bf16[16,4,24,128]{3,2,1,0:T(8,128)(2,1)S(1)} %collective-permute-done.3), kind=kLoop, calls=%fused_computation.8 | loop fusion | flops 1966080 | bytes 2359296 | tf_op jit(solution)/shard_map/convert_element_type | solution.py:262
  127.5 8.0 %all-to-all-start.2 = ((bf16[128,24,128]{2,1,0:T(8,128)(2,1)}), bf16[128,24,128]{2,1,0:T(8,128)(2,1)S(1)}, u32[]{:S(2)}, u32[]{:S(2)}) async-start(bf16[128,24,128]{2,1,0:T(8,128)(2,1)} %bitcast.22), calls=%async_computation.2 | async-start | bytes 1572864 | tf_op jit(solution)/shard_map/all_to_all | solution.py:263
  135.5 27.4 %all-to-all-done.2 = bf16[128,24,128]{2,1,0:T(8,128)(2,1)S(1)} async-done(((bf16[128,24,128]{2,1,0:T(8,128)(2,1)}), bf16[128,24,128]{2,1,0:T(8,128)(2,1)S(1)}, u32[]{:S(2)}, u32[]{:S(2)}) %all-to-all-start.2) | async-done | bytes 786464 | tf_op jit(solution)/shard_map/all_to_all | solution.py:263
  164.0 0.7 broadcast_in_dim.11
  164.7 4.9 %all-to-all-start.3 = ((f32[16,15,128]{2,1,0:T(8,128)}), f32[16,15,128]{2,1,0:T(8,128)S(1)}, u32[]{:S(2)}, u32[]{:S(2)}) async-start(f32[16,15,128]{2,1,0:T(8,128)} %broadcast_in_dim.11), calls=%async_computation.3 | async-start | bytes 262144 | tf_op jit(solution)/shard_map/all_to_all | solution.py:32
  170.8 8.0 %all-to-all-done.3 = f32[16,15,128]{2,1,0:T(8,128)S(1)} async-done(((f32[16,15,128]{2,1,0:T(8,128)}), f32[16,15,128]{2,1,0:T(8,128)S(1)}, u32[]{:S(2)}, u32[]{:S(2)}) %all-to-all-start.3) | async-done | bytes 122912 | tf_op jit(solution)/shard_map/all_to_all | solution.py:32
  178.9 0.7 add_rsqrt_fusion.1
  179.6 0.8 multiply_convert_fusion.1
  (40 shorter events, 3.7 us)
Async XLA Ops:
  0.0 96.9 %copy-start = (bf16[1,2048,320]{1,2,0:T(8,128)(2,1)S(1)}, bf16[1,2048,320]{1,2,0:T(8,128)(2,1)}, u32[]{:S(2)}) copy-start(bf16[1,2048,320]{1,2,0:T(8,128)(2,1)} %param.24) | copy-start | bytes 3932164
  0.0 58.3 %copy-start.1 = (bf16[1,320,2048]{2,1,0:T(8,128)(2,1)S(1)}, bf16[1,320,2048]{2,1,0:T(8,128)(2,1)}, u32[]{:S(2)}) copy-start(bf16[1,320,2048]{2,1,0:T(8,128)(2,1)} %param.26) | copy-start | bytes 3932164
  3.4 36.8 %all-to-all-start = ((bf16[16,64,128]{2,1,0:T(8,128)(2,1)}), bf16[16,64,128]{2,1,0:T(8,128)(2,1)S(1)}, u32[]{:S(2)}, u32[]{:S(2)}) async-start(bf16[16,64,128]{2,1,0:T(8,128)(2,1)} %bitcast_bitcast_fusion), calls=%async_computation | async-start | bytes 524288 | tf_op jit(solution)/shard_map/all_to_all | solution.py:190
  13.5 2.7 %collective-permute-start = (bf16[80,128]{1,0:T(8,128)(2,1)}, bf16[80,128]{1,0:T(8,128)(2,1)S(1)}, u32[]{:S(2)}, u32[]{:S(2)}) collective-permute-start(bf16[80,128]{1,0:T(8,128)(2,1)} %get-tuple-element.18), channel_id=1, source_target_pairs={{0,16},{16,32},{32,48},{48,64},{64,80},{80,96},{96,112},{112,128},... | collective-permute-start | bytes 61448 | tf_op jit(solution)/shard_map/ppermute | solution.py:23
  16.2 0.6 copy-start.5
  40.1 0.7 copy-start.3
  43.8 25.2 %all-to-all-start.1 = ((bf16[32,24,128]{2,1,0:T(8,128)(2,1)}), bf16[32,24,128]{2,1,0:T(8,128)(2,1)S(1)}, u32[]{:S(2)}, u32[]{:S(2)}) async-start(bf16[32,24,128]{2,1,0:T(8,128)(2,1)} %get-tuple-element.22), calls=%async_computation.1 | async-start | bytes 393216 | tf_op jit(solution)/shard_map/all_to_all | solution.py:218
  58.3 44.6 %collective-permute-start.2 = (bf16[320,2048]{1,0:T(8,128)(2,1)S(1)}, bf16[320,2048]{1,0:T(8,128)(2,1)}, u32[]{:S(2)}, u32[]{:S(2)}) collective-permute-start(bf16[320,2048]{1,0:T(8,128)(2,1)S(1)} %bitcast.69), channel_id=1, source_target_pairs={{0,1},{1,0},{2,3},{3,2},{4,5},{5,4},{6,7},{7,6},{8,9},{9,8},{10,11... | collective-permute-start | bytes 3932168 | tf_op jit(solution)/shard_map/ppermute | solution.py:27
  69.0 27.9 %copy-start.6 = (f32[2048]{0:T(1024)S(1)}, f32[2048]{0:T(1024)}, u32[]{:S(2)}) copy-start(f32[2048]{0:T(1024)} %param.21) | copy-start | bytes 24580
  96.9 1.6 copy-start.10
  100.3 3.9 %copy-start.2 = (bf16[320,768]{1,0:T(8,128)(2,1)}, bf16[320,768]{1,0:T(8,128)(2,1)S(1)}, u32[]{:S(2)}) copy-start(bf16[320,768]{1,0:T(8,128)(2,1)S(1)} %fusion.8.mine_ref) | copy-start | bytes 1474564
  100.3 3.9 %collective-permute-start.1 = (bf16[320,768]{1,0:T(8,128)(2,1)S(1)}, bf16[320,768]{1,0:T(8,128)(2,1)}, u32[]{:S(2)}, u32[]{:S(2)}) collective-permute-start(bf16[320,768]{1,0:T(8,128)(2,1)S(1)} %fusion.8.mine_ref), channel_id=1, source_target_pairs={{0,1},{1,0},{2,3},{3,2},{4,5},{5,4},{6,7},{7,6},{8,9},{9,8},{10,11... | collective-permute-start | bytes 1474568 | tf_op jit(solution)/shard_map/ppermute | solution.py:27
  107.8 13.3 %collective-permute-start.3 = (bf16[16,4,24,128]{3,2,1,0:T(8,128)(2,1)}, bf16[16,4,24,128]{3,2,1,0:T(8,128)(2,1)S(1)}, u32[]{:S(2)}, u32[]{:S(2)}) collective-permute-start(bf16[16,4,24,128]{3,2,1,0:T(8,128)(2,1)} %get-tuple-element.23), channel_id=1, source_target_pairs={{0,2},{2,0},{4,6},{6,4},{8,10},{10,8},{12,14},{14,12},{1,3},{3,1},... | collective-permute-start | bytes 1179656 | tf_op jit(solution)/shard_map/ppermute | solution.py:258
  111.6 13.6 %collective-permute-start.4 = (bf16[16,4,24,128]{3,2,1,0:T(8,128)(2,1)}, bf16[16,4,24,128]{3,2,1,0:T(8,128)(2,1)S(1)}, u32[]{:S(2)}, u32[]{:S(2)}) collective-permute-start(bf16[16,4,24,128]{3,2,1,0:T(8,128)(2,1)} %get-tuple-element.24), channel_id=1, source_target_pairs={{0,14},{2,4},{4,2},{6,8},{8,6},{10,12},{12,10},{14,0},{1,15},{3,5}... | collective-permute-start | bytes 1179656 | tf_op jit(solution)/shard_map/ppermute | solution.py:259
  117.9 17.6 %copy-start.7 = (f32[192,2]{0,1:T(2,128)S(1)}, f32[192,2]{0,1:T(2,128)}, u32[]{:S(2)}) copy-start(f32[192,2]{0,1:T(2,128)} %param.23) | copy-start | bytes 4612
  117.9 17.6 %copy-start.8 = (s32[2,192]{1,0:T(2,128)S(1)}, s32[2,192]{1,0:T(2,128)}, u32[]{:S(2)}) copy-start(s32[2,192]{1,0:T(2,128)} %get-tuple-element.21) | copy-start | bytes 4612
  117.9 45.5 %copy-start.4 = (f32[192,128]{1,0:T(8,128)S(1)}, f32[192,128]{1,0:T(8,128)}, u32[]{:S(2)}) copy-start(f32[192,128]{1,0:T(8,128)} %get-tuple-element.20) | copy-start | bytes 294916
  117.9 61.7 %copy-start.9 = (f32[128]{0:T(128)S(1)}, f32[128]{0:T(128)}, u32[]{:S(2)}) copy-start(f32[128]{0:T(128)} %param.27) | copy-start | bytes 1540
  127.5 35.5 %all-to-all-start.2 = ((bf16[128,24,128]{2,1,0:T(8,128)(2,1)}), bf16[128,24,128]{2,1,0:T(8,128)(2,1)S(1)}, u32[]{:S(2)}, u32[]{:S(2)}) async-start(bf16[128,24,128]{2,1,0:T(8,128)(2,1)} %bitcast.22), calls=%async_computation.2 | async-start | bytes 1572864 | tf_op jit(solution)/shard_map/all_to_all | solution.py:263
  164.7 14.1 %all-to-all-start.3 = ((f32[16,15,128]{2,1,0:T(8,128)}), f32[16,15,128]{2,1,0:T(8,128)S(1)}, u32[]{:S(2)}, u32[]{:S(2)}) async-start(f32[16,15,128]{2,1,0:T(8,128)} %broadcast_in_dim.11), calls=%async_computation.3 | async-start | bytes 262144 | tf_op jit(solution)/shard_map/all_to_all | solution.py:32

commit v7 on v6

--- a/solution.py
+++ b/solution.py
@@ -96,7 +96,7 @@
     row_mean = jnp.sum(filtered, 0, keepdims=True) / channels
     row_var = jnp.sum(filtered * filtered, 0, keepdims=True) / channels - row_mean * row_mean
     normed = (filtered - row_mean) * lax.rsqrt(row_var + norm_eps) * gain
-    conv_out = (normed / (1.0 + jnp.exp(-normed))).astype(jnp.bfloat16)
+    conv_out = (normed * (0.5 + 0.5 * jnp.tanh(0.5 * normed))).astype(jnp.bfloat16)
     mix = lax.dot_general(
         conv_out, weight_ref[...], (((0,), (0,)), ((), ())), preferred_element_type=jnp.float32
     )
@@ -217,6 +217,14 @@
     )(at_tp.astype(jnp.int32).reshape(1), routes.T, filtered, weight_own, residual)
     arrived = lax.all_to_all(outgoing, "sp", 0, 0, tiled=True)
     rows = n_sp * capacity
+    at_yl, at_c = lax.axis_index("yl"), lax.axis_index("c")
+    blocks_send, blocks_keep = (
+        ((jnp.arange(n_yh) * n_yl + parity) * n_c + at_c).astype(jnp.int32)
+        for parity in (1 - at_yl, at_yl)
+    )
+    arrived, blocks_send, blocks_keep = lax.optimization_barrier(
+        (arrived, blocks_send, blocks_keep)
+    )
     arrived = (arrived.reshape(rows, feat_block).T.astype(f32) * row_scale).astype(jnp.float16)
     gathered = lax.all_gather(arrived, TP, axis=0, tiled=True)
 
@@ -234,10 +242,7 @@
     w_down = expert_down[0]
     units = w_down.shape[0]
     hidden_else, down_else = swap(hidden, "c"), swap(w_down, "c")
-    at_yl, at_c = lax.axis_index("yl"), lax.axis_index("c")
-
-    def down(parity, outs):
-        blocks = (jnp.arange(n_yh) * n_yl + parity) * n_c + at_c
+    def down(blocks, outs):
         picks = [
             pl.BlockSpec((units, feat_block), lambda i, at, pick=pick: (0, at[pick]))
             for pick in range(n_yh)
@@ -252,14 +257,16 @@
                 in_specs=[full(units, rows), full(units, rows), *picks, *picks],
                 out_specs=[full(*shape)] * outs,
             ),
-        )(blocks.astype(jnp.int32), hidden, hidden_else, *[w_down] * n_yh, *[down_else] * n_yh)
-
-    near, far = down(1 - at_yl, 2)
+        )(blocks, hidden, hidden_else, *[w_down] * n_yh, *[down_else] * n_yh)
+
+    near, far = down(blocks_send, 2)
     near = lax.ppermute(near, Y, [(i, i ^ 1) for i in range(n_y)])
     far = lax.ppermute(far, Y, [(i, (i - 1 if i % 2 == 0 else i + 1) % n_y) for i in range(n_y)])
-    (kept,) = down(at_yl, 1)
-    parts = kept.astype(f32) + jnp.concatenate([near, far], 0).astype(f32)
-    parts = parts.astype(bf16).reshape(n_sp * n_yh, capacity, feat_block)
+    (kept,) = down(blocks_keep, 1)
+    half = n_sp // 2
+    parts = kept.at[:half].set((kept[:half].astype(f32) + near.astype(f32)).astype(bf16))
+    parts = parts.at[half:].set((parts[half:].astype(f32) + far.astype(f32)).astype(bf16))
+    parts = parts.reshape(n_sp * n_yh, capacity, feat_block)
     returned = lax.all_to_all(parts, ("sp", "yh"), 0, 0, tiled=True)
     returned = returned.reshape(experts, n_yh, capacity, feat_block)
     expert_out = jnp.sum(returned.astype(f32), 1).astype(bf16).reshape(rows, feat_block)

time: 181 us -> 181 us (level)
    scatter x0 -> x2, other arithmetic: none -> 3.71 us  [the longest x1 1.86 us: local(): parts.at[half:]]
    convert_element_type x1 -> x0, other arithmetic: 2.28 us -> none  [local(): parts = parts.astype(bf16).reshape(n_sp * n_yh, capacity, feat_block)]
    ppermute x1, waiting for transfers between devices: 4.02 us -> 2.16 us  [local(): lax.ppermute(far, Y, [(i, (i - 1 if i % 2 == 0 else i + 1) % n_y) for i i...]
  transfers between devices with their start and end apart: 9 -> 9, of which waited for: 7 -> 7; matrix products, arithmetic and copies ran while one was open for 3% -> 4% of each run, Pallas kernels for 3% -> 3%
where the time goes in v7:
time: 181 us; the launch traced here: 180 us
  waiting for transfers between devices  52 us (29%)
  starting transfers between devices  49.3 us (27%)
  blocking collectives  48 us (27%)
  Pallas kernels  14.3 us (8%)
  other arithmetic  7.52 us (4%)
  matrix products  4.13 us (2%)
  local copies, waits for them, and re-layouts  3.99 us (2%)
    all_to_all x1, waiting for transfers between devices, local(): returned = lax.all_to_all(parts, ('sp', 'yh'), 0, 0, tiled=True)  27.4 us
    all_gather x1, blocking collectives, local(): gathered = lax.all_gather(arrived, TP, axis=0, tiled=True)  26.9 us
    all_gather x1, blocking collectives, local(): filtered = lax.all_gather(filtered, TP, axis=0, tiled=True)  21.1 us
    all_to_all x1, starting transfers between devices, local(): arrived = lax.all_to_all(outgoing, 'sp', 0, 0, tiled=True)  14.5 us
    all_to_all x1, starting transfers between devices, local(): weight_own = lax.all_to_all(weight_parts, TP, 0, 0, tiled=True)  10.2 us
    all_to_all x1, waiting for transfers between devices, summed_over(): return jnp.sum(lax.all_to_all(copies, axis, 0, 0, tiled=True), axis=0)  8.02 us
    all_to_all x1, starting transfers between devices, local(): returned = lax.all_to_all(parts, ('sp', 'yh'), 0, 0, tiled=True)  8.02 us
    all_to_all x1, waiting for transfers between devices, local(): arrived = lax.all_to_all(outgoing, 'sp', 0, 0, tiled=True)  7.67 us
  transfers between devices with their start and end apart: 9, of which 7 were waited for; matrix products, arithmetic and copies ran while one was open for 4% of the time, Pallas kernels for 3%

profile of v7, /device:TPU:1, one launch (start us, length us, event | category | flops | bytes accessed | tf_op | source)
XLA Modules:
  0.0 180.0 jit_solution(2053992698784403117)
XLA Ops:
  0.0 1.6 head.1
  1.6 1.7 bitcast_bitcast_fusion
  3.4 10.2 %all-to-all-start = ((bf16[16,64,128]{2,1,0:T(8,128)(2,1)}), bf16[16,64,128]{2,1,0:T(8,128)(2,1)S(1)}, u32[]{:S(2)}, u32[]{:S(2)}) async-start(bf16[16,64,128]{2,1,0:T(8,128)(2,1)} %bitcast_bitcast_fusion), calls=%async_computation | async-start | bytes 524288 | tf_op jit(solution)/shard_map/all_to_all | solution.py:190
  13.5 1.6 collective-permute-start
  15.1 1.1 collective-permute-done.rim_ref
  16.8 2.2 %conv.1 = bf16[64,256]{1,0:T(8,128)(2,1)} custom-call(bf16[80,256]{1,0:T(8,128)(2,1)} %get-tuple-element.44.own_ref, bf16[80,128]{1,0:T(8,128)(2,1)} %copy-done.5, bf16[31,64]{1,0:T(8,128)(2,1)} %kernel_ref.1, f32[1,64]{1,0:T(1,128)} %bitcast.101), custom_call_target="tpu_custom_call" | custom-call | tf_op jit(solution)/shard_map/conv/pallas_call | solution.py:181
  19.0 21.1 %all_gather.6.filtered_ref = bf16[1024,256]{1,0:T(8,128)(2,1)} all-gather(bf16[64,256]{1,0:T(8,128)(2,1)} %conv.1), channel_id=1, replica_groups=mesh['sp'=32,'yh'=4,'yl'=2,'c'=2] {'yh','yl','c'}, dimensions={0}, use_global_device_ids=true | all-gather | bytes 557056 | tf_op jit(solution)/shard_map/all_gather | solution.py:188
  40.1 0.7 copy-done.3
  40.8 2.9 %mix.1 = (f32[192,128]{1,0:T(8,128)}, bf16[32,24,128]{2,1,0:T(8,128)(2,1)}, s32[2,192]{1,0:T(2,128)}) custom-call(s32[1]{0:T(128)} %bitcast.at_ref, s32[2,192]{1,0:T(2,128)} %bitcast.86, bf16[1024,256]{1,0:T(8,128)(2,1)} %all_gather.6.filtered_ref, bf16[1024,128]{1,0:T(8,128)(2,1)} %bitcast.71, bf16[192,2048]{1,0:T(8,128)(2,1)} %residual_ref.1), custom_call_target="tpu_custom_call" | custom-call | tf_op jit(solution)/shard_map/mix/pallas_call | solution.py:194
  43.7 14.5 %all-to-all-start.1 = ((bf16[32,24,128]{2,1,0:T(8,128)(2,1)}), bf16[32,24,128]{2,1,0:T(8,128)(2,1)S(1)}, u32[]{:S(2)}, u32[]{:S(2)}) async-start(bf16[32,24,128]{2,1,0:T(8,128)(2,1)} %get-tuple-element.49), calls=%async_computation.1 | async-start | bytes 393216 | tf_op jit(solution)/shard_map/all_to_all | solution.py:218
  58.3 2.4 %collective-permute-start.2 = (bf16[320,2048]{1,0:T(8,128)(2,1)S(1)}, bf16[320,2048]{1,0:T(8,128)(2,1)}, u32[]{:S(2)}, u32[]{:S(2)}) collective-permute-start(bf16[320,2048]{1,0:T(8,128)(2,1)S(1)} %bitcast.69), channel_id=1, source_target_pairs={{0,1},{1,0},{2,3},{3,2},{4,5},{5,4},{6,7},{7,6},{8,9},{9,8},{10,11... | collective-permute-start | bytes 3932168 | tf_op jit(solution)/shard_map/ppermute | solution.py:27
  61.2 7.7 %all-to-all-done.1 = bf16[32,24,128]{2,1,0:T(8,128)(2,1)S(1)} async-done(((bf16[32,24,128]{2,1,0:T(8,128)(2,1)}), bf16[32,24,128]{2,1,0:T(8,128)(2,1)S(1)}, u32[]{:S(2)}, u32[]{:S(2)}) %all-to-all-start.1) | async-done | bytes 196640 | tf_op jit(solution)/shard_map/all_to_all | solution.py:218
  69.0 26.9 %all-gather.1 = f16[2048,768]{0,1:T(8,128)(2,1)S(1)} all-gather(f16[128,768]{0,1:T(8,128)(2,1)S(1)} %bitcast.72), channel_id=1, replica_groups=mesh['sp'=32,'yh'=4,'yl'=2,'c'=2] {'yh','yl','c'}, dimensions={0}, use_global_device_ids=true | all-gather | bytes 3342336 | tf_op jit(solution)/shard_map/all_gather | solution.py:229
  95.9 1.0 convert_reduce_fusion
  96.9 1.6 convolution_bitcast_fusion.1
  98.4 1.7 fusion.8.mine_ref
  100.2 2.1 %collective-permute-start.1 = (bf16[320,768]{1,0:T(8,128)(2,1)S(1)}, bf16[320,768]{1,0:T(8,128)(2,1)}, u32[]{:S(2)}, u32[]{:S(2)}) collective-permute-start(bf16[320,768]{1,0:T(8,128)(2,1)S(1)} %fusion.8.mine_ref), channel_id=1, source_target_pairs={{0,1},{1,0},{2,3},{3,2},{4,5},{5,4},{6,7},{7,6},{8,9},{9,8},{10,11... | collective-permute-start | bytes 1474568 | tf_op jit(solution)/shard_map/ppermute | solution.py:27
  102.3 1.8 %collective-permute-done.1.else_ref = bf16[320,768]{1,0:T(8,128)(2,1)} collective-permute-done((bf16[320,768]{1,0:T(8,128)(2,1)S(1)}, bf16[320,768]{1,0:T(8,128)(2,1)}, u32[]{:S(2)}, u32[]{:S(2)}) %collective-permute-start.1) | collective-permute-done | bytes 491552 | tf_op jit(solution)/shard_map/ppermute | solution.py:27
  104.1 3.7 %shard_map.137 = (bf16[16,4,24,128]{3,2,1,0:T(8,128)(2,1)}, bf16[16,4,24,128]{3,2,1,0:T(8,128)(2,1)}) custom-call(s32[4]{0:T(128)} %get-tuple-element.52.at_ref, bf16[320,768]{1,0:T(8,128)(2,1)} %copy-done.2, bf16[320,768]{1,0:T(8,128)(2,1)} %collective-permute-done.1.else_ref, bf16[320,2048]{1,0:T(8,128)(2,1)} %bitcast.61, bf16[320,2048]{1,0:T(8,128)(2,1)} %bitcast.62, ...), custom_call_target="tpu_custom_call" | custom-call | tf_op jit(solution)/shard_map/pallas_call | solution.py:251
  107.8 3.8 %collective-permute-start.3 = (bf16[16,4,24,128]{3,2,1,0:T(8,128)(2,1)}, bf16[16,4,24,128]{3,2,1,0:T(8,128)(2,1)S(1)}, u32[]{:S(2)}, u32[]{:S(2)}) collective-permute-start(bf16[16,4,24,128]{3,2,1,0:T(8,128)(2,1)} %get-tuple-element.53), channel_id=1, source_target_pairs={{0,2},{2,0},{4,6},{6,4},{8,10},{10,8},{12,14},{14,12},{1,3},{3,1},... | collective-permute-start | bytes 1179656 | tf_op jit(solution)/shard_map/ppermute | solution.py:263
  111.6 1.9 %collective-permute-start.4 = (bf16[16,4,24,128]{3,2,1,0:T(8,128)(2,1)}, bf16[16,4,24,128]{3,2,1,0:T(8,128)(2,1)S(1)}, u32[]{:S(2)}, u32[]{:S(2)}) collective-permute-start(bf16[16,4,24,128]{3,2,1,0:T(8,128)(2,1)} %get-tuple-element.54), channel_id=1, source_target_pairs={{0,14},{2,4},{4,2},{6,8},{8,6},{10,12},{12,10},{14,0},{1,15},{3,5}... | collective-permute-start | bytes 1179656 | tf_op jit(solution)/shard_map/ppermute | solution.py:264
  113.5 3.8 %shard_map.136 = bf16[32,4,24,128]{3,2,1,0:T(8,128)(2,1)} custom-call(s32[4]{0:T(128)} %get-tuple-element.50.at_ref, bf16[320,768]{1,0:T(8,128)(2,1)} %copy-done.2, bf16[320,768]{1,0:T(8,128)(2,1)} %collective-permute-done.1.else_ref, bf16[320,2048]{1,0:T(8,128)(2,1)} %bitcast.65, bf16[320,2048]{1,0:T(8,128)(2,1)} %bitcast.66, bf16[320,2048]{1,0:T(8,128)(2,1)} %bitcast.67, ...), custom_call_target="tpu_custom_call" | custom-call | tf_op jit(solution)/shard_map/pallas_call | solution.py:251
  117.3 3.8 %collective-permute-done.3 = bf16[16,4,24,128]{3,2,1,0:T(8,128)(2,1)S(1)} collective-permute-done((bf16[16,4,24,128]{3,2,1,0:T(8,128)(2,1)}, bf16[16,4,24,128]{3,2,1,0:T(8,128)(2,1)S(1)}, u32[]{:S(2)}, u32[]{:S(2)}) %collective-permute-start.3) | collective-permute-done | bytes 393248 | tf_op jit(solution)/shard_map/ppermute | solution.py:263
  121.1 1.9 %fusion.12 = bf16[32,4,24,128]{3,2,1,0:T(8,128)(2,1)} fusion(bf16[32,4,24,128]{3,2,1,0:T(8,128)(2,1)} %shard_map.136, bf16[16,4,24,128]{3,2,1,0:T(8,128)(2,1)S(1)} %collective-permute-done.3), kind=kLoop, calls=%fused_computation.22 | loop fusion | flops 786432 | bytes 1179648 | tf_op jit(solution)/shard_map/scatter | solution.py:267
  123.0 2.2 %collective-permute-done.4 = bf16[16,4,24,128]{3,2,1,0:T(8,128)(2,1)S(1)} collective-permute-done((bf16[16,4,24,128]{3,2,1,0:T(8,128)(2,1)}, bf16[16,4,24,128]{3,2,1,0:T(8,128)(2,1)S(1)}, u32[]{:S(2)}, u32[]{:S(2)}) %collective-permute-start.4) | collective-permute-done | bytes 393248 | tf_op jit(solution)/shard_map/ppermute | solution.py:264
  125.1 1.9 %fusion.13 = bf16[32,4,24,128]{3,2,1,0:T(8,128)(2,1)} fusion(bf16[32,4,24,128]{3,2,1,0:T(8,128)(2,1)} %fusion.12, bf16[16,4,24,128]{3,2,1,0:T(8,128)(2,1)S(1)} %collective-permute-done.4), kind=kLoop, calls=%fused_computation.23 | loop fusion | flops 786432 | bytes 1179648 | tf_op jit(solution)/shard_map/scatter | solution.py:268
  127.0 8.0 %all-to-all-start.2 = ((bf16[128,24,128]{2,1,0:T(8,128)(2,1)}), bf16[128,24,128]{2,1,0:T(8,128)(2,1)S(1)}, u32[]{:S(2)}, u32[]{:S(2)}) async-start(bf16[128,24,128]{2,1,0:T(8,128)(2,1)} %bitcast.70), calls=%async_computation.2 | async-start | bytes 1572864 | tf_op jit(solution)/shard_map/all_to_all | solution.py:270
  135.1 27.4 %all-to-all-done.2 = bf16[128,24,128]{2,1,0:T(8,128)(2,1)S(1)} async-done(((bf16[128,24,128]{2,1,0:T(8,128)(2,1)}), bf16[128,24,128]{2,1,0:T(8,128)(2,1)S(1)}, u32[]{:S(2)}, u32[]{:S(2)}) %all-to-all-start.2) | async-done | bytes 786464 | tf_op jit(solution)/shard_map/all_to_all | solution.py:270
  164.3 4.9 %all-to-all-start.3 = ((f32[16,15,128]{2,1,0:T(8,128)}), f32[16,15,128]{2,1,0:T(8,128)S(1)}, u32[]{:S(2)}, u32[]{:S(2)}) async-start(f32[16,15,128]{2,1,0:T(8,128)} %broadcast_in_dim.11), calls=%async_computation.3 | async-start | bytes 262144 | tf_op jit(solution)/shard_map/all_to_all | solution.py:32
  170.4 8.0 %all-to-all-done.3 = f32[16,15,128]{2,1,0:T(8,128)S(1)} async-done(((f32[16,15,128]{2,1,0:T(8,128)}), f32[16,15,128]{2,1,0:T(8,128)S(1)}, u32[]{:S(2)}, u32[]{:S(2)}) %all-to-all-start.3) | async-done | bytes 122912 | tf_op jit(solution)/shard_map/all_to_all | solution.py:32
  178.5 0.7 add_rsqrt_fusion.1
  179.2 0.8 multiply_convert_fusion.1
  (40 shorter events, 3.8 us)
Async XLA Ops:
  0.0 96.8 %copy-start = (bf16[1,2048,320]{1,2,0:T(8,128)(2,1)S(1)}, bf16[1,2048,320]{1,2,0:T(8,128)(2,1)}, u32[]{:S(2)}) copy-start(bf16[1,2048,320]{1,2,0:T(8,128)(2,1)} %param.28) | copy-start | bytes 3932164
  0.0 58.3 %copy-start.1 = (bf16[1,320,2048]{2,1,0:T(8,128)(2,1)S(1)}, bf16[1,320,2048]{2,1,0:T(8,128)(2,1)}, u32[]{:S(2)}) copy-start(bf16[1,320,2048]{2,1,0:T(8,128)(2,1)} %param.30) | copy-start | bytes 3932164
  3.4 36.8 %all-to-all-start = ((bf16[16,64,128]{2,1,0:T(8,128)(2,1)}), bf16[16,64,128]{2,1,0:T(8,128)(2,1)S(1)}, u32[]{:S(2)}, u32[]{:S(2)}) async-start(bf16[16,64,128]{2,1,0:T(8,128)(2,1)} %bitcast_bitcast_fusion), calls=%async_computation | async-start | bytes 524288 | tf_op jit(solution)/shard_map/all_to_all | solution.py:190
  13.5 2.7 %collective-permute-start = (bf16[80,128]{1,0:T(8,128)(2,1)}, bf16[80,128]{1,0:T(8,128)(2,1)S(1)}, u32[]{:S(2)}, u32[]{:S(2)}) collective-permute-start(bf16[80,128]{1,0:T(8,128)(2,1)} %get-tuple-element.45), channel_id=1, source_target_pairs={{0,16},{16,32},{32,48},{48,64},{64,80},{80,96},{96,112},{112,128},... | collective-permute-start | bytes 61448 | tf_op jit(solution)/shard_map/ppermute | solution.py:23
  16.2 0.6 copy-start.5
  40.1 0.7 copy-start.3
  43.7 25.2 %all-to-all-start.1 = ((bf16[32,24,128]{2,1,0:T(8,128)(2,1)}), bf16[32,24,128]{2,1,0:T(8,128)(2,1)S(1)}, u32[]{:S(2)}, u32[]{:S(2)}) async-start(bf16[32,24,128]{2,1,0:T(8,128)(2,1)} %get-tuple-element.49), calls=%async_computation.1 | async-start | bytes 393216 | tf_op jit(solution)/shard_map/all_to_all | solution.py:218
  58.3 44.0 %collective-permute-start.2 = (bf16[320,2048]{1,0:T(8,128)(2,1)S(1)}, bf16[320,2048]{1,0:T(8,128)(2,1)}, u32[]{:S(2)}, u32[]{:S(2)}) collective-permute-start(bf16[320,2048]{1,0:T(8,128)(2,1)S(1)} %bitcast.69), channel_id=1, source_target_pairs={{0,1},{1,0},{2,3},{3,2},{4,5},{5,4},{6,7},{7,6},{8,9},{9,8},{10,11... | collective-permute-start | bytes 3932168 | tf_op jit(solution)/shard_map/ppermute | solution.py:27
  69.0 27.9 %copy-start.6 = (f32[2048]{0:T(1024)S(1)}, f32[2048]{0:T(1024)}, u32[]{:S(2)}) copy-start(f32[2048]{0:T(1024)} %param.25) | copy-start | bytes 24580
  96.9 1.6 copy-start.10
  100.2 3.9 %copy-start.2 = (bf16[320,768]{1,0:T(8,128)(2,1)}, bf16[320,768]{1,0:T(8,128)(2,1)S(1)}, u32[]{:S(2)}) copy-start(bf16[320,768]{1,0:T(8,128)(2,1)S(1)} %fusion.8.mine_ref) | copy-start | bytes 1474564
  100.2 3.9 %collective-permute-start.1 = (bf16[320,768]{1,0:T(8,128)(2,1)S(1)}, bf16[320,768]{1,0:T(8,128)(2,1)}, u32[]{:S(2)}, u32[]{:S(2)}) collective-permute-start(bf16[320,768]{1,0:T(8,128)(2,1)S(1)} %fusion.8.mine_ref), channel_id=1, source_target_pairs={{0,1},{1,0},{2,3},{3,2},{4,5},{5,4},{6,7},{7,6},{8,9},{9,8},{10,11... | collective-permute-start | bytes 1474568 | tf_op jit(solution)/shard_map/ppermute | solution.py:27
  107.8 13.3 %collective-permute-start.3 = (bf16[16,4,24,128]{3,2,1,0:T(8,128)(2,1)}, bf16[16,4,24,128]{3,2,1,0:T(8,128)(2,1)S(1)}, u32[]{:S(2)}, u32[]{:S(2)}) collective-permute-start(bf16[16,4,24,128]{3,2,1,0:T(8,128)(2,1)} %get-tuple-element.53), channel_id=1, source_target_pairs={{0,2},{2,0},{4,6},{6,4},{8,10},{10,8},{12,14},{14,12},{1,3},{3,1},... | collective-permute-start | bytes 1179656 | tf_op jit(solution)/shard_map/ppermute | solution.py:263
  111.6 13.6 %collective-permute-start.4 = (bf16[16,4,24,128]{3,2,1,0:T(8,128)(2,1)}, bf16[16,4,24,128]{3,2,1,0:T(8,128)(2,1)S(1)}, u32[]{:S(2)}, u32[]{:S(2)}) collective-permute-start(bf16[16,4,24,128]{3,2,1,0:T(8,128)(2,1)} %get-tuple-element.54), channel_id=1, source_target_pairs={{0,14},{2,4},{4,2},{6,8},{8,6},{10,12},{12,10},{14,0},{1,15},{3,5}... | collective-permute-start | bytes 1179656 | tf_op jit(solution)/shard_map/ppermute | solution.py:264
  117.3 17.8 %copy-start.7 = (f32[192,2]{0,1:T(2,128)S(1)}, f32[192,2]{0,1:T(2,128)}, u32[]{:S(2)}) copy-start(f32[192,2]{0,1:T(2,128)} %param.27) | copy-start | bytes 4612
  117.3 17.8 %copy-start.8 = (s32[2,192]{1,0:T(2,128)S(1)}, s32[2,192]{1,0:T(2,128)}, u32[]{:S(2)}) copy-start(s32[2,192]{1,0:T(2,128)} %get-tuple-element.48) | copy-start | bytes 4612
  117.3 45.6 %copy-start.4 = (f32[192,128]{1,0:T(8,128)S(1)}, f32[192,128]{1,0:T(8,128)}, u32[]{:S(2)}) copy-start(f32[192,128]{1,0:T(8,128)} %get-tuple-element.47) | copy-start | bytes 294916
  123.0 56.2 %copy-start.9 = (f32[128]{0:T(128)S(1)}, f32[128]{0:T(128)}, u32[]{:S(2)}) copy-start(f32[128]{0:T(128)} %param.31) | copy-start | bytes 1540
  127.0 35.6 %all-to-all-start.2 = ((bf16[128,24,128]{2,1,0:T(8,128)(2,1)}), bf16[128,24,128]{2,1,0:T(8,128)(2,1)S(1)}, u32[]{:S(2)}, u32[]{:S(2)}) async-start(bf16[128,24,128]{2,1,0:T(8,128)(2,1)} %bitcast.70), calls=%async_computation.2 | async-start | bytes 1572864 | tf_op jit(solution)/shard_map/all_to_all | solution.py:270
  164.3 14.1 %all-to-all-start.3 = ((f32[16,15,128]{2,1,0:T(8,128)}), f32[16,15,128]{2,1,0:T(8,128)S(1)}, u32[]{:S(2)}, u32[]{:S(2)}) async-start(f32[16,15,128]{2,1,0:T(8,128)} %broadcast_in_dim.11), calls=%async_computation.3 | async-start | bytes 262144 | tf_op jit(solution)/shard_map/all_to_all | solution.py:32
